TPU v7x, 256 devices: a whole 4x4x8 slice. The times are simulated.
256 devices in a mesh: ep: 64 (over z, x, core), tp: 4 (over y).
Axes of the slice: x: 4, y: 4, z: 8, core: 2. Of those that a mesh axis runs over, the one named last changes fastest.
Arguments:
- tokens: bfloat16 [1536, 4096], P('ep'), may hold values from -6 to 6
- norm_gain: bfloat16 [4096], replicated, may hold values from 0.099609375 to 1.8984375
- w_query: bfloat16 [4096, 1024], P('ep', 'tp'), may hold values from -0.09375 to 0.09375
- w_key: bfloat16 [4096, 1024], P('ep', 'tp'), may hold values from -0.09375 to 0.09375
- w_value: bfloat16 [4096, 2048], P('ep', 'tp'), may hold values from -0.09375 to 0.09375
- w_rgate: bfloat16 [4096, 2048], P('ep', 'tp'), may hold values from -0.09375 to 0.09375
- w_decay: bfloat16 [4096, 1024], P('ep', 'tp'), may hold values from -0.375 to 0.375
- decay_shift: float32 [1536, 1024], P('ep', 'tp'), may hold values from -2 to 0
- state: float32 [1536, 8, 128, 256], P('ep', 'tp'), may hold values from -6 to 6
- head_gain: bfloat16 [2048], P('tp'), may hold values from 0.099609375 to 1.8984375
- w_out: bfloat16 [2048, 4096], P('tp', 'ep'), may hold values from -0.125 to 0.125
- ffn_gain: bfloat16 [4096], replicated, may hold values from 0.099609375 to 1.8984375
- w_gate: bfloat16 [64, 4096, 1024], P('ep', None, 'tp'), may hold values from -0.21875 to 0.21875
- w_lin: bfloat16 [64, 4096, 1024], P('ep', None, 'tp'), may hold values from -0.21875 to 0.21875
- w_down: bfloat16 [64, 1024, 4096], P('ep', 'tp'), may hold values from -0.046875 to 0.046875
- expert_ids: int32 [1536, 4], P('ep'), may hold values from 0 to 63, all different within a row; in each aligned block of 24 rows (0 to 23, 24 to 47, ...) at most 3 rows name the same one
- route_weight: float32 [1536, 4], P('ep'), may hold values from 0.2 to 1
Outputs:
- result: bfloat16 [1536, 4096], P('ep')
Inputs may be any that keep to these rules, and one draw needn't show every extreme that they name: `expert_ids`: each row names 4 different experts; among the rows of one index of ep no expert is named more than 3 times, a bound that some block reaches.
All inputs are finite; a program needn't handle non-finite values.
Results may differ from a plain program's by a relative error of at most 0.022.
Values may be sent and summed in bfloat16 or wider, within the bound.
No kernel may reach another device: no remote copies, remote signals or barrier semaphores. Data moves between devices by JAX's collectives and lax.ppermute only.
A program may use at most 128 MiB of HBM per device.

v0:
```python
import functools
import jax
import jax.numpy as jnp
from jax import lax
from jax.experimental import pallas as pl
from jax.experimental.pallas import tpu as pltpu
from jax.sharding import Mesh
from jax.sharding import PartitionSpec as P


EP = ("ep_0", "ep_1", "ep_2")
Z, X, C, T = "ep_0", "ep_1", "ep_2", "tp"

eps = 1e-06
tau = 16.0
limit = 7.0
glu_alpha = 1.702
CAP = 3

f32 = jnp.float32
bf16 = jnp.bfloat16


def shift(value, axis, by):
    n = lax.axis_size(axis)
    return lax.ppermute(value, axis, [(i, (i + by) % n) for i in range(n)])


def order_of(n):
    return sorted(range(1, n), key=lambda s: (-min(s, n - s), s))


VMEM = pl.BlockSpec(memory_space=pltpu.VMEM)
SMEM = pl.BlockSpec(memory_space=pltpu.SMEM)
ANY = pl.BlockSpec(memory_space=pl.ANY)


def shaped(shape, dtype):
    return jax.ShapeDtypeStruct(shape, dtype)


def cost(flops, moved):
    return pl.CostEstimate(flops=int(flops), bytes_accessed=int(moved), transcendentals=0)


def pack_kernel(*refs):
    out, at = refs[-1], 0
    for ref in refs[:-1]:
        out[:, at : at + ref.shape[1]] = ref[...]
        at += ref.shape[1]


def pack(arrays):
    rows = arrays[0].shape[0]
    cols = sum(a.shape[1] for a in arrays)
    return pl.pallas_call(
        pack_kernel,
        out_shape=shaped((rows, cols), arrays[0].dtype),
        cost_estimate=cost(1e6, 4 * rows * cols),
        name="pack",
    )(*arrays)


def scale_kernel(tokens, gain, out, scale):
    values = tokens[...].astype(f32)
    meansq = jnp.mean(values * values, axis=-1, keepdims=True)
    scale[...] = jnp.broadcast_to(lax.rsqrt(meansq + eps), scale.shape)
    values = (values * gain[...].astype(f32)).astype(bf16)
    cols = out.shape[2]
    for i in range(out.shape[0]):
        out[i] = values[:, i * cols : (i + 1) * cols]


def scale(tokens, gain, nz):
    seqs, width = tokens.shape
    return pl.pallas_call(
        scale_kernel,
        out_shape=[shaped((nz, seqs, width // nz), bf16), shaped((seqs, 128), f32)],
        cost_estimate=cost(1e6, 4 * seqs * width),
        name="scale",
    )(tokens, gain[None])


def split_kernel(nz, where, down, *outs):
    nt = len(outs)
    chunk = outs[0].shape[1] // nz
    for s in range(nt):
        other = lax.rem(where[3] + s, nt)
        for i in range(nz):
            at = pl.multiple_of((i * nt + other) * chunk, chunk)
            outs[s][:, i * chunk : (i + 1) * chunk] = down[:, pl.ds(at, chunk)]


def split(where, down, nz, nt):
    rows, cols = down.shape
    return pl.pallas_call(
        functools.partial(split_kernel, nz),
        out_shape=[shaped((rows, cols // nt), bf16)] * nt,
        in_specs=[SMEM, VMEM],
        out_specs=[VMEM] * nt,
        cost_estimate=cost(1e6, 4 * rows * cols),
        name="split",
    )(where, down)


def project_kernel(nz, nx, where, tok, *refs):
    own, other = refs[:nx], refs[nx : 2 * nx]
    outs = refs[2 * nx : 2 * nx + nz]
    weight, turned = refs[-2:]
    z, x, c = where[0], where[1], where[2]
    rows = own[0].shape[0]
    seqs = outs[0].shape[0]
    for i in range(nx):
        base = lax.rem(x - i + nx, nx) * (2 * rows)
        weight[pl.ds(pl.multiple_of(base + c * rows, rows), rows), :] = own[i][...]
        weight[pl.ds(pl.multiple_of(base + (1 - c) * rows, rows), rows), :] = other[i][...]
    for s in range(nz):
        turned[s * seqs : (s + 1) * seqs, :] = tok[lax.rem(z + s, nz)].astype(f32)
    total = jnp.dot(turned[...].astype(bf16), weight[...], preferred_element_type=f32)
    for s in range(nz):
        outs[s][...] = total[s * seqs : (s + 1) * seqs, :].astype(bf16)


def project(where, tok, own, other):
    nz, seqs, depth = tok.shape
    nx, cols = len(own), own[0].shape[1]
    return pl.pallas_call(
        functools.partial(project_kernel, nz, nx),
        out_shape=[shaped((seqs, cols), bf16)] * nz,
        in_specs=[SMEM] + [VMEM] * (1 + 2 * nx),
        out_specs=[VMEM] * nz,
        scratch_shapes=[pltpu.VMEM((depth, cols), bf16), pltpu.VMEM((nz * seqs, depth), f32)],
        cost_estimate=cost(2 * nz * seqs * depth * cols, 2 * depth * cols),
        name="project",
    )(where, tok, *own, *other)


def join_kernel(*refs):
    for i, ref in enumerate(refs[:-1]):
        refs[-1][i] = ref[...]


def join(arrays):
    shape = (len(arrays), *arrays[0].shape)
    return pl.pallas_call(
        join_kernel,
        out_shape=shaped(shape, arrays[0].dtype),
        cost_estimate=cost(1e6, 4 * len(arrays) * arrays[0].size),
        name="join",
    )(*arrays)


def mix_kernel(nx, where, gated, partner, *refs):
    blocks = refs[:nx]
    outs = refs[nx : 2 * nx]
    weight, sems = refs[-2:]
    z, x, t = where[0], where[1], where[3]
    pairs = weight.shape[1]
    copies = []
    for i in range(nx):
        for r in range(pairs):
            copy = pltpu.make_async_copy(
                blocks[i].at[r],
                weight.at[lax.rem(x - i + nx, nx), lax.rem(lax.div(z, 2) - r + pairs, pairs)],
                sems.at[i, r],
            )
            copy.start()
            copies.append(copy)
    rows = jnp.concatenate([gated[...], partner[...]], axis=0)
    for copy in copies:
        copy.wait()
    depth, cols = weight.shape[4], pairs * 2 * weight.shape[3]
    for s in range(nx):
        block = weight[lax.rem(t + s, nx)].reshape(cols, depth)
        outs[s][...] = lax.dot_general(
            rows, block, (((1,), (1,)), ((), ())), preferred_element_type=f32
        ).astype(bf16)


def mix(where, gated, partner, blocks):
    nx = len(blocks)
    pairs, two, rows, depth = blocks[0].shape
    cols = pairs * two * rows
    seqs = 2 * gated.shape[0]
    return pl.pallas_call(
        functools.partial(mix_kernel, nx),
        out_shape=[shaped((seqs, cols), bf16)] * nx,
        in_specs=[SMEM, VMEM, VMEM] + [ANY] * nx,
        out_specs=[VMEM] * nx,
        scratch_shapes=[
            pltpu.VMEM((nx, pairs, two, rows, depth), bf16),
            pltpu.SemaphoreType.DMA((nx, pairs)),
        ],
        cost_estimate=cost(2 * seqs * cols * nx * depth, 2 * cols * nx * depth),
        name="mix",
    )(where, gated, partner, *blocks)


def put_rows(values, wide):
    chunks = values.shape[1] // 128
    for j in range(chunks):
        wide[pl.ds(j, values.shape[0], stride=chunks), :] = values[:, j * 128 : (j + 1) * 128]
    return wide[...].astype(bf16)


def dispatch_kernel(nz, nt, where, tokens, gain, sender, mine, other, out, stream, wide):
    c, t = where[2], where[3]
    chunk = stream.shape[1] // nz
    half = chunk // 2
    first, second = mine[...].astype(f32), other[...].astype(f32)
    first, second = jnp.where(c == 0, first, second), jnp.where(c == 0, second, first)
    for i in range(nz):
        own = tokens[:, pl.ds(pl.multiple_of((i * nt + t) * chunk, chunk), chunk)]
        at = slice(i * half, (i + 1) * half)
        mixed = jnp.concatenate([first[:, at], second[:, at]], axis=1)
        stream[:, i * chunk : (i + 1) * chunk] = own.astype(f32) + mixed
    rows = jnp.dot(
        sender[...], (stream[...] * gain[t]).astype(bf16), preferred_element_type=f32
    )
    out[...] = put_rows(rows, wide)


def dispatch(where, tokens, gain, sender, mine, other, nz, nt):
    slots, seqs = sender.shape
    part = 2 * mine.shape[1]
    wide = slots * part // 128
    return pl.pallas_call(
        functools.partial(dispatch_kernel, nz, nt),
        out_shape=[shaped((wide, 128), bf16), shaped((seqs, part), f32)],
        in_specs=[SMEM] + [VMEM] * 5,
        out_specs=[VMEM] * 2,
        scratch_shapes=[pltpu.VMEM((wide, 128), f32)],
        cost_estimate=cost(2 * slots * seqs * part, 6 * slots * part),
        name="dispatch",
    )(where, tokens, gain, sender, mine, other)


def unpack_kernel(rows, out, wide):
    wide[...] = rows[...].astype(f32)
    chunks = out.shape[1] // 128
    for j in range(chunks):
        out[:, j * 128 : (j + 1) * 128] = wide[
            pl.ds(j, out.shape[0], stride=chunks), :
        ].astype(bf16)


def unpack(rows, slots):
    part = rows.shape[0] * 128 // slots
    return pl.pallas_call(
        unpack_kernel,
        out_shape=shaped((slots, part), bf16),
        scratch_shapes=[pltpu.VMEM(rows.shape, f32)],
        cost_estimate=cost(1e6, 4 * slots * part),
        name="unpack",
    )(rows)


def expert_kernel(steps, nt, last, where, inverse, w_gate, w_lin, *refs):
    count = len(steps)
    pieces, refs = refs[:count], refs[count:]
    if last:
        before, refs = refs[:3], refs[3:]
    outs, (gates, lins, sems) = refs[:-3], refs[-3:]
    t = where[3]
    copies = []
    for i, s in enumerate(steps):
        at = lax.rem(t - s + nt, nt)
        pair = (
            pltpu.make_async_copy(w_gate.at[:, at], gates.at[i], sems.at[i, 0]),
            pltpu.make_async_copy(w_lin.at[:, at], lins.at[i], sems.at[i, 1]),
        )
        for copy in pair:
            copy.start()
        copies.append(pair)
    if last:
        gate, lin, sumsq = before[0][...], before[1][...], before[2][:, :1]
    else:
        gate, lin, sumsq = 0.0, 0.0, 0.0
    units = w_gate.shape[-1]
    for i, s in enumerate(steps):
        at = lax.rem(t - s + nt, nt)
        piece = pieces[i][...]
        plain = piece.astype(f32) * inverse[at]
        sumsq = sumsq + jnp.sum(plain * plain, axis=-1, keepdims=True)
        copies[i][0].wait()
        gate = gate + jnp.dot(
            piece, gates[i].reshape(piece.shape[1], units), preferred_element_type=f32
        )
        copies[i][1].wait()
        lin = lin + jnp.dot(
            piece, lins[i].reshape(piece.shape[1], units), preferred_element_type=f32
        )
    if last:
        width = nt * pieces[0].shape[1]
        scale = lax.rsqrt(sumsq / width + eps)
        gate = jnp.minimum(gate * scale, limit)
        lin = jnp.clip(lin * scale, -limit, limit)
        outs[0][...] = (gate * jax.nn.sigmoid(glu_alpha * gate) * (lin + 1.0)).astype(bf16)
    else:
        outs[0][...] = gate
        outs[1][...] = lin
        outs[2][...] = jnp.broadcast_to(sumsq, outs[2].shape)


def expert(where, inverse, w_gate, w_lin, steps, pieces, before):
    nz, nt, chunk, units = w_gate.shape
    slots, part = pieces[0].shape
    last = before is not None
    out_shape = (
        [shaped((slots, units), bf16)]
        if last
        else [shaped((slots, units), f32)] * 2 + [shaped((slots, 128), f32)]
    )
    count = len(steps)
    return pl.pallas_call(
        functools.partial(expert_kernel, steps, nt, last),
        out_shape=out_shape,
        in_specs=[SMEM, VMEM, ANY, ANY] + [VMEM] * (count + (3 if last else 0)),
        out_specs=[VMEM] * len(out_shape),
        scratch_shapes=[
            pltpu.VMEM((count, nz, chunk, units), bf16),
            pltpu.VMEM((count, nz, chunk, units), bf16),
            pltpu.SemaphoreType.DMA((count, 2)),
        ],
        cost_estimate=cost(4 * count * slots * part * units, 4 * count * part * units),
        name="expert_last" if last else "expert_first",
    )(where, inverse, w_gate, w_lin, *pieces, *(before or ()))


def down_kernel(nt, *refs):
    acts, downs = refs[:nt], refs[nt : 2 * nt]
    out, wide = refs[2 * nt :]
    total = jnp.dot(acts[0][...], downs[0][...], preferred_element_type=f32)
    for s in range(1, nt):
        total = total + jnp.dot(acts[s][...], downs[s][...], preferred_element_type=f32)
    out[...] = put_rows(total, wide)


def down_sum(acts, downs):
    nt = len(acts)
    slots, units = acts[0].shape
    part = downs[0].shape[1]
    wide = slots * part // 128
    return pl.pallas_call(
        functools.partial(down_kernel, nt),
        out_shape=shaped((wide, 128), bf16),
        scratch_shapes=[pltpu.VMEM((wide, 128), f32)],
        cost_estimate=cost(2 * nt * slots * units * part, 2 * nt * units * part),
        name="down",
    )(*acts, *downs)


def combine_kernel(rows, weights, stream, out, wide):
    wide[...] = rows[...].astype(f32)
    seqs, part = out.shape
    chunks = part // 128
    slots = wide.shape[0] // chunks
    for j in range(chunks):
        values = wide[pl.ds(j, slots, stride=chunks), :].astype(bf16)
        sums = jnp.dot(weights[...], values, preferred_element_type=f32)
        routed = sums[:seqs] + sums[seqs : 2 * seqs] + sums[2 * seqs :]
        at = slice(j * 128, (j + 1) * 128)
        out[:, at] = (stream[:, at] + routed).astype(bf16)


def combine(rows, weights, stream):
    return pl.pallas_call(
        combine_kernel,
        out_shape=shaped(stream.shape, bf16),
        scratch_shapes=[pltpu.VMEM(rows.shape, f32)],
        cost_estimate=cost(2 * weights.size * stream.shape[1], 2 * rows.size),
        name="combine",
    )(rows, weights, stream)


def finish_kernel(nz, where, *refs):
    pieces, out = refs[:-1], refs[-1]
    nt = len(pieces)
    chunk = pieces[0].shape[1] // nz
    for s in range(nt):
        other = lax.rem(where[3] - s + nt, nt)
        for i in range(nz):
            at = pl.multiple_of((i * nt + other) * chunk, chunk)
            out[:, pl.ds(at, chunk)] = pieces[s][:, i * chunk : (i + 1) * chunk]


def finish(where, pieces, nz):
    seqs, part = pieces[0].shape
    return pl.pallas_call(
        functools.partial(finish_kernel, nz),
        out_shape=shaped((seqs, part * len(pieces)), bf16),
        in_specs=[SMEM] + [VMEM] * len(pieces),
        out_specs=VMEM,
        cost_estimate=cost(1e6, 4 * seqs * part * len(pieces)),
        name="finish",
    )(where, *pieces)


def attention(arrived, first_scale, decay_shift, state, head_gain, key_cols, val_cols):
    seq_dev, heads_dev, key_dim, val_dim = state.shape
    projected = functools.reduce(jnp.add, [a.astype(f32) for a in arrived]) * first_scale
    q_rows = projected[:, :key_cols].reshape(seq_dev, heads_dev, key_dim) * key_dim ** (-0.5)
    k_rows = projected[:, key_cols : 2 * key_cols].reshape(seq_dev, heads_dev, key_dim)
    decay_pre = projected[:, 2 * key_cols : 3 * key_cols]
    v_rows = projected[:, 3 * key_cols : 3 * key_cols + val_cols].reshape(
        seq_dev, heads_dev, val_dim
    )
    rgates = projected[:, 3 * key_cols + val_cols :].reshape(seq_dev, heads_dev, val_dim)
    log_decay = jax.nn.log_sigmoid(decay_pre) / tau + decay_shift
    new_state = (
        jnp.exp(log_decay.reshape(seq_dev, heads_dev, key_dim))[..., None] * state
        + k_rows[..., None] * v_rows[:, :, None, :]
    )
    read = jnp.einsum("shk,shkv->shv", q_rows, new_state)
    read_sq = jnp.mean(read * read, axis=-1, keepdims=True)
    gated = (
        read
        * lax.rsqrt(read_sq + eps)
        * head_gain.astype(f32).reshape(heads_dev, val_dim)
        * jax.nn.silu(rgates)
    )
    return gated.reshape(seq_dev, heads_dev * val_dim).astype(bf16)


def to_bf16(value):
    return lax.reduce_precision(value, 8, 7)


def routing(expert_ids, route_weight, n_ep):
    seq_dev, top = expert_ids.shape
    flat_ids = expert_ids.reshape(-1)
    onehot = (flat_ids[:, None] == jnp.arange(n_ep, dtype=jnp.int32)[None, :]).astype(jnp.int32)
    rank = jnp.sum((jnp.cumsum(onehot, axis=0) - onehot) * onehot, axis=1)
    slot_of = (flat_ids * CAP + rank).reshape(seq_dev, top)
    slots = n_ep * CAP
    hits = jnp.arange(slots, dtype=jnp.int32)[None, None, :] == slot_of[:, :, None]
    sender = jnp.sum(hits.astype(f32), axis=1).T.astype(bf16)
    weights = jnp.sum(jnp.where(hits, route_weight[:, :, None], 0.0), axis=1)
    high = to_bf16(weights)
    middle = to_bf16(weights - high)
    low = weights - high - middle
    return sender, jnp.concatenate([high, middle, low], axis=0).astype(bf16)


def on_device(
    tokens,
    norm_gain,
    w_query,
    w_key,
    w_value,
    w_rgate,
    w_decay,
    decay_shift,
    state,
    head_gain,
    w_out,
    ffn_gain,
    w_gate,
    w_lin,
    w_down,
    expert_ids,
    route_weight,
):
    width = tokens.shape[1]
    nz, nx, nt = lax.axis_size(Z), lax.axis_size(X), lax.axis_size(T)
    n_ep = lax.axis_size(EP)
    slots = n_ep * CAP
    part = width // nt
    chunk = part // nz
    where = jnp.stack([lax.axis_index(a) for a in (Z, X, C, T)]).astype(jnp.int32)

    packed = pack((w_query, w_key, w_decay, w_value, w_rgate))
    own = [packed] + [shift(packed, X, i) for i in range(1, nx)]
    other = [shift(packed, C, 1)]
    other += [shift(w, C, 1) for w in own[1:]]

    tok_parts, first_scale = scale(tokens, norm_gain, nz)
    tok = lax.all_to_all(tok_parts, Z, 0, 0, tiled=True)

    out_t = w_out.T
    near = lax.ppermute(out_t, Z, [(i, i ^ 1) for i in range(nz)])
    odd = lax.rem(lax.axis_index(Z), 2) == 1
    pair = jnp.where(odd, jnp.stack([near, out_t]), jnp.stack([out_t, near]))
    pairs = [pair] + [shift(pair, Z, 2 * i) for i in order_of(nz // 2)]
    pairs = [pairs[0]] + [pairs[1 + order_of(nz // 2).index(i)] for i in range(1, nz // 2)]
    out_z = join(pairs)
    blocks = [out_z] + [shift(out_z, X, i) for i in range(1, nx)]

    downs = split(where, w_down[0], nz, nt)
    downs = [downs[0]] + [shift(downs[s], T, s) for s in range(1, nt)]

    sender, weights = routing(expert_ids, route_weight, n_ep)
    gain_of = ffn_gain.astype(f32).reshape(nz, nt, chunk)
    gain_of = jnp.moveaxis(gain_of, 1, 0).reshape(nt, 1, part)
    inverse = 1.0 / gain_of

    parts = project(where, tok, own, other)
    arrived = [parts[0]] + [shift(parts[s], Z, s) for s in order_of(nz)]
    gated = attention(
        arrived,
        first_scale[:, :1],
        decay_shift,
        state,
        head_gain,
        w_query.shape[1],
        w_value.shape[1],
    )
    partner = shift(gated, C, 1)
    mixed = mix(where, gated, partner, blocks)
    mixed = [mixed[0]] + [shift(mixed[s], T, s) for s in range(1, nt)]
    seqs = gated.shape[0]
    mine = functools.reduce(jnp.add, [m[:seqs].astype(f32) for m in mixed]).astype(bf16)
    theirs = functools.reduce(jnp.add, [m[seqs:].astype(f32) for m in mixed]).astype(bf16)
    other_half = shift(theirs, C, 1)
    outbound, stream = dispatch(
        where, tokens, gain_of, sender, mine, other_half, nz, nt
    )
    rows = lax.all_to_all(outbound.reshape(n_ep, -1, 128), EP, 0, 0, tiled=True).reshape(-1, 128)
    rows = unpack(rows, slots)
    pieces = [rows] + [shift(rows, T, s) for s in range(1, nt)]
    gates = w_gate.reshape(nz, nt, chunk, -1)
    lins = w_lin.reshape(nz, nt, chunk, -1)
    steps = [s for s in range(nt) if s != nt // 2]
    before = expert(where, inverse, gates, lins, steps, [pieces[s] for s in steps], None)
    act = expert(where, inverse, gates, lins, [nt // 2], [pieces[nt // 2]], before)[0]
    acts = [act] + [shift(act, T, s) for s in range(1, nt)]
    done = down_sum(acts, downs)
    returned = lax.all_to_all(done.reshape(n_ep, -1, 128), EP, 0, 0, tiled=True).reshape(-1, 128)
    result = combine(returned, weights, stream)
    results = [result] + [shift(result, T, s) for s in range(1, nt)]
    return finish(where, results, nz)


def solution(mesh):
    sizes = dict(mesh.shape)
    torus = Mesh(
        mesh.devices.reshape(sizes.get("z", 8), sizes.get("x", 4), 2, sizes["tp"]),
        (Z, X, C, T),
    )
    return jax.shard_map(
        on_device,
        mesh=torus,
        in_specs=(
            P(EP, None),
            P(),
            P(EP, T),
            P(EP, T),
            P(EP, T),
            P(EP, T),
            P(EP, T),
            P(EP, T),
            P(EP, T, None, None),
            P(T),
            P(T, EP),
            P(),
            P(EP, None, T),
            P(EP, None, T),
            P(EP, T, None),
            P(EP, None),
            P(EP, None),
        ),
        out_specs=P(EP, None),
        check_vma=False,
    )
```

profile of v0, /device:TPU:1, one launch (start us, length us, event | category | flops | bytes accessed | tf_op | source)
XLA Modules:
  0.0 226.4 jit_solution(6216528085466559599)
XLA Ops:
  0.0 1.6 pack.1.refs_0_
  1.6 2.0 collective-permute-start
  3.7 2.5 %collective-permute-start.1 = (bf16[64,1792]{1,0:T(8,128)(2,1)}, bf16[64,1792]{1,0:T(8,128)(2,1)S(1)}, u32[]{:S(2)}, u32[]{:S(2)}) collective-permute-start(bf16[64,1792]{1,0:T(8,128)(2,1)} %pack.1.refs_0_), channel_id=1, source_target_pairs={{0,16},{8,24},{16,0},{24,8},{1,17},{9,25},{17,1},{25,9},{2,18},{10... | collective-permute-start | bytes 688136 | tf_op jit(solution)/shard_map/ppermute | solution.py:26
  6.1 1.2 collective-permute-start.2
  7.3 1.5 collective-permute-start.3
  8.8 1.3 broadcast_in_dim.20.gain
  10.1 1.7 scale.1
  11.8 8.2 %all-to-all-start = ((bf16[8,24,512]{2,1,0:T(8,128)(2,1)}), bf16[8,24,512]{2,1,0:T(8,128)(2,1)S(1)}, u32[]{:S(2)}, u32[]{:S(2)}) async-start(bf16[8,24,512]{2,1,0:T(8,128)(2,1)} %get-tuple-element.28), calls=%async_computation | async-start | bytes 393216 | tf_op jit(solution)/shard_map/all_to_all | solution.py:478
  20.0 1.5 collective-permute-start.15
  22.4 0.9 collective-permute-start.4
  24.5 3.2 %collective-permute-done.15 = bf16[64,512]{1,0:T(8,128)(2,1)S(1)} collective-permute-done((bf16[64,512]{1,0:T(8,128)(2,1)}, bf16[64,512]{1,0:T(8,128)(2,1)S(1)}, u32[]{:S(2)}, u32[]{:S(2)}) %collective-permute-start.15) | collective-permute-done | bytes 65568 | tf_op jit(solution)/shard_map/ppermute | solution.py:481
  27.7 0.9 maximum_select_fusion.refs_0_
  29.2 4.2 %collective-permute-start.17 = (bf16[2,64,512]{2,1,0:T(8,128)(2,1)S(1)}, bf16[2,64,512]{2,1,0:T(8,128)(2,1)S(1)}, u32[]{:S(2)}, u32[]{:S(2)}) collective-permute-start(bf16[2,64,512]{2,1,0:T(8,128)(2,1)S(1)} %maximum_select_fusion.refs_0_), channel_id=1, source_target_pairs={{0,128},{32,160},{64,192},{96,224},{128,0},{160,32},{192,64},{224,... | collective-permute-start | bytes 393224 | tf_op jit(solution)/shard_map/ppermute | solution.py:26
  33.5 3.4 %collective-permute-start.18 = (bf16[2,64,512]{2,1,0:T(8,128)(2,1)S(1)}, bf16[2,64,512]{2,1,0:T(8,128)(2,1)S(1)}, u32[]{:S(2)}, u32[]{:S(2)}) collective-permute-start(bf16[2,64,512]{2,1,0:T(8,128)(2,1)S(1)} %maximum_select_fusion.refs_0_), channel_id=1, source_target_pairs={{0,192},{32,224},{64,0},{96,32},{128,64},{160,96},{192,128},{224,1... | collective-permute-start | bytes 393224 | tf_op jit(solution)/shard_map/ppermute | solution.py:26
  38.3 3.1 %project.1 = (bf16[24,1792]{1,0:T(8,128)(2,1)}, bf16[24,1792]{1,0:T(8,128)(2,1)}, bf16[24,1792]{1,0:T(8,128)(2,1)}, bf16[24,1792]{1,0:T(8,128)(2,1)}, bf16[24,17...) custom-call(s32[4]{0:T(128)} %pad_add_fusion.where, ...), custom_call_target="tpu_custom_call" | custom-call | flops 352321536 | bytes 1835008 | tf_op jit(solution)/shard_map/project/pallas_call | solution.py:127
  41.5 3.6 %collective-permute-start.11 = (bf16[24,1792]{1,0:T(8,128)(2,1)}, bf16[24,1792]{1,0:T(8,128)(2,1)S(1)}, u32[]{:S(2)}, u32[]{:S(2)}) collective-permute-start(bf16[24,1792]{1,0:T(8,128)(2,1)} %get-tuple-element.34), channel_id=1, source_target_pairs={{0,192},{32,224},{64,0},{96,32},{128,64},{160,96},{192,128},{224,1... | collective-permute-start | bytes 258056 | tf_op jit(solution)/shard_map/ppermute | solution.py:26
  46.6 1.5 collective-permute-start.12
  48.1 1.2 collective-permute-start.13
  49.4 2.8 %collective-permute-start.7 = (bf16[24,1792]{1,0:T(8,128)(2,1)}, bf16[24,1792]{1,0:T(8,128)(2,1)S(1)}, u32[]{:S(2)}, u32[]{:S(2)}) collective-permute-start(bf16[24,1792]{1,0:T(8,128)(2,1)} %get-tuple-element.30), channel_id=1, source_target_pairs={{0,128},{32,160},{64,192},{96,224},{128,0},{160,32},{192,64},{224,... | collective-permute-start | bytes 258056 | tf_op jit(solution)/shard_map/ppermute | solution.py:26
  52.5 4.2 %collective-permute-start.9 = (bf16[24,1792]{1,0:T(8,128)(2,1)}, bf16[24,1792]{1,0:T(8,128)(2,1)S(1)}, u32[]{:S(2)}, u32[]{:S(2)}) collective-permute-start(bf16[24,1792]{1,0:T(8,128)(2,1)} %get-tuple-element.32), channel_id=1, source_target_pairs={{0,160},{32,192},{64,224},{96,0},{128,32},{160,64},{192,96},{224,1... | collective-permute-start | bytes 258056 | tf_op jit(solution)/shard_map/ppermute | solution.py:26
  56.7 0.8 slice_reduce_fusion
  57.5 1.9 join.1.refs_0_
  60.4 1.9 collective-permute-start.21
  62.3 1.6 collective-permute-done.8
  63.9 1.0 add_multiply_fusion
  65.8 3.9 %fusion = f32[24,2,1,256]{3,2,1,0:T(1,128)S(1)} fusion(f32[24,2,128,1]{2,3,1,0:T(1,128)S(1)} %bitcast.50, f32[24,2,128,256]{3,2,1,0:T(8,128)} %param.25, f32[24,2,256]{2,1,0:T(2,128)S(1)} %mul.99, f32[24,2,128]{2,1,0:T(2,128)S(1)} %mul.97, f32[24,2,128]{2,1,0:T(2,128)S(1)} %exp.21), kind=kOutput, calls=%fused_computation | convolution fusion | flops 7864320 | bytes 6463488 | tf_op jit(solution)/shard_map/shk,shkv->shv/dot_general | solution.py:414
  70.0 2.1 collective-permute-start.14
  72.9 0.8 collective-permute-done.19.refs_1_
  73.7 7.7 %collective-permute-done.20.refs_2_ = bf16[4,2,64,512]{3,2,1,0:T(8,128)(2,1)S(1)} collective-permute-done((bf16[4,2,64,512]{3,2,1,0:T(8,128)(2,1)}, bf16[4,2,64,512]{3,2,1,0:T(8,128)(2,1)S(1)}, u32[]{:S(2)}, u32[]{:S(2)}) %collective-permute-start.20) | collective-permute-done | bytes 524320 | tf_op jit(solution)/shard_map/ppermute | solution.py:26
  81.4 3.9 %collective-permute-done.21.refs_3_ = bf16[4,2,64,512]{3,2,1,0:T(8,128)(2,1)S(1)} collective-permute-done((bf16[4,2,64,512]{3,2,1,0:T(8,128)(2,1)}, bf16[4,2,64,512]{3,2,1,0:T(8,128)(2,1)S(1)}, u32[]{:S(2)}, u32[]{:S(2)}) %collective-permute-start.21) | collective-permute-done | bytes 524320 | tf_op jit(solution)/shard_map/ppermute | solution.py:26
  86.1 3.9 %mix.1 = (bf16[48,512]{1,0:T(8,128)(2,1)}, bf16[48,512]{1,0:T(8,128)(2,1)}, bf16[48,512]{1,0:T(8,128)(2,1)}, bf16[48,512]{1,0:T(8,128)(2,1)}) custom-call(s32[4]{0:T(128)} %pad_add_fusion.where, bf16[24,512]{1,0:T(8,128)(2,1)} %bitcast.49, bf16[24,512]{1,0:T(8,128)(2,1)} %copy-done.29, bf16[4,2,64,512]{3,2,1,0:T(8,128)(2,1)} %join.1.refs_0_, ...), custom_call_target="tpu_custom_call" | custom-call | flops 100663296 | bytes 2097152 | tf_op jit(solution)/shard_map/mix/pallas_call | solution.py:185
  90.0 1.4 collective-permute-start.22
  91.4 2.6 %collective-permute-start.23 = (bf16[48,512]{1,0:T(8,128)(2,1)}, bf16[48,512]{1,0:T(8,128)(2,1)S(1)}, u32[]{:S(2)}, u32[]{:S(2)}) collective-permute-start(bf16[48,512]{1,0:T(8,128)(2,1)} %get-tuple-element.40), channel_id=1, source_target_pairs={{0,2},{1,3},{2,0},{3,1},{4,6},{5,7},{6,4},{7,5},{8,10},{9,11},{10,... | collective-permute-start | bytes 147464 | tf_op jit(solution)/shard_map/ppermute | solution.py:26
  94.0 1.1 collective-permute-start.24
  95.1 1.1 collective-permute-done.23
  96.2 1.1 collective-permute-done.24
  97.3 1.4 add_convert_fusion
  98.7 3.7 %collective-permute-start.25 = (bf16[24,512]{1,0:T(8,128)(2,1)S(1)}, bf16[24,512]{1,0:T(8,128)(2,1)S(1)}, u32[]{:S(2)}, u32[]{:S(2)}) collective-permute-start(bf16[24,512]{1,0:T(8,128)(2,1)S(1)} %get-tuple-element.53), channel_id=1, source_target_pairs={{0,4},{4,0},{1,5},{5,1},{2,6},{6,2},{3,7},{7,3},{8,12},{12,8},{9,1... | collective-permute-start | bytes 73736 | tf_op jit(solution)/shard_map/ppermute | solution.py:26
  104.4 2.1 dispatch.1
  106.5 21.6 %all_to_all.15 = bf16[64,24,128]{2,1,0:T(8,128)(2,1)} all-to-all(bf16[64,24,128]{2,1,0:T(8,128)(2,1)} %bitcast.44), channel_id=1, replica_groups=mesh['ep_0'=8,'ep_1'=4,'ep_2'=2,'tp'=4] {'ep_0','ep_1','ep_2'}, dimensions={0} | all-to-all | bytes 786432 | tf_op jit(solution)/shard_map/all_to_all | solution.py:518
  128.1 1.9 unpack.1.refs_0_
  130.1 3.5 %split.1 = (bf16[256,1024]{1,0:T(8,128)(2,1)}, bf16[256,1024]{1,0:T(8,128)(2,1)}, bf16[256,1024]{1,0:T(8,128)(2,1)}, bf16[256,1024]{1,0:T(8,128)(2,1)}) custom-call(s32[4]{0:T(128)} %pad_add_fusion.where, bf16[256,4096]{1,0:T(8,128)(2,1)} %bitcast.40), custom_call_target="tpu_custom_call" | custom-call | flops 1000000 | bytes 4194304 | tf_op jit(solution)/shard_map/split/pallas_call | solution.py:96
  133.6 0.9 collective-permute-start.32
  134.5 1.8 collective-permute-start.28
  136.3 2.2 collective-permute-start.33
  139.1 2.8 %collective-permute-done.27.refs_1_ = bf16[192,1024]{1,0:T(8,128)(2,1)S(1)} collective-permute-done((bf16[192,1024]{1,0:T(8,128)(2,1)}, bf16[192,1024]{1,0:T(8,128)(2,1)S(1)}, u32[]{:S(2)}, u32[]{:S(2)}) %collective-permute-start.27) | collective-permute-done | bytes 393248 | tf_op jit(solution)/shard_map/ppermute | solution.py:26
  142.1 1.3 broadcast_divide_fusion.inverse
  143.4 2.2 collective-permute-done.28.refs_2_
  146.3 5.1 %expert_first.1 = (f32[192,256]{1,0:T(8,128)}, f32[192,256]{1,0:T(8,128)}, f32[192,128]{1,0:T(8,128)}) custom-call(s32[4]{0:T(128)} %pad_add_fusion.where, f32[4,1,1024]{2,1,0:T(1,128)} %broadcast_divide_fusion.inverse, bf16[8,4,128,256]{3,2,1,0:T(8,128)(2,1)} %bitcast.36, bf16[8,4,128,256]{3,2,1,0:T(8,128)(2,1)} %bitcast.38, ...), custom_call_target="tpu_custom_call" | custom-call | flops 603979776 | bytes 3145728 | tf_op jit(solution)/shard_map/expert_first/pallas_call | solution.py:315
  151.4 22.2 %collective-permute-done.26.refs_0_ = bf16[192,1024]{1,0:T(8,128)(2,1)S(1)} collective-permute-done((bf16[192,1024]{1,0:T(8,128)(2,1)}, bf16[192,1024]{1,0:T(8,128)(2,1)S(1)}, u32[]{:S(2)}, u32[]{:S(2)}) %collective-permute-start.26) | collective-permute-done | bytes 393248 | tf_op jit(solution)/shard_map/ppermute | solution.py:26
  174.3 3.6 %expert_last.1.refs_0_ = bf16[192,256]{1,0:T(8,128)(2,1)} custom-call(s32[4]{0:T(128)} %pad_add_fusion.where, f32[4,1,1024]{2,1,0:T(1,128)} %broadcast_divide_fusion.inverse, bf16[8,4,128,256]{3,2,1,0:T(8,128)(2,1)} %bitcast.37, bf16[8,4,128,256]{3,2,1,0:T(8,128)(2,1)} %bitcast.39, bf16[192,1024]{1,0:T(8,128)(2,1)} %copy-done.11, ...), custom_call_target="tpu_custom_call" | custom-call | flops 201326592 | bytes 1048576 | tf_op jit(solution)/shard_map/expert_last/pallas_call | solution.py:315
  177.9 4.3 %collective-permute-start.29 = (bf16[192,256]{1,0:T(8,128)(2,1)}, bf16[192,256]{1,0:T(8,128)(2,1)S(1)}, u32[]{:S(2)}, u32[]{:S(2)}) collective-permute-start(bf16[192,256]{1,0:T(8,128)(2,1)} %expert_last.1.refs_0_), channel_id=1, source_target_pairs={{0,1},{1,2},{2,3},{3,0},{4,5},{5,6},{6,7},{7,4},{8,9},{9,10},{10,1... | collective-permute-start | bytes 294920 | tf_op jit(solution)/shard_map/ppermute | solution.py:26
  182.3 2.3 %collective-permute-start.30 = (bf16[192,256]{1,0:T(8,128)(2,1)}, bf16[192,256]{1,0:T(8,128)(2,1)S(1)}, u32[]{:S(2)}, u32[]{:S(2)}) collective-permute-start(bf16[192,256]{1,0:T(8,128)(2,1)} %expert_last.1.refs_0_), channel_id=1, source_target_pairs={{0,2},{1,3},{2,0},{3,1},{4,6},{5,7},{6,4},{7,5},{8,10},{9,11},{10,... | collective-permute-start | bytes 294920 | tf_op jit(solution)/shard_map/ppermute | solution.py:26
  185.6 2.5 %collective-permute-done.30.refs_2_ = bf16[192,256]{1,0:T(8,128)(2,1)S(1)} collective-permute-done((bf16[192,256]{1,0:T(8,128)(2,1)}, bf16[192,256]{1,0:T(8,128)(2,1)S(1)}, u32[]{:S(2)}, u32[]{:S(2)}) %collective-permute-start.30) | collective-permute-done | bytes 98336 | tf_op jit(solution)/shard_map/ppermute | solution.py:26
  188.1 1.4 collective-permute-done.31.refs_3_
  190.1 3.1 %down.1 = bf16[1536,128]{1,0:T(8,128)(2,1)} custom-call(bf16[192,256]{1,0:T(8,128)(2,1)} %expert_last.1.refs_0_, bf16[192,256]{1,0:T(8,128)(2,1)} %copy-done.23, bf16[192,256]{1,0:T(8,128)(2,1)} %copy-done.24, bf16[192,256]{1,0:T(8,128)(2,1)} %copy-done.25, bf16[256,1024]{1,0:T(8,128)(2,1)} %get-tuple-element.46.refs_4_, bf16[256,1024]{1,0:T(8,128)(2,1)} %copy-done.5, ...), custom_call_target="tpu_custom_call" | custom-call | flops 402653184 | bytes 2097152 | tf_op jit(solution)/shard_map/down/pallas_call | solution.py:344
  193.2 6.6 %all-to-all-start.2 = ((bf16[64,24,128]{2,1,0:T(8,128)(2,1)}), bf16[64,24,128]{2,1,0:T(8,128)(2,1)S(1)}, u32[]{:S(2)}, u32[]{:S(2)}) async-start(bf16[64,24,128]{2,1,0:T(8,128)(2,1)} %bitcast.43), calls=%async_computation.2 | async-start | bytes 786432 | tf_op jit(solution)/shard_map/all_to_all | solution.py:528
  200.4 14.5 %all-to-all-done.2 = bf16[64,24,128]{2,1,0:T(8,128)(2,1)S(1)} async-done(((bf16[64,24,128]{2,1,0:T(8,128)(2,1)}), bf16[64,24,128]{2,1,0:T(8,128)(2,1)S(1)}, u32[]{:S(2)}, u32[]{:S(2)}) %all-to-all-start.2) | async-done | bytes 393248 | tf_op jit(solution)/shard_map/all_to_all | solution.py:528
  215.7 2.0 combine.1.refs_0_
  217.8 2.8 %collective-permute-start.36 = (bf16[24,1024]{1,0:T(8,128)(2,1)}, bf16[24,1024]{1,0:T(8,128)(2,1)S(1)}, u32[]{:S(2)}, u32[]{:S(2)}) collective-permute-start(bf16[24,1024]{1,0:T(8,128)(2,1)} %combine.1.refs_0_), channel_id=1, source_target_pairs={{0,2},{1,3},{2,0},{3,1},{4,6},{5,7},{6,4},{7,5},{8,10},{9,11},{10,... | collective-permute-start | bytes 147464 | tf_op jit(solution)/shard_map/ppermute | solution.py:26
  221.0 1.0 collective-permute-done.35.refs_1_
  222.0 1.0 collective-permute-done.36.refs_2_
  223.1 1.1 collective-permute-done.37.refs_3_
  224.8 1.6 finish.1
  (130 shorter events, 18.2 us)
Async XLA Ops:
  1.6 20.8 %collective-permute-start = (bf16[64,1792]{1,0:T(8,128)(2,1)}, bf16[64,1792]{1,0:T(8,128)(2,1)S(1)}, u32[]{:S(2)}, u32[]{:S(2)}) collective-permute-start(bf16[64,1792]{1,0:T(8,128)(2,1)} %pack.1.refs_0_), channel_id=1, source_target_pairs={{0,8},{8,16},{16,24},{24,0},{1,9},{9,17},{17,25},{25,1},{2,10},{10... | collective-permute-start | bytes 688136 | tf_op jit(solution)/shard_map/ppermute | solution.py:26
  3.7 19.7 %collective-permute-start.1 = (bf16[64,1792]{1,0:T(8,128)(2,1)}, bf16[64,1792]{1,0:T(8,128)(2,1)S(1)}, u32[]{:S(2)}, u32[]{:S(2)}) collective-permute-start(bf16[64,1792]{1,0:T(8,128)(2,1)} %pack.1.refs_0_), channel_id=1, source_target_pairs={{0,16},{8,24},{16,0},{24,8},{1,17},{9,25},{17,1},{25,9},{2,18},{10... | collective-permute-start | bytes 688136 | tf_op jit(solution)/shard_map/ppermute | solution.py:26
  6.1 17.3 %collective-permute-start.2 = (bf16[64,1792]{1,0:T(8,128)(2,1)}, bf16[64,1792]{1,0:T(8,128)(2,1)S(1)}, u32[]{:S(2)}, u32[]{:S(2)}) collective-permute-start(bf16[64,1792]{1,0:T(8,128)(2,1)} %pack.1.refs_0_), channel_id=1, source_target_pairs={{0,24},{8,0},{16,8},{24,16},{1,25},{9,1},{17,9},{25,17},{2,26},{10... | collective-permute-start | bytes 688136 | tf_op jit(solution)/shard_map/ppermute | solution.py:26
  7.3 22.0 %collective-permute-start.3 = (bf16[64,1792]{1,0:T(8,128)(2,1)}, bf16[64,1792]{1,0:T(8,128)(2,1)S(1)}, u32[]{:S(2)}, u32[]{:S(2)}) collective-permute-start(bf16[64,1792]{1,0:T(8,128)(2,1)} %pack.1.refs_0_), channel_id=1, source_target_pairs={{0,4},{4,0},{1,5},{5,1},{2,6},{6,2},{3,7},{7,3},{8,12},{12,8},{9,1... | collective-permute-start | bytes 688136 | tf_op jit(solution)/shard_map/ppermute | solution.py:26
  11.8 25.0 %all-to-all-start = ((bf16[8,24,512]{2,1,0:T(8,128)(2,1)}), bf16[8,24,512]{2,1,0:T(8,128)(2,1)S(1)}, u32[]{:S(2)}, u32[]{:S(2)}) async-start(bf16[8,24,512]{2,1,0:T(8,128)(2,1)} %get-tuple-element.28), calls=%async_computation | async-start | bytes 393216 | tf_op jit(solution)/shard_map/all_to_all | solution.py:478
  20.0 7.7 %collective-permute-start.15 = (bf16[64,512]{1,0:T(8,128)(2,1)}, bf16[64,512]{1,0:T(8,128)(2,1)S(1)}, u32[]{:S(2)}, u32[]{:S(2)}) collective-permute-start(bf16[64,512]{1,0:T(8,128)(2,1)} %bitcast.52), channel_id=1, source_target_pairs={{0,32},{32,0},{64,96},{96,64},{128,160},{160,128},{192,224},{224,1... | collective-permute-start | bytes 196616 | tf_op jit(solution)/shard_map/ppermute | solution.py:481
  22.4 14.5 %copy-start.12 = (bf16[64,1792]{1,0:T(8,128)(2,1)}, bf16[64,1792]{1,0:T(8,128)(2,1)S(1)}, u32[]{:S(2)}) copy-start(bf16[64,1792]{1,0:T(8,128)(2,1)S(1)} %collective-permute-done.refs_1_) | copy-start | bytes 688132
  22.4 11.1 %collective-permute-start.4 = (bf16[64,1792]{1,0:T(8,128)(2,1)S(1)}, bf16[64,1792]{1,0:T(8,128)(2,1)S(1)}, u32[]{:S(2)}, u32[]{:S(2)}) collective-permute-start(bf16[64,1792]{1,0:T(8,128)(2,1)S(1)} %collective-permute-done.refs_1_), channel_id=1, source_target_pairs={{0,4},{4,0},{1,5},{5,1},{2,6},{6,2},{3,7},{7,3},{8,12},{12,8},{9,1... | collective-permute-start | bytes 688136 | tf_op jit(solution)/shard_map/ppermute | solution.py:26
  23.3 13.5 %copy-start.13 = (bf16[64,1792]{1,0:T(8,128)(2,1)}, bf16[64,1792]{1,0:T(8,128)(2,1)S(1)}, u32[]{:S(2)}) copy-start(bf16[64,1792]{1,0:T(8,128)(2,1)S(1)} %collective-permute-done.1.refs_2_) | copy-start | bytes 688132
  23.3 13.5 %collective-permute-start.5 = (bf16[64,1792]{1,0:T(8,128)(2,1)S(1)}, bf16[64,1792]{1,0:T(8,128)(2,1)S(1)}, u32[]{:S(2)}, u32[]{:S(2)}) collective-permute-start(bf16[64,1792]{1,0:T(8,128)(2,1)S(1)} %collective-permute-done.1.refs_2_), channel_id=1, source_target_pairs={{0,4},{4,0},{1,5},{5,1},{2,6},{6,2},{3,7},{7,3},{8,12},{12,8},{9,1... | collective-permute-start | bytes 688136 | tf_op jit(solution)/shard_map/ppermute | solution.py:26
  23.5 13.4 %copy-start.14 = (bf16[64,1792]{1,0:T(8,128)(2,1)}, bf16[64,1792]{1,0:T(8,128)(2,1)S(1)}, u32[]{:S(2)}) copy-start(bf16[64,1792]{1,0:T(8,128)(2,1)S(1)} %collective-permute-done.2.refs_3_) | copy-start | bytes 688132
  23.5 13.4 %collective-permute-start.6 = (bf16[64,1792]{1,0:T(8,128)(2,1)S(1)}, bf16[64,1792]{1,0:T(8,128)(2,1)S(1)}, u32[]{:S(2)}, u32[]{:S(2)}) collective-permute-start(bf16[64,1792]{1,0:T(8,128)(2,1)S(1)} %collective-permute-done.2.refs_3_), channel_id=1, source_target_pairs={{0,4},{4,0},{1,5},{5,1},{2,6},{6,2},{3,7},{7,3},{8,12},{12,8},{9,1... | collective-permute-start | bytes 688136 | tf_op jit(solution)/shard_map/ppermute | solution.py:26
  28.6 28.9 %copy-start.8 = (bf16[2,64,512]{2,1,0:T(8,128)(2,1)}, bf16[2,64,512]{2,1,0:T(8,128)(2,1)S(1)}, u32[]{:S(2)}) copy-start(bf16[2,64,512]{2,1,0:T(8,128)(2,1)S(1)} %maximum_select_fusion.refs_0_) | copy-start | bytes 393220
  28.6 18.0 %collective-permute-start.16 = (bf16[2,64,512]{2,1,0:T(8,128)(2,1)S(1)}, bf16[2,64,512]{2,1,0:T(8,128)(2,1)S(1)}, u32[]{:S(2)}, u32[]{:S(2)}) collective-permute-start(bf16[2,64,512]{2,1,0:T(8,128)(2,1)S(1)} %maximum_select_fusion.refs_0_), channel_id=1, source_target_pairs={{0,64},{32,96},{64,128},{96,160},{128,192},{160,224},{192,0},{224,... | collective-permute-start | bytes 393224 | tf_op jit(solution)/shard_map/ppermute | solution.py:26
  29.2 7.6 %copy-start.15 = (bf16[64,1792]{1,0:T(8,128)(2,1)}, bf16[64,1792]{1,0:T(8,128)(2,1)S(1)}, u32[]{:S(2)}) copy-start(bf16[64,1792]{1,0:T(8,128)(2,1)S(1)} %collective-permute-done.3.refs_4_) | copy-start | bytes 688132
  29.2 18.9 %collective-permute-start.17 = (bf16[2,64,512]{2,1,0:T(8,128)(2,1)S(1)}, bf16[2,64,512]{2,1,0:T(8,128)(2,1)S(1)}, u32[]{:S(2)}, u32[]{:S(2)}) collective-permute-start(bf16[2,64,512]{2,1,0:T(8,128)(2,1)S(1)} %maximum_select_fusion.refs_0_), channel_id=1, source_target_pairs={{0,128},{32,160},{64,192},{96,224},{128,0},{160,32},{192,64},{224,... | collective-permute-start | bytes 393224 | tf_op jit(solution)/shard_map/ppermute | solution.py:26
  33.5 3.4 %copy-start.16 = (bf16[64,1792]{1,0:T(8,128)(2,1)}, bf16[64,1792]{1,0:T(8,128)(2,1)S(1)}, u32[]{:S(2)}) copy-start(bf16[64,1792]{1,0:T(8,128)(2,1)S(1)} %collective-permute-done.4.refs_5_) | copy-start | bytes 688132
  33.5 15.9 %collective-permute-start.18 = (bf16[2,64,512]{2,1,0:T(8,128)(2,1)S(1)}, bf16[2,64,512]{2,1,0:T(8,128)(2,1)S(1)}, u32[]{:S(2)}, u32[]{:S(2)}) collective-permute-start(bf16[2,64,512]{2,1,0:T(8,128)(2,1)S(1)} %maximum_select_fusion.refs_0_), channel_id=1, source_target_pairs={{0,192},{32,224},{64,0},{96,32},{128,64},{160,96},{192,128},{224,1... | collective-permute-start | bytes 393224 | tf_op jit(solution)/shard_map/ppermute | solution.py:26
  41.4 53.7 %copy-start.31 = (s32[24,4]{0,1:T(4,128)S(1)}, s32[24,4]{0,1:T(4,128)}, u32[]{:S(2)}) copy-start(s32[24,4]{0,1:T(4,128)} %param.32) | copy-start | bytes 1156
  41.4 61.0 %copy-start.32 = (f32[24,4]{0,1:T(4,128)S(1)}, f32[24,4]{0,1:T(4,128)}, u32[]{:S(2)}) copy-start(f32[24,4]{0,1:T(4,128)} %param.33) | copy-start | bytes 1156
  41.4 10.8 %collective-permute-start.10 = (bf16[24,1792]{1,0:T(8,128)(2,1)}, bf16[24,1792]{1,0:T(8,128)(2,1)S(1)}, u32[]{:S(2)}, u32[]{:S(2)}) collective-permute-start(bf16[24,1792]{1,0:T(8,128)(2,1)} %get-tuple-element.33), channel_id=1, source_target_pairs={{0,64},{32,96},{64,128},{96,160},{128,192},{160,224},{192,0},{224,... | collective-permute-start | bytes 258056 | tf_op jit(solution)/shard_map/ppermute | solution.py:26
  41.5 11.0 %collective-permute-start.11 = (bf16[24,1792]{1,0:T(8,128)(2,1)}, bf16[24,1792]{1,0:T(8,128)(2,1)S(1)}, u32[]{:S(2)}, u32[]{:S(2)}) collective-permute-start(bf16[24,1792]{1,0:T(8,128)(2,1)} %get-tuple-element.34), channel_id=1, source_target_pairs={{0,192},{32,224},{64,0},{96,32},{128,64},{160,96},{192,128},{224,1... | collective-permute-start | bytes 258056 | tf_op jit(solution)/shard_map/ppermute | solution.py:26
  46.6 10.9 %copy-start.19 = (bf16[2,64,512]{2,1,0:T(8,128)(2,1)}, bf16[2,64,512]{2,1,0:T(8,128)(2,1)S(1)}, u32[]{:S(2)}) copy-start(bf16[2,64,512]{2,1,0:T(8,128)(2,1)S(1)} %collective-permute-done.16.refs_1_) | copy-start | bytes 393220
  46.6 12.9 %collective-permute-start.12 = (bf16[24,1792]{1,0:T(8,128)(2,1)}, bf16[24,1792]{1,0:T(8,128)(2,1)S(1)}, u32[]{:S(2)}, u32[]{:S(2)}) collective-permute-start(bf16[24,1792]{1,0:T(8,128)(2,1)} %get-tuple-element.35), channel_id=1, source_target_pairs={{0,32},{32,64},{64,96},{96,128},{128,160},{160,192},{192,224},{224... | collective-permute-start | bytes 258056 | tf_op jit(solution)/shard_map/ppermute | solution.py:26
  48.1 9.4 %copy-start.20 = (bf16[2,64,512]{2,1,0:T(8,128)(2,1)}, bf16[2,64,512]{2,1,0:T(8,128)(2,1)S(1)}, u32[]{:S(2)}) copy-start(bf16[2,64,512]{2,1,0:T(8,128)(2,1)S(1)} %collective-permute-done.17.refs_2_) | copy-start | bytes 393220
  48.1 11.7 %collective-permute-start.13 = (bf16[24,1792]{1,0:T(8,128)(2,1)}, bf16[24,1792]{1,0:T(8,128)(2,1)S(1)}, u32[]{:S(2)}, u32[]{:S(2)}) collective-permute-start(bf16[24,1792]{1,0:T(8,128)(2,1)} %get-tuple-element.36), channel_id=1, source_target_pairs={{0,224},{32,0},{64,32},{96,64},{128,96},{160,128},{192,160},{224,1... | collective-permute-start | bytes 258056 | tf_op jit(solution)/shard_map/ppermute | solution.py:26
  49.4 8.2 %copy-start.21 = (bf16[2,64,512]{2,1,0:T(8,128)(2,1)}, bf16[2,64,512]{2,1,0:T(8,128)(2,1)S(1)}, u32[]{:S(2)}) copy-start(bf16[2,64,512]{2,1,0:T(8,128)(2,1)S(1)} %collective-permute-done.18.refs_3_) | copy-start | bytes 393220
  49.4 11.0 %collective-permute-start.7 = (bf16[24,1792]{1,0:T(8,128)(2,1)}, bf16[24,1792]{1,0:T(8,128)(2,1)S(1)}, u32[]{:S(2)}, u32[]{:S(2)}) collective-permute-start(bf16[24,1792]{1,0:T(8,128)(2,1)} %get-tuple-element.30), channel_id=1, source_target_pairs={{0,128},{32,160},{64,192},{96,224},{128,0},{160,32},{192,64},{224,... | collective-permute-start | bytes 258056 | tf_op jit(solution)/shard_map/ppermute | solution.py:26
  52.2 11.7 %collective-permute-start.8 = (bf16[24,1792]{1,0:T(8,128)(2,1)}, bf16[24,1792]{1,0:T(8,128)(2,1)S(1)}, u32[]{:S(2)}, u32[]{:S(2)}) collective-permute-start(bf16[24,1792]{1,0:T(8,128)(2,1)} %get-tuple-element.31), channel_id=1, source_target_pairs={{0,96},{32,128},{64,160},{96,192},{128,224},{160,0},{192,32},{224,... | collective-permute-start | bytes 258056 | tf_op jit(solution)/shard_map/ppermute | solution.py:26
  52.5 11.4 %collective-permute-start.9 = (bf16[24,1792]{1,0:T(8,128)(2,1)}, bf16[24,1792]{1,0:T(8,128)(2,1)S(1)}, u32[]{:S(2)}, u32[]{:S(2)}) collective-permute-start(bf16[24,1792]{1,0:T(8,128)(2,1)} %get-tuple-element.32), channel_id=1, source_target_pairs={{0,160},{32,192},{64,224},{96,0},{128,32},{160,64},{192,96},{224,1... | collective-permute-start | bytes 258056 | tf_op jit(solution)/shard_map/ppermute | solution.py:26
  59.5 14.2 %collective-permute-start.19 = (bf16[4,2,64,512]{3,2,1,0:T(8,128)(2,1)}, bf16[4,2,64,512]{3,2,1,0:T(8,128)(2,1)S(1)}, u32[]{:S(2)}, u32[]{:S(2)}) collective-permute-start(bf16[4,2,64,512]{3,2,1,0:T(8,128)(2,1)} %join.1.refs_0_), channel_id=1, source_target_pairs={{0,8},{8,16},{16,24},{24,0},{1,9},{9,17},{17,25},{25,1},{2,10},{10... | collective-permute-start | bytes 1572872 | tf_op jit(solution)/shard_map/ppermute | solution.py:26
  59.8 21.6 %collective-permute-start.20 = (bf16[4,2,64,512]{3,2,1,0:T(8,128)(2,1)}, bf16[4,2,64,512]{3,2,1,0:T(8,128)(2,1)S(1)}, u32[]{:S(2)}, u32[]{:S(2)}) collective-permute-start(bf16[4,2,64,512]{3,2,1,0:T(8,128)(2,1)} %join.1.refs_0_), channel_id=1, source_target_pairs={{0,16},{8,24},{16,0},{24,8},{1,17},{9,25},{17,1},{25,9},{2,18},{10... | collective-permute-start | bytes 1572872 | tf_op jit(solution)/shard_map/ppermute | solution.py:26
  60.4 24.9 %collective-permute-start.21 = (bf16[4,2,64,512]{3,2,1,0:T(8,128)(2,1)}, bf16[4,2,64,512]{3,2,1,0:T(8,128)(2,1)S(1)}, u32[]{:S(2)}, u32[]{:S(2)}) collective-permute-start(bf16[4,2,64,512]{3,2,1,0:T(8,128)(2,1)} %join.1.refs_0_), channel_id=1, source_target_pairs={{0,24},{8,0},{16,8},{24,16},{1,25},{9,1},{17,9},{25,17},{2,26},{10... | collective-permute-start | bytes 1572872 | tf_op jit(solution)/shard_map/ppermute | solution.py:26
  70.0 15.4 %copy-start.22 = (bf16[3,8,2,256]{3,1,2,0:T(8,128)(2,1)}, bf16[3,8,2,256]{3,1,2,0:T(8,128)(2,1)S(1)}, u32[]{:S(2)}) copy-start(bf16[3,8,2,256]{3,1,2,0:T(8,128)(2,1)S(1)} %copy.39) | copy-start | bytes 73732
  70.0 2.9 %collective-permute-start.14 = (bf16[24,512]{1,0:T(8,128)(2,1)S(1)}, bf16[24,512]{1,0:T(8,128)(2,1)S(1)}, u32[]{:S(2)}, u32[]{:S(2)}) collective-permute-start(bf16[24,512]{1,0:T(8,128)(2,1)S(1)} %bitcast.48), channel_id=1, source_target_pairs={{0,4},{4,0},{1,5},{5,1},{2,6},{6,2},{3,7},{7,3},{8,12},{12,8},{9,1... | collective-permute-start | bytes 73736 | tf_op jit(solution)/shard_map/ppermute | solution.py:26
  72.9 12.4 %copy-start.29 = (bf16[24,512]{1,0:T(8,128)(2,1)}, bf16[24,512]{1,0:T(8,128)(2,1)S(1)}, u32[]{:S(2)}) copy-start(bf16[24,512]{1,0:T(8,128)(2,1)S(1)} %collective-permute-done.14.partner) | copy-start | bytes 73732
  73.7 11.6 %copy-start.2 = (bf16[4,2,64,512]{3,2,1,0:T(8,128)(2,1)}, bf16[4,2,64,512]{3,2,1,0:T(8,128)(2,1)S(1)}, u32[]{:S(2)}) copy-start(bf16[4,2,64,512]{3,2,1,0:T(8,128)(2,1)S(1)} %collective-permute-done.19.refs_1_) | copy-start | bytes 1572868
  81.4 3.9 %copy-start.3 = (bf16[4,2,64,512]{3,2,1,0:T(8,128)(2,1)}, bf16[4,2,64,512]{3,2,1,0:T(8,128)(2,1)S(1)}, u32[]{:S(2)}) copy-start(bf16[4,2,64,512]{3,2,1,0:T(8,128)(2,1)S(1)} %collective-permute-done.20.refs_2_) | copy-start | bytes 1572868
  85.3 0.8 copy-start.4
  90.0 5.1 %collective-permute-start.22 = (bf16[48,512]{1,0:T(8,128)(2,1)}, bf16[48,512]{1,0:T(8,128)(2,1)S(1)}, u32[]{:S(2)}, u32[]{:S(2)}) collective-permute-start(bf16[48,512]{1,0:T(8,128)(2,1)} %get-tuple-element.39), channel_id=1, source_target_pairs={{0,1},{1,2},{2,3},{3,0},{4,5},{5,6},{6,7},{7,4},{8,9},{9,10},{10,1... | collective-permute-start | bytes 147464 | tf_op jit(solution)/shard_map/ppermute | solution.py:26
  91.4 4.8 %collective-permute-start.23 = (bf16[48,512]{1,0:T(8,128)(2,1)}, bf16[48,512]{1,0:T(8,128)(2,1)S(1)}, u32[]{:S(2)}, u32[]{:S(2)}) collective-permute-start(bf16[48,512]{1,0:T(8,128)(2,1)} %get-tuple-element.40), channel_id=1, source_target_pairs={{0,2},{1,3},{2,0},{3,1},{4,6},{5,7},{6,4},{7,5},{8,10},{9,11},{10,... | collective-permute-start | bytes 147464 | tf_op jit(solution)/shard_map/ppermute | solution.py:26
  94.0 3.3 %collective-permute-start.24 = (bf16[48,512]{1,0:T(8,128)(2,1)}, bf16[48,512]{1,0:T(8,128)(2,1)S(1)}, u32[]{:S(2)}, u32[]{:S(2)}) collective-permute-start(bf16[48,512]{1,0:T(8,128)(2,1)} %get-tuple-element.41), channel_id=1, source_target_pairs={{0,3},{1,0},{2,1},{3,2},{4,7},{5,4},{6,5},{7,6},{8,11},{9,8},{10,9... | collective-permute-start | bytes 147464 | tf_op jit(solution)/shard_map/ppermute | solution.py:26
  98.7 5.1 %collective-permute-start.25 = (bf16[24,512]{1,0:T(8,128)(2,1)S(1)}, bf16[24,512]{1,0:T(8,128)(2,1)S(1)}, u32[]{:S(2)}, u32[]{:S(2)}) collective-permute-start(bf16[24,512]{1,0:T(8,128)(2,1)S(1)} %get-tuple-element.53), channel_id=1, source_target_pairs={{0,4},{4,0},{1,5},{5,1},{2,6},{6,2},{3,7},{7,3},{8,12},{12,8},{9,1... | collective-permute-start | bytes 73736 | tf_op jit(solution)/shard_map/ppermute | solution.py:26
  130.1 11.8 %collective-permute-start.27 = (bf16[192,1024]{1,0:T(8,128)(2,1)}, bf16[192,1024]{1,0:T(8,128)(2,1)S(1)}, u32[]{:S(2)}, u32[]{:S(2)}) collective-permute-start(bf16[192,1024]{1,0:T(8,128)(2,1)} %unpack.1.refs_0_), channel_id=1, source_target_pairs={{0,1},{1,2},{2,3},{3,0},{4,5},{5,6},{6,7},{7,4},{8,9},{9,10},{10,1... | collective-permute-start | bytes 1179656 | tf_op jit(solution)/shard_map/ppermute | solution.py:26
  133.6 51.0 %collective-permute-start.32 = (bf16[256,1024]{1,0:T(8,128)(2,1)}, bf16[256,1024]{1,0:T(8,128)(2,1)S(1)}, u32[]{:S(2)}, u32[]{:S(2)}) collective-permute-start(bf16[256,1024]{1,0:T(8,128)(2,1)} %get-tuple-element.47), channel_id=1, source_target_pairs={{0,1},{1,2},{2,3},{3,0},{4,5},{5,6},{6,7},{7,4},{8,9},{9,10},{10,1... | collective-permute-start | bytes 1572872 | tf_op jit(solution)/shard_map/ppermute | solution.py:26
  134.5 11.1 %collective-permute-start.28 = (bf16[192,1024]{1,0:T(8,128)(2,1)}, bf16[192,1024]{1,0:T(8,128)(2,1)S(1)}, u32[]{:S(2)}, u32[]{:S(2)}) collective-permute-start(bf16[192,1024]{1,0:T(8,128)(2,1)} %unpack.1.refs_0_), channel_id=1, source_target_pairs={{0,3},{1,0},{2,1},{3,2},{4,7},{5,4},{6,5},{7,6},{8,11},{9,8},{10,9... | collective-permute-start | bytes 1179656 | tf_op jit(solution)/shard_map/ppermute | solution.py:26
  136.3 48.5 %collective-permute-start.33 = (bf16[256,1024]{1,0:T(8,128)(2,1)}, bf16[256,1024]{1,0:T(8,128)(2,1)S(1)}, u32[]{:S(2)}, u32[]{:S(2)}) collective-permute-start(bf16[256,1024]{1,0:T(8,128)(2,1)} %get-tuple-element.48), channel_id=1, source_target_pairs={{0,2},{1,3},{2,0},{3,1},{4,6},{5,7},{6,4},{7,5},{8,10},{9,11},{10,... | collective-permute-start | bytes 1572872 | tf_op jit(solution)/shard_map/ppermute | solution.py:26
  138.5 46.3 %collective-permute-start.34 = (bf16[256,1024]{1,0:T(8,128)(2,1)}, bf16[256,1024]{1,0:T(8,128)(2,1)S(1)}, u32[]{:S(2)}, u32[]{:S(2)}) collective-permute-start(bf16[256,1024]{1,0:T(8,128)(2,1)} %get-tuple-element.49), channel_id=1, source_target_pairs={{0,3},{1,0},{2,1},{3,2},{4,7},{5,4},{6,5},{7,6},{8,11},{9,8},{10,9... | collective-permute-start | bytes 1572872 | tf_op jit(solution)/shard_map/ppermute | solution.py:26
  141.9 3.7 %copy-start.9 = (bf16[192,1024]{1,0:T(8,128)(2,1)}, bf16[192,1024]{1,0:T(8,128)(2,1)S(1)}, u32[]{:S(2)}) copy-start(bf16[192,1024]{1,0:T(8,128)(2,1)S(1)} %collective-permute-done.27.refs_1_) | copy-start | bytes 1179652
  141.9 31.7 %collective-permute-start.26 = (bf16[192,1024]{1,0:T(8,128)(2,1)}, bf16[192,1024]{1,0:T(8,128)(2,1)S(1)}, u32[]{:S(2)}, u32[]{:S(2)}) collective-permute-start(bf16[192,1024]{1,0:T(8,128)(2,1)} %unpack.1.refs_0_), channel_id=1, source_target_pairs={{0,2},{1,3},{2,0},{3,1},{4,6},{5,7},{6,4},{7,5},{8,10},{9,11},{10,... | collective-permute-start | bytes 1179656 | tf_op jit(solution)/shard_map/ppermute | solution.py:26
  177.9 7.6 %collective-permute-start.29 = (bf16[192,256]{1,0:T(8,128)(2,1)}, bf16[192,256]{1,0:T(8,128)(2,1)S(1)}, u32[]{:S(2)}, u32[]{:S(2)}) collective-permute-start(bf16[192,256]{1,0:T(8,128)(2,1)} %expert_last.1.refs_0_), channel_id=1, source_target_pairs={{0,1},{1,2},{2,3},{3,0},{4,5},{5,6},{6,7},{7,4},{8,9},{9,10},{10,1... | collective-permute-start | bytes 294920 | tf_op jit(solution)/shard_map/ppermute | solution.py:26
  182.3 5.8 %collective-permute-start.30 = (bf16[192,256]{1,0:T(8,128)(2,1)}, bf16[192,256]{1,0:T(8,128)(2,1)S(1)}, u32[]{:S(2)}, u32[]{:S(2)}) collective-permute-start(bf16[192,256]{1,0:T(8,128)(2,1)} %expert_last.1.refs_0_), channel_id=1, source_target_pairs={{0,2},{1,3},{2,0},{3,1},{4,6},{5,7},{6,4},{7,5},{8,10},{9,11},{10,... | collective-permute-start | bytes 294920 | tf_op jit(solution)/shard_map/ppermute | solution.py:26
  184.5 4.9 %copy-start.5 = (bf16[256,1024]{1,0:T(8,128)(2,1)}, bf16[256,1024]{1,0:T(8,128)(2,1)S(1)}, u32[]{:S(2)}) copy-start(bf16[256,1024]{1,0:T(8,128)(2,1)S(1)} %collective-permute-done.32.refs_5_) | copy-start | bytes 1572868
  184.6 4.9 %collective-permute-start.31 = (bf16[192,256]{1,0:T(8,128)(2,1)}, bf16[192,256]{1,0:T(8,128)(2,1)S(1)}, u32[]{:S(2)}, u32[]{:S(2)}) collective-permute-start(bf16[192,256]{1,0:T(8,128)(2,1)} %expert_last.1.refs_0_), channel_id=1, source_target_pairs={{0,3},{1,0},{2,1},{3,2},{4,7},{5,4},{6,5},{7,6},{8,11},{9,8},{10,9... | collective-permute-start | bytes 294920 | tf_op jit(solution)/shard_map/ppermute | solution.py:26
  184.8 4.7 %copy-start.6 = (bf16[256,1024]{1,0:T(8,128)(2,1)}, bf16[256,1024]{1,0:T(8,128)(2,1)S(1)}, u32[]{:S(2)}) copy-start(bf16[256,1024]{1,0:T(8,128)(2,1)S(1)} %collective-permute-done.33.refs_6_) | copy-start | bytes 1572868
  184.8 4.7 %copy-start.7 = (bf16[256,1024]{1,0:T(8,128)(2,1)}, bf16[256,1024]{1,0:T(8,128)(2,1)S(1)}, u32[]{:S(2)}) copy-start(bf16[256,1024]{1,0:T(8,128)(2,1)S(1)} %collective-permute-done.34.refs_7_) | copy-start | bytes 1572868
  185.6 3.9 %copy-start.23 = (bf16[192,256]{1,0:T(8,128)(2,1)}, bf16[192,256]{1,0:T(8,128)(2,1)S(1)}, u32[]{:S(2)}) copy-start(bf16[192,256]{1,0:T(8,128)(2,1)S(1)} %collective-permute-done.29.refs_1_) | copy-start | bytes 294916
  188.1 1.4 copy-start.24
  193.2 21.8 %all-to-all-start.2 = ((bf16[64,24,128]{2,1,0:T(8,128)(2,1)}), bf16[64,24,128]{2,1,0:T(8,128)(2,1)S(1)}, u32[]{:S(2)}, u32[]{:S(2)}) async-start(bf16[64,24,128]{2,1,0:T(8,128)(2,1)} %bitcast.43), calls=%async_computation.2 | async-start | bytes 786432 | tf_op jit(solution)/shard_map/all_to_all | solution.py:528
  217.7 4.4 %collective-permute-start.35 = (bf16[24,1024]{1,0:T(8,128)(2,1)}, bf16[24,1024]{1,0:T(8,128)(2,1)S(1)}, u32[]{:S(2)}, u32[]{:S(2)}) collective-permute-start(bf16[24,1024]{1,0:T(8,128)(2,1)} %combine.1.refs_0_), channel_id=1, source_target_pairs={{0,1},{1,2},{2,3},{3,0},{4,5},{5,6},{6,7},{7,4},{8,9},{9,10},{10,1... | collective-permute-start | bytes 147464 | tf_op jit(solution)/shard_map/ppermute | solution.py:26
  217.8 5.3 %collective-permute-start.36 = (bf16[24,1024]{1,0:T(8,128)(2,1)}, bf16[24,1024]{1,0:T(8,128)(2,1)S(1)}, u32[]{:S(2)}, u32[]{:S(2)}) collective-permute-start(bf16[24,1024]{1,0:T(8,128)(2,1)} %combine.1.refs_0_), channel_id=1, source_target_pairs={{0,2},{1,3},{2,0},{3,1},{4,6},{5,7},{6,4},{7,5},{8,10},{9,11},{10,... | collective-permute-start | bytes 147464 | tf_op jit(solution)/shard_map/ppermute | solution.py:26
  220.5 3.6 %collective-permute-start.37 = (bf16[24,1024]{1,0:T(8,128)(2,1)}, bf16[24,1024]{1,0:T(8,128)(2,1)S(1)}, u32[]{:S(2)}, u32[]{:S(2)}) collective-permute-start(bf16[24,1024]{1,0:T(8,128)(2,1)} %combine.1.refs_0_), channel_id=1, source_target_pairs={{0,3},{1,0},{2,1},{3,2},{4,7},{5,4},{6,5},{7,6},{8,11},{9,8},{10,9... | collective-permute-start | bytes 147464 | tf_op jit(solution)/shard_map/ppermute | solution.py:26
  222.0 2.1 copy-start.26
  223.1 1.1 copy-start.27
  (9 other events, 6.2 us)
where the time goes:
time: 228 us; the launch traced here: 226 us
  starting transfers between devices  76.2 us (33%)
  waiting for transfers between devices  69.5 us (30%)
  Pallas kernels  35.1 us (15%)
  blocking collectives  21.6 us (9%)
  local copies, waits for them, and re-layouts  11.6 us (5%)
  other arithmetic  8.08 us (4%)
  matrix products  3.89 us (2%)
    ppermute x37, starting transfers between devices, shift(): return lax.ppermute(value, axis, [(i, (i + by) % n) for i in range(n)])  59.9 us
    ppermute x37, waiting for transfers between devices, shift(): return lax.ppermute(value, axis, [(i, (i + by) % n) for i in range(n)])  51.7 us
    all_to_all x1, blocking collectives, on_device(): lax.all_to_all(outbound.reshape(n_ep, -1, 128), EP, 0, 0, tiled=True)  21.6 us
    all_to_all x1, waiting for transfers between devices, on_device(): lax.all_to_all(done.reshape(n_ep, -1, 128), EP, 0, 0, tiled=True)  14.5 us
    pallas_call x2, Pallas kernels, expert(): pl.pallas_call(functools.partial(expert_kernel, steps, nt, last), out_sha...  8.65 us
    all_to_all x1, starting transfers between devices, on_device(): tok = lax.all_to_all(tok_parts, Z, 0, 0, tiled=True)  8.19 us
    unnamed x68, local copies, waits for them, and re-layouts  7.1 us
    all_to_all x1, starting transfers between devices, on_device(): lax.all_to_all(done.reshape(n_ep, -1, 128), EP, 0, 0, tiled=True)  6.61 us
  transfers between devices with their start and end apart: 40, of which 18 were waited for; matrix products, arithmetic and copies ran while one was open for 7% of the time, Pallas kernels for 8%

commit v1 on v0

--- a/solution.py
+++ b/solution.py
@@ -26,10 +26,6 @@
     return lax.ppermute(value, axis, [(i, (i + by) % n) for i in range(n)])
 
 
-def order_of(n):
-    return sorted(range(1, n), key=lambda s: (-min(s, n - s), s))
-
-
 VMEM = pl.BlockSpec(memory_space=pltpu.VMEM)
 SMEM = pl.BlockSpec(memory_space=pltpu.SMEM)
 ANY = pl.BlockSpec(memory_space=pl.ANY)
@@ -61,24 +57,29 @@
     )(*arrays)
 
 
-def scale_kernel(tokens, gain, out, scale):
+def scale_kernel(tokens, gain, weight, out, scale):
     values = tokens[...].astype(f32)
+    seqs = values.shape[0]
     meansq = jnp.mean(values * values, axis=-1, keepdims=True)
     scale[...] = jnp.broadcast_to(lax.rsqrt(meansq + eps), scale.shape)
-    values = (values * gain[...].astype(f32)).astype(bf16)
+    values = (values * gain[...].astype(f32).reshape(1, -1)).astype(bf16)
     cols = out.shape[2]
     for i in range(out.shape[0]):
-        out[i] = values[:, i * cols : (i + 1) * cols]
-
-
-def scale(tokens, gain, nz):
+        out[i, :seqs] = values[:, i * cols : (i + 1) * cols]
+        out[i, seqs:] = weight[...]
+
+
+def scale(tokens, gain, weight, nz):
     seqs, width = tokens.shape
     return pl.pallas_call(
         scale_kernel,
-        out_shape=[shaped((nz, seqs, width // nz), bf16), shaped((seqs, 128), f32)],
+        out_shape=[
+            shaped((nz, seqs + weight.shape[0], width // nz), bf16),
+            shaped((seqs, 128), f32),
+        ],
         cost_estimate=cost(1e6, 4 * seqs * width),
         name="scale",
-    )(tokens, gain[None])
+    )(tokens, gain, weight)
 
 
 def split_kernel(nz, where, down, *outs):
@@ -103,75 +104,108 @@
     )(where, down)
 
 
-def project_kernel(nz, nx, where, tok, *refs):
+def project_kernel(nx, where, tok, *refs):
     own, other = refs[:nx], refs[nx : 2 * nx]
-    outs = refs[2 * nx : 2 * nx + nz]
-    weight, turned = refs[-2:]
-    z, x, c = where[0], where[1], where[2]
+    out, weight = refs[2 * nx :]
+    x, c = where[1], where[2]
     rows = own[0].shape[0]
-    seqs = outs[0].shape[0]
+    nz, seqs, cols = out.shape
     for i in range(nx):
         base = lax.rem(x - i + nx, nx) * (2 * rows)
         weight[pl.ds(pl.multiple_of(base + c * rows, rows), rows), :] = own[i][...]
         weight[pl.ds(pl.multiple_of(base + (1 - c) * rows, rows), rows), :] = other[i][...]
-    for s in range(nz):
-        turned[s * seqs : (s + 1) * seqs, :] = tok[lax.rem(z + s, nz)].astype(f32)
-    total = jnp.dot(turned[...].astype(bf16), weight[...], preferred_element_type=f32)
-    for s in range(nz):
-        outs[s][...] = total[s * seqs : (s + 1) * seqs, :].astype(bf16)
-
-
-def project(where, tok, own, other):
-    nz, seqs, depth = tok.shape
+    left = tok[:, :seqs].astype(f32).reshape(nz * seqs, tok.shape[2]).astype(bf16)
+    total = jnp.dot(left, weight[...], preferred_element_type=f32)
+    out[...] = total.reshape(nz, seqs, cols).astype(bf16)
+
+
+def project(where, tok, seqs, own, other):
+    nz, _, depth = tok.shape
     nx, cols = len(own), own[0].shape[1]
     return pl.pallas_call(
-        functools.partial(project_kernel, nz, nx),
-        out_shape=[shaped((seqs, cols), bf16)] * nz,
+        functools.partial(project_kernel, nx),
+        out_shape=shaped((nz, seqs, cols), bf16),
         in_specs=[SMEM] + [VMEM] * (1 + 2 * nx),
-        out_specs=[VMEM] * nz,
-        scratch_shapes=[pltpu.VMEM((depth, cols), bf16), pltpu.VMEM((nz * seqs, depth), f32)],
+        out_specs=VMEM,
+        scratch_shapes=[pltpu.VMEM((depth, cols), bf16)],
         cost_estimate=cost(2 * nz * seqs * depth * cols, 2 * depth * cols),
         name="project",
     )(where, tok, *own, *other)
 
 
-def join_kernel(*refs):
-    for i, ref in enumerate(refs[:-1]):
-        refs[-1][i] = ref[...]
-
-
-def join(arrays):
-    shape = (len(arrays), *arrays[0].shape)
-    return pl.pallas_call(
-        join_kernel,
-        out_shape=shaped(shape, arrays[0].dtype),
-        cost_estimate=cost(1e6, 4 * len(arrays) * arrays[0].size),
-        name="join",
-    )(*arrays)
+def attend_kernel(heads, arrived, scale, shift_of, state, gain, out):
+    total = jnp.sum(arrived[...].astype(f32), axis=0) * scale[:, :1]
+    rows = total.shape[0]
+    keys = shift_of.shape[1]
+    vals = out.shape[1]
+    dim, width = keys // heads, vals // heads
+    query = total[:, :keys] * dim ** (-0.5)
+    key = total[:, keys : 2 * keys]
+    pre = total[:, 2 * keys : 3 * keys]
+    value = total[:, 3 * keys : 3 * keys + vals]
+    rgate = total[:, 3 * keys + vals :]
+    log_sig = jnp.minimum(pre, 0.0) - jnp.log1p(jnp.exp(-jnp.abs(pre)))
+    faded = query * jnp.exp(log_sig / tau + shift_of[...])
+    product = query * key
+    silu = rgate * jax.nn.sigmoid(rgate)
+    for h in range(heads):
+        at = slice(h * dim, (h + 1) * dim)
+        turned = jnp.transpose(faded[:, at])
+        reads = [
+            jnp.sum(turned[:, s : s + 1] * state[s, h], axis=0, keepdims=True)
+            for s in range(rows)
+        ]
+        cols = slice(h * width, (h + 1) * width)
+        read = jnp.concatenate(reads, axis=0)
+        read = read + jnp.sum(product[:, at], axis=-1, keepdims=True) * value[:, cols]
+        meansq = jnp.mean(read * read, axis=-1, keepdims=True)
+        out[:, cols] = (
+            read
+            * lax.rsqrt(meansq + eps)
+            * gain[...].astype(f32).reshape(1, -1)[:, cols]
+            * silu[:, cols]
+        ).astype(bf16)
+
+
+def attend(arrived, scale, decay_shift, state, head_gain):
+    seqs, heads, dim, width = state.shape
+    step = 8
+    vals = heads * width
+    return pl.pallas_call(
+        functools.partial(attend_kernel, heads),
+        grid=(seqs // step,),
+        out_shape=shaped((seqs, vals), bf16),
+        in_specs=[
+            pl.BlockSpec((arrived.shape[0], step, arrived.shape[2]), lambda i: (0, i, 0)),
+            pl.BlockSpec((step, scale.shape[1]), lambda i: (i, 0)),
+            pl.BlockSpec((step, heads * dim), lambda i: (i, 0)),
+            pl.BlockSpec((step, heads, dim, width), lambda i: (i, 0, 0, 0)),
+            pl.BlockSpec((vals,), lambda i: (0,)),
+        ],
+        out_specs=pl.BlockSpec((step, vals), lambda i: (i, 0)),
+        cost_estimate=cost(4 * state.size, 4 * state.size),
+        name="attend",
+    )(arrived, scale, decay_shift, state, head_gain)
 
 
 def mix_kernel(nx, where, gated, partner, *refs):
     blocks = refs[:nx]
     outs = refs[nx : 2 * nx]
     weight, sems = refs[-2:]
-    z, x, t = where[0], where[1], where[3]
-    pairs = weight.shape[1]
+    x, t = where[1], where[3]
     copies = []
     for i in range(nx):
-        for r in range(pairs):
-            copy = pltpu.make_async_copy(
-                blocks[i].at[r],
-                weight.at[lax.rem(x - i + nx, nx), lax.rem(lax.div(z, 2) - r + pairs, pairs)],
-                sems.at[i, r],
-            )
-            copy.start()
-            copies.append(copy)
+        copy = pltpu.make_async_copy(
+            blocks[i], weight.at[lax.rem(x - i + nx, nx)], sems.at[i]
+        )
+        copy.start()
+        copies.append(copy)
     rows = jnp.concatenate([gated[...], partner[...]], axis=0)
     for copy in copies:
         copy.wait()
-    depth, cols = weight.shape[4], pairs * 2 * weight.shape[3]
+    _, nz, cols, depth = weight.shape
     for s in range(nx):
-        block = weight[lax.rem(t + s, nx)].reshape(cols, depth)
+        block = weight[lax.rem(t + s, nx)].reshape(nz * cols, depth)
         outs[s][...] = lax.dot_general(
             rows, block, (((1,), (1,)), ((), ())), preferred_element_type=f32
         ).astype(bf16)
@@ -179,8 +213,8 @@
 
 def mix(where, gated, partner, blocks):
     nx = len(blocks)
-    pairs, two, rows, depth = blocks[0].shape
-    cols = pairs * two * rows
+    nz, rows, depth = blocks[0].shape
+    cols = nz * rows
     seqs = 2 * gated.shape[0]
     return pl.pallas_call(
         functools.partial(mix_kernel, nx),
@@ -188,8 +222,8 @@
         in_specs=[SMEM, VMEM, VMEM] + [ANY] * nx,
         out_specs=[VMEM] * nx,
         scratch_shapes=[
-            pltpu.VMEM((nx, pairs, two, rows, depth), bf16),
-            pltpu.SemaphoreType.DMA((nx, pairs)),
+            pltpu.VMEM((nx, nz, rows, depth), bf16),
+            pltpu.SemaphoreType.DMA((nx,)),
         ],
         cost_estimate=cost(2 * seqs * cols * nx * depth, 2 * cols * nx * depth),
         name="mix",
@@ -235,32 +269,43 @@
     )(where, tokens, gain, sender, mine, other)
 
 
-def unpack_kernel(rows, out, wide):
+def take_rows(rows, wide, slots):
     wide[...] = rows[...].astype(f32)
-    chunks = out.shape[1] // 128
-    for j in range(chunks):
-        out[:, j * 128 : (j + 1) * 128] = wide[
-            pl.ds(j, out.shape[0], stride=chunks), :
-        ].astype(bf16)
-
-
-def unpack(rows, slots):
-    part = rows.shape[0] * 128 // slots
-    return pl.pallas_call(
-        unpack_kernel,
-        out_shape=shaped((slots, part), bf16),
-        scratch_shapes=[pltpu.VMEM(rows.shape, f32)],
-        cost_estimate=cost(1e6, 4 * slots * part),
-        name="unpack",
-    )(rows)
-
-
-def expert_kernel(steps, nt, last, where, inverse, w_gate, w_lin, *refs):
+    chunks = wide.shape[0] // slots
+    return jnp.concatenate(
+        [wide[pl.ds(j, slots, stride=chunks), :] for j in range(chunks)], axis=1
+    )
+
+
+def pick_kernel(step, nt, where, w_gate, w_lin, gate, lin, sems):
+    at = lax.rem(where[3] - step + nt, nt)
+    copies = (
+        pltpu.make_async_copy(w_gate.at[:, at], gate, sems.at[0]),
+        pltpu.make_async_copy(w_lin.at[:, at], lin, sems.at[1]),
+    )
+    for copy in copies:
+        copy.start()
+    for copy in copies:
+        copy.wait()
+
+
+def pick(where, w_gate, w_lin, step):
+    nz, nt, chunk, units = w_gate.shape
+    return pl.pallas_call(
+        functools.partial(pick_kernel, step, nt),
+        out_shape=[shaped((nz, chunk, units), bf16)] * 2,
+        in_specs=[SMEM, ANY, ANY],
+        out_specs=[VMEM, VMEM],
+        scratch_shapes=[pltpu.SemaphoreType.DMA((2,))],
+        cost_estimate=cost(1e6, 8 * nz * chunk * units),
+        name="pick",
+    )(where, w_gate, w_lin)
+
+
+def expert_first_kernel(steps, nt, slots, where, inverse, w_gate, w_lin, *refs):
     count = len(steps)
     pieces, refs = refs[:count], refs[count:]
-    if last:
-        before, refs = refs[:3], refs[3:]
-    outs, (gates, lins, sems) = refs[:-3], refs[-3:]
+    outs, (gates, lins, wide, sems) = refs[:3], refs[3:]
     t = where[3]
     copies = []
     for i, s in enumerate(steps):
@@ -272,59 +317,77 @@
         for copy in pair:
             copy.start()
         copies.append(pair)
-    if last:
-        gate, lin, sumsq = before[0][...], before[1][...], before[2][:, :1]
-    else:
-        gate, lin, sumsq = 0.0, 0.0, 0.0
+    gate, lin, sumsq = 0.0, 0.0, 0.0
     units = w_gate.shape[-1]
     for i, s in enumerate(steps):
         at = lax.rem(t - s + nt, nt)
-        piece = pieces[i][...]
-        plain = piece.astype(f32) * inverse[at]
+        rows = take_rows(pieces[i], wide, slots)
+        plain = rows * inverse[at]
         sumsq = sumsq + jnp.sum(plain * plain, axis=-1, keepdims=True)
+        rows = rows.astype(bf16)
         copies[i][0].wait()
         gate = gate + jnp.dot(
-            piece, gates[i].reshape(piece.shape[1], units), preferred_element_type=f32
+            rows, gates[i].reshape(-1, units), preferred_element_type=f32
         )
         copies[i][1].wait()
-        lin = lin + jnp.dot(
-            piece, lins[i].reshape(piece.shape[1], units), preferred_element_type=f32
-        )
-    if last:
-        width = nt * pieces[0].shape[1]
-        scale = lax.rsqrt(sumsq / width + eps)
-        gate = jnp.minimum(gate * scale, limit)
-        lin = jnp.clip(lin * scale, -limit, limit)
-        outs[0][...] = (gate * jax.nn.sigmoid(glu_alpha * gate) * (lin + 1.0)).astype(bf16)
-    else:
-        outs[0][...] = gate
-        outs[1][...] = lin
-        outs[2][...] = jnp.broadcast_to(sumsq, outs[2].shape)
-
-
-def expert(where, inverse, w_gate, w_lin, steps, pieces, before):
+        lin = lin + jnp.dot(rows, lins[i].reshape(-1, units), preferred_element_type=f32)
+    outs[0][...] = gate
+    outs[1][...] = lin
+    outs[2][...] = jnp.broadcast_to(sumsq, outs[2].shape)
+
+
+def expert_first(where, inverse, w_gate, w_lin, steps, pieces, slots):
     nz, nt, chunk, units = w_gate.shape
-    slots, part = pieces[0].shape
-    last = before is not None
-    out_shape = (
-        [shaped((slots, units), bf16)]
-        if last
-        else [shaped((slots, units), f32)] * 2 + [shaped((slots, 128), f32)]
-    )
     count = len(steps)
-    return pl.pallas_call(
-        functools.partial(expert_kernel, steps, nt, last),
-        out_shape=out_shape,
-        in_specs=[SMEM, VMEM, ANY, ANY] + [VMEM] * (count + (3 if last else 0)),
-        out_specs=[VMEM] * len(out_shape),
+    part = nz * chunk
+    return pl.pallas_call(
+        functools.partial(expert_first_kernel, steps, nt, slots),
+        out_shape=[shaped((slots, units), f32)] * 2 + [shaped((slots, 128), f32)],
+        in_specs=[SMEM, VMEM, ANY, ANY] + [VMEM] * count,
+        out_specs=[VMEM] * 3,
         scratch_shapes=[
             pltpu.VMEM((count, nz, chunk, units), bf16),
             pltpu.VMEM((count, nz, chunk, units), bf16),
+            pltpu.VMEM(pieces[0].shape, f32),
             pltpu.SemaphoreType.DMA((count, 2)),
         ],
         cost_estimate=cost(4 * count * slots * part * units, 4 * count * part * units),
-        name="expert_last" if last else "expert_first",
-    )(where, inverse, w_gate, w_lin, *pieces, *(before or ()))
+        name="expert_first",
+    )(where, inverse, w_gate, w_lin, *pieces)
+
+
+def expert_last_kernel(step, nt, where, inverse, w_gate, w_lin, piece, *refs):
+    gate, lin, sumsq, out, wide = refs
+    slots, units = out.shape
+    rows = take_rows(piece, wide, slots)
+    plain = rows * inverse[lax.rem(where[3] - step + nt, nt)]
+    meansq = (sumsq[:, :1] + jnp.sum(plain * plain, axis=-1, keepdims=True)) / (
+        nt * rows.shape[1]
+    )
+    rows = rows.astype(bf16)
+    scale = lax.rsqrt(meansq + eps)
+    gated = gate[...] + jnp.dot(
+        rows, w_gate[...].reshape(-1, units), preferred_element_type=f32
+    )
+    linear = lin[...] + jnp.dot(
+        rows, w_lin[...].reshape(-1, units), preferred_element_type=f32
+    )
+    gated = jnp.minimum(gated * scale, limit)
+    linear = jnp.clip(linear * scale, -limit, limit)
+    out[...] = (gated * jax.nn.sigmoid(glu_alpha * gated) * (linear + 1.0)).astype(bf16)
+
+
+def expert_last(where, inverse, w_gate, w_lin, step, nt, piece, before):
+    slots, units = before[0].shape
+    return pl.pallas_call(
+        functools.partial(expert_last_kernel, step, nt),
+        out_shape=shaped((slots, units), bf16),
+        in_specs=[SMEM] + [VMEM] * 7,
+        out_specs=VMEM,
+        scratch_shapes=[pltpu.VMEM(piece.shape, f32)],
+        cost_estimate=cost(4 * slots * w_gate.size, 4 * w_gate.size),
+        name="expert_last",
+    )(where, inverse, w_gate, w_lin, piece, *before)
 
 
 def down_kernel(nt, *refs):
@@ -394,32 +457,6 @@
         cost_estimate=cost(1e6, 4 * seqs * part * len(pieces)),
         name="finish",
     )(where, *pieces)
-
-
-def attention(arrived, first_scale, decay_shift, state, head_gain, key_cols, val_cols):
-    seq_dev, heads_dev, key_dim, val_dim = state.shape
-    projected = functools.reduce(jnp.add, [a.astype(f32) for a in arrived]) * first_scale
-    q_rows = projected[:, :key_cols].reshape(seq_dev, heads_dev, key_dim) * key_dim ** (-0.5)
-    k_rows = projected[:, key_cols : 2 * key_cols].reshape(seq_dev, heads_dev, key_dim)
-    decay_pre = projected[:, 2 * key_cols : 3 * key_cols]
-    v_rows = projected[:, 3 * key_cols : 3 * key_cols + val_cols].reshape(
-        seq_dev, heads_dev, val_dim
-    )
-    rgates = projected[:, 3 * key_cols + val_cols :].reshape(seq_dev, heads_dev, val_dim)
-    log_decay = jax.nn.log_sigmoid(decay_pre) / tau + decay_shift
-    new_state = (
-        jnp.exp(log_decay.reshape(seq_dev, heads_dev, key_dim))[..., None] * state
-        + k_rows[..., None] * v_rows[:, :, None, :]
-    )
-    read = jnp.einsum("shk,shkv->shv", q_rows, new_state)
-    read_sq = jnp.mean(read * read, axis=-1, keepdims=True)
-    gated = (
-        read
-        * lax.rsqrt(read_sq + eps)
-        * head_gain.astype(f32).reshape(heads_dev, val_dim)
-        * jax.nn.silu(rgates)
-    )
-    return gated.reshape(seq_dev, heads_dev * val_dim).astype(bf16)
 
 
 def to_bf16(value):
@@ -474,16 +511,10 @@
     other = [shift(packed, C, 1)]
     other += [shift(w, C, 1) for w in own[1:]]
 
-    tok_parts, first_scale = scale(tokens, norm_gain, nz)
-    tok = lax.all_to_all(tok_parts, Z, 0, 0, tiled=True)
-
-    out_t = w_out.T
-    near = lax.ppermute(out_t, Z, [(i, i ^ 1) for i in range(nz)])
-    odd = lax.rem(lax.axis_index(Z), 2) == 1
-    pair = jnp.where(odd, jnp.stack([near, out_t]), jnp.stack([out_t, near]))
-    pairs = [pair] + [shift(pair, Z, 2 * i) for i in order_of(nz // 2)]
-    pairs = [pairs[0]] + [pairs[1 + order_of(nz // 2).index(i)] for i in range(1, nz // 2)]
-    out_z = join(pairs)
+    seqs = tokens.shape[0]
+    payload, first_scale = scale(tokens, norm_gain, w_out.T, nz)
+    moved = lax.all_to_all(payload, Z, 0, 0, tiled=True)
+    out_z = moved[:, seqs:]
     blocks = [out_z] + [shift(out_z, X, i) for i in range(1, nx)]
 
     downs = split(where, w_down[0], nz, nt)
@@ -494,38 +525,36 @@
     gain_of = jnp.moveaxis(gain_of, 1, 0).reshape(nt, 1, part)
     inverse = 1.0 / gain_of
 
-    parts = project(where, tok, own, other)
-    arrived = [parts[0]] + [shift(parts[s], Z, s) for s in order_of(nz)]
-    gated = attention(
-        arrived,
-        first_scale[:, :1],
-        decay_shift,
-        state,
-        head_gain,
-        w_query.shape[1],
-        w_value.shape[1],
-    )
+    parts = project(where, moved, seqs, own, other)
+    arrived = lax.all_to_all(parts, Z, 0, 0, tiled=True)
+    gated = attend(arrived, first_scale, decay_shift, state, head_gain)
     partner = shift(gated, C, 1)
     mixed = mix(where, gated, partner, blocks)
     mixed = [mixed[0]] + [shift(mixed[s], T, s) for s in range(1, nt)]
-    seqs = gated.shape[0]
     mine = functools.reduce(jnp.add, [m[:seqs].astype(f32) for m in mixed]).astype(bf16)
     theirs = functools.reduce(jnp.add, [m[seqs:].astype(f32) for m in mixed]).astype(bf16)
     other_half = shift(theirs, C, 1)
     outbound, stream = dispatch(
         where, tokens, gain_of, sender, mine, other_half, nz, nt
     )
-    rows = lax.all_to_all(outbound.reshape(n_ep, -1, 128), EP, 0, 0, tiled=True).reshape(-1, 128)
-    rows = unpack(rows, slots)
+    rows = lax.all_to_all(
+        outbound.reshape(n_ep, -1, 128), EP, 0, 0, tiled=True
+    ).reshape(-1, 128)
     pieces = [rows] + [shift(rows, T, s) for s in range(1, nt)]
     gates = w_gate.reshape(nz, nt, chunk, -1)
     lins = w_lin.reshape(nz, nt, chunk, -1)
-    steps = [s for s in range(nt) if s != nt // 2]
-    before = expert(where, inverse, gates, lins, steps, [pieces[s] for s in steps], None)
-    act = expert(where, inverse, gates, lins, [nt // 2], [pieces[nt // 2]], before)[0]
+    far = nt // 2
+    picked = pick(where, gates, lins, far)
+    steps = [s for s in range(nt) if s != far]
+    before = expert_first(
+        where, inverse, gates, lins, steps, [pieces[s] for s in steps], slots
+    )
+    act = expert_last(where, inverse, *picked, far, nt, pieces[far], before)
     acts = [act] + [shift(act, T, s) for s in range(1, nt)]
     done = down_sum(acts, downs)
-    returned = lax.all_to_all(done.reshape(n_ep, -1, 128), EP, 0, 0, tiled=True).reshape(-1, 128)
+    returned = lax.all_to_all(
+        done.reshape(n_ep, -1, 128), EP, 0, 0, tiled=True
+    ).reshape(-1, 128)
     result = combine(returned, weights, stream)
     results = [result] + [shift(result, T, s) for s in range(1, nt)]
     return finish(where, results, nz)

time: 228 us -> 210 us (0.921)
  starting transfers between devices: 76.2 us -> 58.1 us
  waiting for transfers between devices: 69.5 us -> 75 us
  other arithmetic: 8.08 us -> 3.71 us
  Pallas kernels: 35.1 us -> 39.4 us
  matrix products: 3.89 us -> 0 us
    ppermute x37 -> x27, starting transfers between devices: 59.9 us -> 38.7 us  [shift(): return lax.ppermute(value, axis, [(i, (i + by) % n) for i in range(n)])]
    all_to_all x1 -> x2, waiting for transfers between devices: 0.01 us -> 19.4 us  [the longest x1 15.7 us: on_device(): arrived = lax.all_to_all(parts, Z, 0, 0, tiled=True)]
    ppermute x37 -> x27, waiting for transfers between devices: 51.7 us -> 41.1 us  [shift(): return lax.ppermute(value, axis, [(i, (i + by) % n) for i in range(n)])]
    all_to_all x1 -> x2, starting transfers between devices: 8.19 us -> 12.7 us  [the longest x1 9 us: on_device(): moved = lax.all_to_all(payload, Z, 0, 0, tiled=True)]
    pallas_call x6, Pallas kernels: 17.3 us -> 21.7 us  [the longest x1 5.67 us: attend(): pl.pallas_call(functools.partial(attend_kernel, heads), grid=(seqs // ste...]
    dot_general x1 -> x0, matrix products: 3.89 us -> none  [attention(): read = jnp.einsum('shk,shkv->shv', q_rows, new_state)]
    ppermute x1 -> x0, waiting for transfers between devices: 3.22 us -> none  [on_device(): near = lax.ppermute(out_t, Z, [(i, i ^ 1) for i in range(nz)])]
    unnamed x68 -> x67, local copies, waits for them, and re-layouts: 7.1 us -> 7.09 us
  transfers between devices with their start and end apart: 40 -> 30, of which waited for: 18 -> 18; matrix products, arithmetic and copies ran while one was open for 7% -> 2% of each run, Pallas kernels for 8% -> 10%
where the time goes in v1:
time: 210 us; the launch traced here: 209 us
  waiting for transfers between devices  75 us (36%)
  starting transfers between devices  58.1 us (28%)
  Pallas kernels  39.4 us (19%)
  blocking collectives  22.7 us (11%)
  local copies, waits for them, and re-layouts  9.78 us (5%)
  other arithmetic  3.71 us (2%)
    ppermute x27, waiting for transfers between devices, shift(): return lax.ppermute(value, axis, [(i, (i + by) % n) for i in range(n)])  41.1 us
    ppermute x27, starting transfers between devices, shift(): return lax.ppermute(value, axis, [(i, (i + by) % n) for i in range(n)])  38.7 us
    all_to_all x1, blocking collectives, on_device(): lax.all_to_all(outbound.reshape(n_ep, -1, 128), EP, 0, 0, tiled=True)  22.7 us
    all_to_all x1, waiting for transfers between devices, on_device(): arrived = lax.all_to_all(parts, Z, 0, 0, tiled=True)  15.7 us
    all_to_all x1, waiting for transfers between devices, on_device(): lax.all_to_all(done.reshape(n_ep, -1, 128), EP, 0, 0, tiled=True)  14.5 us
    all_to_all x1, starting transfers between devices, on_device(): moved = lax.all_to_all(payload, Z, 0, 0, tiled=True)  9 us
    unnamed x67, local copies, waits for them, and re-layouts  7.09 us
    all_to_all x1, starting transfers between devices, on_device(): lax.all_to_all(done.reshape(n_ep, -1, 128), EP, 0, 0, tiled=True)  6.7 us
  transfers between devices with their start and end apart: 30, of which 18 were waited for; matrix products, arithmetic and copies ran while one was open for 2% of the time, Pallas kernels for 10%

profile of v1, /device:TPU:1, one launch (start us, length us, event | category | flops | bytes accessed | tf_op | source)
XLA Modules:
  0.0 208.9 jit_solution(806764797784076325)
XLA Ops:
  0.0 2.0 scale.1
  2.0 9.0 %all-to-all-start = ((bf16[8,88,512]{2,1,0:T(8,128)(2,1)}), bf16[8,88,512]{2,1,0:T(8,128)(2,1)S(1)}, u32[]{:S(2)}, u32[]{:S(2)}) async-start(bf16[8,88,512]{2,1,0:T(8,128)(2,1)} %get-tuple-element.24), calls=%async_computation | async-start | bytes 1441792 | tf_op jit(solution)/shard_map/all_to_all | solution.py:516
  11.0 1.6 pack.1.refs_0_
  12.6 1.2 collective-permute-start
  13.8 2.5 %collective-permute-start.1 = (bf16[64,1792]{1,0:T(8,128)(2,1)}, bf16[64,1792]{1,0:T(8,128)(2,1)S(1)}, u32[]{:S(2)}, u32[]{:S(2)}) collective-permute-start(bf16[64,1792]{1,0:T(8,128)(2,1)} %pack.1.refs_0_), channel_id=1, source_target_pairs={{0,16},{8,24},{16,0},{24,8},{1,17},{9,25},{17,1},{25,9},{2,18},{10... | collective-permute-start | bytes 688136 | tf_op jit(solution)/shard_map/ppermute | solution.py:26
  16.2 1.2 collective-permute-start.2
  17.4 1.8 collective-permute-start.3
  19.2 1.0 collective-permute-done.refs_1_
  20.2 2.2 %collective-permute-start.4 = (bf16[64,1792]{1,0:T(8,128)(2,1)S(1)}, bf16[64,1792]{1,0:T(8,128)(2,1)S(1)}, u32[]{:S(2)}, u32[]{:S(2)}) collective-permute-start(bf16[64,1792]{1,0:T(8,128)(2,1)S(1)} %collective-permute-done.refs_1_), channel_id=1, source_target_pairs={{0,4},{4,0},{1,5},{5,1},{2,6},{6,2},{3,7},{7,3},{8,12},{12,8},{9,1... | collective-permute-start | bytes 688136 | tf_op jit(solution)/shard_map/ppermute | solution.py:26
  22.5 3.7 %collective-permute-done.1.refs_2_ = bf16[64,1792]{1,0:T(8,128)(2,1)S(1)} collective-permute-done((bf16[64,1792]{1,0:T(8,128)(2,1)}, bf16[64,1792]{1,0:T(8,128)(2,1)S(1)}, u32[]{:S(2)}, u32[]{:S(2)}) %collective-permute-start.1) | collective-permute-done | bytes 229408 | tf_op jit(solution)/shard_map/ppermute | solution.py:26
  26.1 1.8 collective-permute-start.5
  29.4 3.7 %all-to-all-done.tok = bf16[8,88,512]{2,1,0:T(8,128)(2,1)S(1)} async-done(((bf16[8,88,512]{2,1,0:T(8,128)(2,1)}), bf16[8,88,512]{2,1,0:T(8,128)(2,1)S(1)}, u32[]{:S(2)}, u32[]{:S(2)}) %all-to-all-start) | async-done | bytes 720928 | tf_op jit(solution)/shard_map/all_to_all | solution.py:516
  33.2 0.9 copy-done
  34.1 3.3 %project.1 = bf16[8,24,1792]{2,1,0:T(8,128)(2,1)} custom-call(s32[4]{0:T(128)} %pad_add_fusion.where, bf16[8,88,512]{2,1,0:T(8,128)(2,1)} %copy-done, bf16[64,1792]{1,0:T(8,128)(2,1)} %pack.1.refs_0_, bf16[64,1792]{1,0:T(8,128)(2,1)} %copy-done.14, bf16[64,1792]{1,0:T(8,128)(2,1)} %copy-done.15, bf16[64,1792]{1,0:T(8,128)(2,1)} %copy-done.16, ...), custom_call_target="tpu_custom_call" | custom-call | flops 352321536 | bytes 1835008 | tf_op jit(solution)/shard_map/project/pallas_call | solution.py:125
  37.4 3.7 %all-to-all-start.1 = ((bf16[8,24,1792]{2,1,0:T(8,128)(2,1)}), bf16[8,24,1792]{2,1,0:T(8,128)(2,1)S(1)}, u32[]{:S(2)}, u32[]{:S(2)}) async-start(bf16[8,24,1792]{2,1,0:T(8,128)(2,1)} %project.1), calls=%async_computation.1 | async-start | bytes 1376256 | tf_op jit(solution)/shard_map/all_to_all | solution.py:529
  41.3 1.1 slice.36.refs_0_
  42.4 2.5 %collective-permute-start.10 = (bf16[8,64,512]{2,1,0:T(8,128)(2,1)S(1)}, bf16[8,64,512]{2,1,0:T(8,128)(2,1)S(1)}, u32[]{:S(2)}, u32[]{:S(2)}) collective-permute-start(bf16[8,64,512]{2,1,0:T(8,128)(2,1)S(1)} %slice.36.refs_0_), channel_id=1, source_target_pairs={{0,24},{8,0},{16,8},{24,16},{1,25},{9,1},{17,9},{25,17},{2,26},{10... | collective-permute-start | bytes 1572872 | tf_op jit(solution)/shard_map/ppermute | solution.py:26
  44.9 1.7 collective-permute-start.9
  46.9 15.7 %all-to-all-done.1.arrived = bf16[8,24,1792]{2,1,0:T(8,128)(2,1)S(1)} async-done(((bf16[8,24,1792]{2,1,0:T(8,128)(2,1)}), bf16[8,24,1792]{2,1,0:T(8,128)(2,1)S(1)}, u32[]{:S(2)}, u32[]{:S(2)}) %all-to-all-start.1) | async-done | bytes 688160 | tf_op jit(solution)/shard_map/all_to_all | solution.py:529
  62.6 0.9 copy-done.1
  63.4 5.7 %attend.1.gated = bf16[24,512]{1,0:T(8,128)(2,1)} custom-call(bf16[8,24,1792]{2,1,0:T(8,128)(2,1)} %copy-done.1, f32[24,128]{1,0:T(8,128)} %get-tuple-element.25.scale, f32[24,256]{1,0:T(8,128)} %shift_of.1, f32[24,2,128,256]{3,2,1,0:T(8,128)} %state.1, bf16[512]{0:T(512)(128)(2,1)} %gain.3), custom_call_target="tpu_custom_call" | custom-call | flops 6291456 | bytes 6291456 | tf_op jit(solution)/shard_map/attend/pallas_call | solution.py:174
  70.0 0.7 collective-permute-done.7.partner
  71.8 3.7 %mix.1 = (bf16[48,512]{1,0:T(8,128)(2,1)}, bf16[48,512]{1,0:T(8,128)(2,1)}, bf16[48,512]{1,0:T(8,128)(2,1)}, bf16[48,512]{1,0:T(8,128)(2,1)}) custom-call(s32[4]{0:T(128)} %pad_add_fusion.where, bf16[24,512]{1,0:T(8,128)(2,1)} %attend.1.gated, bf16[24,512]{1,0:T(8,128)(2,1)} %copy-done.28, bf16[8,64,512]{2,1,0:T(8,128)(2,1)} %copy-done.2, ...), custom_call_target="tpu_custom_call" | custom-call | flops 100663296 | bytes 2097152 | tf_op jit(solution)/shard_map/mix/pallas_call | solution.py:219
  75.4 1.4 collective-permute-start.11
  76.8 2.6 %collective-permute-start.12 = (bf16[48,512]{1,0:T(8,128)(2,1)}, bf16[48,512]{1,0:T(8,128)(2,1)S(1)}, u32[]{:S(2)}, u32[]{:S(2)}) collective-permute-start(bf16[48,512]{1,0:T(8,128)(2,1)} %get-tuple-element.28), channel_id=1, source_target_pairs={{0,2},{1,3},{2,0},{3,1},{4,6},{5,7},{6,4},{7,5},{8,10},{9,11},{10,... | collective-permute-start | bytes 147464 | tf_op jit(solution)/shard_map/ppermute | solution.py:26
  79.4 1.1 collective-permute-start.13
  80.5 1.2 collective-permute-done.12
  81.7 1.5 collective-permute-done.13
  83.2 1.4 add_convert_fusion
  84.6 2.7 %collective-permute-start.14 = (bf16[24,512]{1,0:T(8,128)(2,1)S(1)}, bf16[24,512]{1,0:T(8,128)(2,1)S(1)}, u32[]{:S(2)}, u32[]{:S(2)}) collective-permute-start(bf16[24,512]{1,0:T(8,128)(2,1)S(1)} %get-tuple-element.41), channel_id=1, source_target_pairs={{0,4},{4,0},{1,5},{5,1},{2,6},{6,2},{3,7},{7,3},{8,12},{12,8},{9,1... | collective-permute-start | bytes 73736 | tf_op jit(solution)/shard_map/ppermute | solution.py:26
  87.4 0.7 copy.36
  89.3 2.1 %dispatch.1 = (bf16[1536,128]{1,0:T(8,128)(2,1)}, f32[24,1024]{1,0:T(8,128)}) custom-call(s32[4]{0:T(128)} %pad_add_fusion.where, bf16[24,4096]{1,0:T(8,128)(2,1)} %tokens.3, f32[4,1,1024]{2,1,0:T(1,128)} %bitcast.31, bf16[192,24]{1,0:T(8,128)(2,1)} %bitcast.30, bf16[24,512]{1,0:T(8,128)(2,1)} %get-tuple-element.42.mine, bf16[24,512]{1,0:T(8,128)(2,1)} %copy-done.29), custom_call_target="tpu_custom_call" | custom-call | flops 9437184 | bytes 1179648 | tf_op jit(solution)/shard_map/dispatch/pallas_call | solution.py:261
  91.4 22.7 %all_to_all.20 = bf16[64,24,128]{2,1,0:T(8,128)(2,1)S(1)} all-to-all(bf16[64,24,128]{2,1,0:T(8,128)(2,1)} %bitcast.29), channel_id=1, replica_groups=mesh['ep_0'=8,'ep_1'=4,'ep_2'=2,'tp'=4] {'ep_0','ep_1','ep_2'}, dimensions={0} | all-to-all | bytes 786432 | tf_op jit(solution)/shard_map/all_to_all | solution.py:540
  114.1 3.7 %split.1 = (bf16[256,1024]{1,0:T(8,128)(2,1)}, bf16[256,1024]{1,0:T(8,128)(2,1)}, bf16[256,1024]{1,0:T(8,128)(2,1)}, bf16[256,1024]{1,0:T(8,128)(2,1)}) custom-call(s32[4]{0:T(128)} %pad_add_fusion.where, bf16[256,4096]{1,0:T(8,128)(2,1)} %bitcast.22), custom_call_target="tpu_custom_call" | custom-call | flops 1000000 | bytes 4194304 | tf_op jit(solution)/shard_map/split/pallas_call | solution.py:97
  117.7 0.8 collective-permute-start.21
  118.5 1.9 collective-permute-start.17
  120.4 2.1 %collective-permute-start.22 = (bf16[256,1024]{1,0:T(8,128)(2,1)}, bf16[256,1024]{1,0:T(8,128)(2,1)S(1)}, u32[]{:S(2)}, u32[]{:S(2)}) collective-permute-start(bf16[256,1024]{1,0:T(8,128)(2,1)} %get-tuple-element.36), channel_id=1, source_target_pairs={{0,2},{1,3},{2,0},{3,1},{4,6},{5,7},{6,4},{7,5},{8,10},{9,11},{10,... | collective-permute-start | bytes 1572872 | tf_op jit(solution)/shard_map/ppermute | solution.py:26
  122.5 0.6 collective-permute-start.23
  123.1 2.6 %collective-permute-done.16.refs_1_ = bf16[1536,128]{1,0:T(8,128)(2,1)S(1)} collective-permute-done((bf16[1536,128]{1,0:T(8,128)(2,1)S(1)}, bf16[1536,128]{1,0:T(8,128)(2,1)S(1)}, u32[]{:S(2)}, u32[]{:S(2)}) %collective-permute-start.16) | collective-permute-done | bytes 393248 | tf_op jit(solution)/shard_map/ppermute | solution.py:26
  125.7 3.0 %pick.1 = (bf16[8,128,256]{2,1,0:T(8,128)(2,1)}, bf16[8,128,256]{2,1,0:T(8,128)(2,1)}) custom-call(s32[4]{0:T(128)} %pad_add_fusion.where, bf16[8,4,128,256]{3,2,1,0:T(8,128)(2,1)} %bitcast.18, bf16[8,4,128,256]{3,2,1,0:T(8,128)(2,1)} %bitcast.20), custom_call_target="tpu_custom_call" | custom-call | flops 1000000 | bytes 2097152 | tf_op jit(solution)/shard_map/pick/pallas_call | solution.py:294
  128.8 0.6 broadcast_divide_fusion.inverse
  129.4 0.7 copy-done.13
  130.1 5.2 %expert_first.1 = (f32[192,256]{1,0:T(8,128)}, f32[192,256]{1,0:T(8,128)}, f32[192,128]{1,0:T(8,128)}) custom-call(s32[4]{0:T(128)} %pad_add_fusion.where, f32[4,1,1024]{2,1,0:T(1,128)} %broadcast_divide_fusion.inverse, bf16[8,4,128,256]{3,2,1,0:T(8,128)(2,1)} %bitcast.19, bf16[8,4,128,256]{3,2,1,0:T(8,128)(2,1)} %bitcast.21, bf16[1536,128]{1,0:T(8,128)(2,1)} %bitcast.28, ...), custom_call_target="tpu_custom_call" | custom-call | flops 603979776 | bytes 3145728 | tf_op jit(solution)/shard_map/expert_first/pallas_call | solution.py:343
  135.3 22.0 %collective-permute-done.15.piece = bf16[1536,128]{1,0:T(8,128)(2,1)S(1)} collective-permute-done((bf16[1536,128]{1,0:T(8,128)(2,1)S(1)}, bf16[1536,128]{1,0:T(8,128)(2,1)S(1)}, u32[]{:S(2)}, u32[]{:S(2)}) %collective-permute-start.15) | collective-permute-done | bytes 393248 | tf_op jit(solution)/shard_map/ppermute | solution.py:26
  157.4 0.8 copy-done.11
  158.1 2.6 %expert_last.1.refs_0_ = bf16[192,256]{1,0:T(8,128)(2,1)} custom-call(s32[4]{0:T(128)} %pad_add_fusion.where, f32[4,1,1024]{2,1,0:T(1,128)} %broadcast_divide_fusion.inverse, bf16[8,128,256]{2,1,0:T(8,128)(2,1)} %get-tuple-element.22.w_gate, bf16[8,128,256]{2,1,0:T(8,128)(2,1)} %get-tuple-element.23.w_lin, bf16[1536,128]{1,0:T(8,128)(2,1)} %copy-done.11, ...), custom_call_target="tpu_custom_call" | custom-call | flops 201326592 | bytes 1048576 | tf_op jit(solution)/shard_map/expert_last/pallas_call | solution.py:382
  160.7 4.3 %collective-permute-start.18 = (bf16[192,256]{1,0:T(8,128)(2,1)}, bf16[192,256]{1,0:T(8,128)(2,1)S(1)}, u32[]{:S(2)}, u32[]{:S(2)}) collective-permute-start(bf16[192,256]{1,0:T(8,128)(2,1)} %expert_last.1.refs_0_), channel_id=1, source_target_pairs={{0,1},{1,2},{2,3},{3,0},{4,5},{5,6},{6,7},{7,4},{8,9},{9,10},{10,1... | collective-permute-start | bytes 294920 | tf_op jit(solution)/shard_map/ppermute | solution.py:26
  165.0 2.3 %collective-permute-start.19 = (bf16[192,256]{1,0:T(8,128)(2,1)}, bf16[192,256]{1,0:T(8,128)(2,1)S(1)}, u32[]{:S(2)}, u32[]{:S(2)}) collective-permute-start(bf16[192,256]{1,0:T(8,128)(2,1)} %expert_last.1.refs_0_), channel_id=1, source_target_pairs={{0,2},{1,3},{2,0},{3,1},{4,6},{5,7},{6,4},{7,5},{8,10},{9,11},{10,... | collective-permute-start | bytes 294920 | tf_op jit(solution)/shard_map/ppermute | solution.py:26
  167.4 0.9 collective-permute-done.18.refs_1_
  168.3 2.5 %collective-permute-done.19.refs_2_ = bf16[192,256]{1,0:T(8,128)(2,1)S(1)} collective-permute-done((bf16[192,256]{1,0:T(8,128)(2,1)}, bf16[192,256]{1,0:T(8,128)(2,1)S(1)}, u32[]{:S(2)}, u32[]{:S(2)}) %collective-permute-start.19) | collective-permute-done | bytes 98336 | tf_op jit(solution)/shard_map/ppermute | solution.py:26
  170.8 1.3 collective-permute-done.20.refs_3_
  172.7 3.1 %down.1 = bf16[1536,128]{1,0:T(8,128)(2,1)} custom-call(bf16[192,256]{1,0:T(8,128)(2,1)} %expert_last.1.refs_0_, bf16[192,256]{1,0:T(8,128)(2,1)} %copy-done.22, bf16[192,256]{1,0:T(8,128)(2,1)} %copy-done.23, bf16[192,256]{1,0:T(8,128)(2,1)} %copy-done.24, bf16[256,1024]{1,0:T(8,128)(2,1)} %get-tuple-element.34.refs_4_, bf16[256,1024]{1,0:T(8,128)(2,1)} %copy-done.8, ...), custom_call_target="tpu_custom_call" | custom-call | flops 402653184 | bytes 2097152 | tf_op jit(solution)/shard_map/down/pallas_call | solution.py:407
  175.8 6.7 %all-to-all-start.3 = ((bf16[64,24,128]{2,1,0:T(8,128)(2,1)}), bf16[64,24,128]{2,1,0:T(8,128)(2,1)S(1)}, u32[]{:S(2)}, u32[]{:S(2)}) async-start(bf16[64,24,128]{2,1,0:T(8,128)(2,1)} %bitcast.24), calls=%async_computation.3 | async-start | bytes 786432 | tf_op jit(solution)/shard_map/all_to_all | solution.py:555
  182.5 0.6 pad_maximum_fusion.weights
  183.1 14.5 %all-to-all-done.3 = bf16[64,24,128]{2,1,0:T(8,128)(2,1)S(1)} async-done(((bf16[64,24,128]{2,1,0:T(8,128)(2,1)}), bf16[64,24,128]{2,1,0:T(8,128)(2,1)S(1)}, u32[]{:S(2)}, u32[]{:S(2)}) %all-to-all-start.3) | async-done | bytes 393248 | tf_op jit(solution)/shard_map/all_to_all | solution.py:555
  197.7 0.7 copy-done.3
  198.4 2.0 combine.1.refs_0_
  200.4 2.7 %collective-permute-start.25 = (bf16[24,1024]{1,0:T(8,128)(2,1)}, bf16[24,1024]{1,0:T(8,128)(2,1)S(1)}, u32[]{:S(2)}, u32[]{:S(2)}) collective-permute-start(bf16[24,1024]{1,0:T(8,128)(2,1)} %combine.1.refs_0_), channel_id=1, source_target_pairs={{0,2},{1,3},{2,0},{3,1},{4,6},{5,7},{6,4},{7,5},{8,10},{9,11},{10,... | collective-permute-start | bytes 147464 | tf_op jit(solution)/shard_map/ppermute | solution.py:26
  203.1 0.6 collective-permute-start.26
  203.7 1.0 collective-permute-done.24.refs_1_
  204.7 0.9 collective-permute-done.25.refs_2_
  205.6 1.1 collective-permute-done.26.refs_3_
  206.7 0.6 copy-done.27
  207.3 1.6 finish.1
  (94 shorter events, 6.0 us)
Async XLA Ops:
  2.0 31.2 %all-to-all-start = ((bf16[8,88,512]{2,1,0:T(8,128)(2,1)}), bf16[8,88,512]{2,1,0:T(8,128)(2,1)S(1)}, u32[]{:S(2)}, u32[]{:S(2)}) async-start(bf16[8,88,512]{2,1,0:T(8,128)(2,1)} %get-tuple-element.24), calls=%async_computation | async-start | bytes 1441792 | tf_op jit(solution)/shard_map/all_to_all | solution.py:516
  12.6 7.6 %collective-permute-start = (bf16[64,1792]{1,0:T(8,128)(2,1)}, bf16[64,1792]{1,0:T(8,128)(2,1)S(1)}, u32[]{:S(2)}, u32[]{:S(2)}) collective-permute-start(bf16[64,1792]{1,0:T(8,128)(2,1)} %pack.1.refs_0_), channel_id=1, source_target_pairs={{0,8},{8,16},{16,24},{24,0},{1,9},{9,17},{17,25},{25,1},{2,10},{10... | collective-permute-start | bytes 688136 | tf_op jit(solution)/shard_map/ppermute | solution.py:26
  13.8 12.3 %collective-permute-start.1 = (bf16[64,1792]{1,0:T(8,128)(2,1)}, bf16[64,1792]{1,0:T(8,128)(2,1)S(1)}, u32[]{:S(2)}, u32[]{:S(2)}) collective-permute-start(bf16[64,1792]{1,0:T(8,128)(2,1)} %pack.1.refs_0_), channel_id=1, source_target_pairs={{0,16},{8,24},{16,0},{24,8},{1,17},{9,25},{17,1},{25,9},{2,18},{10... | collective-permute-start | bytes 688136 | tf_op jit(solution)/shard_map/ppermute | solution.py:26
  16.2 11.7 %collective-permute-start.2 = (bf16[64,1792]{1,0:T(8,128)(2,1)}, bf16[64,1792]{1,0:T(8,128)(2,1)S(1)}, u32[]{:S(2)}, u32[]{:S(2)}) collective-permute-start(bf16[64,1792]{1,0:T(8,128)(2,1)} %pack.1.refs_0_), channel_id=1, source_target_pairs={{0,24},{8,0},{16,8},{24,16},{1,25},{9,1},{17,9},{25,17},{2,26},{10... | collective-permute-start | bytes 688136 | tf_op jit(solution)/shard_map/ppermute | solution.py:26
  17.4 11.2 %collective-permute-start.3 = (bf16[64,1792]{1,0:T(8,128)(2,1)}, bf16[64,1792]{1,0:T(8,128)(2,1)S(1)}, u32[]{:S(2)}, u32[]{:S(2)}) collective-permute-start(bf16[64,1792]{1,0:T(8,128)(2,1)} %pack.1.refs_0_), channel_id=1, source_target_pairs={{0,4},{4,0},{1,5},{5,1},{2,6},{6,2},{3,7},{7,3},{8,12},{12,8},{9,1... | collective-permute-start | bytes 688136 | tf_op jit(solution)/shard_map/ppermute | solution.py:26
  20.2 12.9 %copy-start.14 = (bf16[64,1792]{1,0:T(8,128)(2,1)}, bf16[64,1792]{1,0:T(8,128)(2,1)S(1)}, u32[]{:S(2)}) copy-start(bf16[64,1792]{1,0:T(8,128)(2,1)S(1)} %collective-permute-done.refs_1_) | copy-start | bytes 688132
  20.2 8.4 %collective-permute-start.4 = (bf16[64,1792]{1,0:T(8,128)(2,1)S(1)}, bf16[64,1792]{1,0:T(8,128)(2,1)S(1)}, u32[]{:S(2)}, u32[]{:S(2)}) collective-permute-start(bf16[64,1792]{1,0:T(8,128)(2,1)S(1)} %collective-permute-done.refs_1_), channel_id=1, source_target_pairs={{0,4},{4,0},{1,5},{5,1},{2,6},{6,2},{3,7},{7,3},{8,12},{12,8},{9,1... | collective-permute-start | bytes 688136 | tf_op jit(solution)/shard_map/ppermute | solution.py:26
  26.1 7.0 %copy-start.15 = (bf16[64,1792]{1,0:T(8,128)(2,1)}, bf16[64,1792]{1,0:T(8,128)(2,1)S(1)}, u32[]{:S(2)}) copy-start(bf16[64,1792]{1,0:T(8,128)(2,1)S(1)} %collective-permute-done.1.refs_2_) | copy-start | bytes 688132
  26.1 2.9 %collective-permute-start.5 = (bf16[64,1792]{1,0:T(8,128)(2,1)S(1)}, bf16[64,1792]{1,0:T(8,128)(2,1)S(1)}, u32[]{:S(2)}, u32[]{:S(2)}) collective-permute-start(bf16[64,1792]{1,0:T(8,128)(2,1)S(1)} %collective-permute-done.1.refs_2_), channel_id=1, source_target_pairs={{0,4},{4,0},{1,5},{5,1},{2,6},{6,2},{3,7},{7,3},{8,12},{12,8},{9,1... | collective-permute-start | bytes 688136 | tf_op jit(solution)/shard_map/ppermute | solution.py:26
  27.9 5.2 %copy-start.16 = (bf16[64,1792]{1,0:T(8,128)(2,1)}, bf16[64,1792]{1,0:T(8,128)(2,1)S(1)}, u32[]{:S(2)}) copy-start(bf16[64,1792]{1,0:T(8,128)(2,1)S(1)} %collective-permute-done.2.refs_3_) | copy-start | bytes 688132
  27.9 1.5 collective-permute-start.6
  28.6 12.5 %copy-start.31 = (s32[24,4]{0,1:T(4,128)S(1)}, s32[24,4]{0,1:T(4,128)}, u32[]{:S(2)}) copy-start(s32[24,4]{0,1:T(4,128)} %param.32) | copy-start | bytes 1156
  28.6 4.5 %copy-start.17 = (bf16[64,1792]{1,0:T(8,128)(2,1)}, bf16[64,1792]{1,0:T(8,128)(2,1)S(1)}, u32[]{:S(2)}) copy-start(bf16[64,1792]{1,0:T(8,128)(2,1)S(1)} %collective-permute-done.3.refs_4_) | copy-start | bytes 688132
  28.6 4.5 %copy-start.18 = (bf16[64,1792]{1,0:T(8,128)(2,1)}, bf16[64,1792]{1,0:T(8,128)(2,1)S(1)}, u32[]{:S(2)}) copy-start(bf16[64,1792]{1,0:T(8,128)(2,1)S(1)} %collective-permute-done.4.refs_5_) | copy-start | bytes 688132
  29.0 4.1 %copy-start.19 = (bf16[64,1792]{1,0:T(8,128)(2,1)}, bf16[64,1792]{1,0:T(8,128)(2,1)S(1)}, u32[]{:S(2)}) copy-start(bf16[64,1792]{1,0:T(8,128)(2,1)S(1)} %collective-permute-done.5.refs_6_) | copy-start | bytes 688132
  29.4 3.7 %copy-start.20 = (bf16[64,1792]{1,0:T(8,128)(2,1)}, bf16[64,1792]{1,0:T(8,128)(2,1)S(1)}, u32[]{:S(2)}) copy-start(bf16[64,1792]{1,0:T(8,128)(2,1)S(1)} %collective-permute-done.6.refs_7_) | copy-start | bytes 688132
  33.2 0.9 copy-start
  37.4 9.5 %copy-start.30 = (bf16[4096]{0:T(1024)(128)(2,1)S(1)}, bf16[4096]{0:T(1024)(128)(2,1)}, u32[]{:S(2)}) copy-start(bf16[4096]{0:T(1024)(128)(2,1)} %param.28) | copy-start | bytes 24580
  37.4 25.2 %all-to-all-start.1 = ((bf16[8,24,1792]{2,1,0:T(8,128)(2,1)}), bf16[8,24,1792]{2,1,0:T(8,128)(2,1)S(1)}, u32[]{:S(2)}, u32[]{:S(2)}) async-start(bf16[8,24,1792]{2,1,0:T(8,128)(2,1)} %project.1), calls=%async_computation.1 | async-start | bytes 1376256 | tf_op jit(solution)/shard_map/all_to_all | solution.py:529
  42.4 28.3 %copy-start.2 = (bf16[8,64,512]{2,1,0:T(8,128)(2,1)}, bf16[8,64,512]{2,1,0:T(8,128)(2,1)S(1)}, u32[]{:S(2)}) copy-start(bf16[8,64,512]{2,1,0:T(8,128)(2,1)S(1)} %slice.36.refs_0_) | copy-start | bytes 1572868
  42.4 27.6 %collective-permute-start.10 = (bf16[8,64,512]{2,1,0:T(8,128)(2,1)S(1)}, bf16[8,64,512]{2,1,0:T(8,128)(2,1)S(1)}, u32[]{:S(2)}, u32[]{:S(2)}) collective-permute-start(bf16[8,64,512]{2,1,0:T(8,128)(2,1)S(1)} %slice.36.refs_0_), channel_id=1, source_target_pairs={{0,24},{8,0},{16,8},{24,16},{1,25},{9,1},{17,9},{25,17},{2,26},{10... | collective-permute-start | bytes 1572872 | tf_op jit(solution)/shard_map/ppermute | solution.py:26
  44.9 25.0 %collective-permute-start.8 = (bf16[8,64,512]{2,1,0:T(8,128)(2,1)S(1)}, bf16[8,64,512]{2,1,0:T(8,128)(2,1)S(1)}, u32[]{:S(2)}, u32[]{:S(2)}) collective-permute-start(bf16[8,64,512]{2,1,0:T(8,128)(2,1)S(1)} %slice.36.refs_0_), channel_id=1, source_target_pairs={{0,8},{8,16},{16,24},{24,0},{1,9},{9,17},{17,25},{25,1},{2,10},{10... | collective-permute-start | bytes 1572872 | tf_op jit(solution)/shard_map/ppermute | solution.py:26
  44.9 25.1 %collective-permute-start.9 = (bf16[8,64,512]{2,1,0:T(8,128)(2,1)S(1)}, bf16[8,64,512]{2,1,0:T(8,128)(2,1)S(1)}, u32[]{:S(2)}, u32[]{:S(2)}) collective-permute-start(bf16[8,64,512]{2,1,0:T(8,128)(2,1)S(1)} %slice.36.refs_0_), channel_id=1, source_target_pairs={{0,16},{8,24},{16,0},{24,8},{1,17},{9,25},{17,1},{25,9},{2,18},{10... | collective-permute-start | bytes 1572872 | tf_op jit(solution)/shard_map/ppermute | solution.py:26
  62.6 0.9 copy-start.1
  69.1 18.2 %copy-start.32 = (f32[24,4]{0,1:T(4,128)S(1)}, f32[24,4]{0,1:T(4,128)}, u32[]{:S(2)}) copy-start(f32[24,4]{0,1:T(4,128)} %param.33) | copy-start | bytes 1156
  69.1 1.6 collective-permute-start.7
  70.0 0.8 copy-start.5
  70.0 1.0 copy-start.6
  70.0 1.2 copy-start.7
  71.2 0.6 copy-start.28
  75.4 5.1 %collective-permute-start.11 = (bf16[48,512]{1,0:T(8,128)(2,1)}, bf16[48,512]{1,0:T(8,128)(2,1)S(1)}, u32[]{:S(2)}, u32[]{:S(2)}) collective-permute-start(bf16[48,512]{1,0:T(8,128)(2,1)} %get-tuple-element.27), channel_id=1, source_target_pairs={{0,1},{1,2},{2,3},{3,0},{4,5},{5,6},{6,7},{7,4},{8,9},{9,10},{10,1... | collective-permute-start | bytes 147464 | tf_op jit(solution)/shard_map/ppermute | solution.py:26
  76.8 4.9 %collective-permute-start.12 = (bf16[48,512]{1,0:T(8,128)(2,1)}, bf16[48,512]{1,0:T(8,128)(2,1)S(1)}, u32[]{:S(2)}, u32[]{:S(2)}) collective-permute-start(bf16[48,512]{1,0:T(8,128)(2,1)} %get-tuple-element.28), channel_id=1, source_target_pairs={{0,2},{1,3},{2,0},{3,1},{4,6},{5,7},{6,4},{7,5},{8,10},{9,11},{10,... | collective-permute-start | bytes 147464 | tf_op jit(solution)/shard_map/ppermute | solution.py:26
  79.4 3.8 %collective-permute-start.13 = (bf16[48,512]{1,0:T(8,128)(2,1)}, bf16[48,512]{1,0:T(8,128)(2,1)S(1)}, u32[]{:S(2)}, u32[]{:S(2)}) collective-permute-start(bf16[48,512]{1,0:T(8,128)(2,1)} %get-tuple-element.29), channel_id=1, source_target_pairs={{0,3},{1,0},{2,1},{3,2},{4,7},{5,4},{6,5},{7,6},{8,11},{9,8},{10,9... | collective-permute-start | bytes 147464 | tf_op jit(solution)/shard_map/ppermute | solution.py:26
  84.6 4.1 %collective-permute-start.14 = (bf16[24,512]{1,0:T(8,128)(2,1)S(1)}, bf16[24,512]{1,0:T(8,128)(2,1)S(1)}, u32[]{:S(2)}, u32[]{:S(2)}) collective-permute-start(bf16[24,512]{1,0:T(8,128)(2,1)S(1)} %get-tuple-element.41), channel_id=1, source_target_pairs={{0,4},{4,0},{1,5},{5,1},{2,6},{6,2},{3,7},{7,3},{8,12},{12,8},{9,1... | collective-permute-start | bytes 73736 | tf_op jit(solution)/shard_map/ppermute | solution.py:26
  88.7 0.6 copy-start.29
  114.1 14.7 %copy-start.4 = (bf16[64,24,128]{2,1,0:T(8,128)(2,1)}, bf16[64,24,128]{2,1,0:T(8,128)(2,1)S(1)}, u32[]{:S(2)}) copy-start(bf16[64,24,128]{2,1,0:T(8,128)(2,1)S(1)} %all_to_all.20) | copy-start | bytes 1179652
  114.1 11.6 %collective-permute-start.16 = (bf16[1536,128]{1,0:T(8,128)(2,1)S(1)}, bf16[1536,128]{1,0:T(8,128)(2,1)S(1)}, u32[]{:S(2)}, u32[]{:S(2)}) collective-permute-start(bf16[1536,128]{1,0:T(8,128)(2,1)S(1)} %bitcast.25), channel_id=1, source_target_pairs={{0,1},{1,2},{2,3},{3,0},{4,5},{5,6},{6,7},{7,4},{8,9},{9,10},{10,1... | collective-permute-start | bytes 1179656 | tf_op jit(solution)/shard_map/ppermute | solution.py:26
  117.7 49.6 %collective-permute-start.21 = (bf16[256,1024]{1,0:T(8,128)(2,1)}, bf16[256,1024]{1,0:T(8,128)(2,1)S(1)}, u32[]{:S(2)}, u32[]{:S(2)}) collective-permute-start(bf16[256,1024]{1,0:T(8,128)(2,1)} %get-tuple-element.35), channel_id=1, source_target_pairs={{0,1},{1,2},{2,3},{3,0},{4,5},{5,6},{6,7},{7,4},{8,9},{9,10},{10,1... | collective-permute-start | bytes 1572872 | tf_op jit(solution)/shard_map/ppermute | solution.py:26
  118.5 10.9 %collective-permute-start.17 = (bf16[1536,128]{1,0:T(8,128)(2,1)S(1)}, bf16[1536,128]{1,0:T(8,128)(2,1)S(1)}, u32[]{:S(2)}, u32[]{:S(2)}) collective-permute-start(bf16[1536,128]{1,0:T(8,128)(2,1)S(1)} %bitcast.26), channel_id=1, source_target_pairs={{0,3},{1,0},{2,1},{3,2},{4,7},{5,4},{6,5},{7,6},{8,11},{9,8},{10,9... | collective-permute-start | bytes 1179656 | tf_op jit(solution)/shard_map/ppermute | solution.py:26
  120.4 47.0 %collective-permute-start.22 = (bf16[256,1024]{1,0:T(8,128)(2,1)}, bf16[256,1024]{1,0:T(8,128)(2,1)S(1)}, u32[]{:S(2)}, u32[]{:S(2)}) collective-permute-start(bf16[256,1024]{1,0:T(8,128)(2,1)} %get-tuple-element.36), channel_id=1, source_target_pairs={{0,2},{1,3},{2,0},{3,1},{4,6},{5,7},{6,4},{7,5},{8,10},{9,11},{10,... | collective-permute-start | bytes 1572872 | tf_op jit(solution)/shard_map/ppermute | solution.py:26
  122.5 44.9 %collective-permute-start.23 = (bf16[256,1024]{1,0:T(8,128)(2,1)}, bf16[256,1024]{1,0:T(8,128)(2,1)S(1)}, u32[]{:S(2)}, u32[]{:S(2)}) collective-permute-start(bf16[256,1024]{1,0:T(8,128)(2,1)} %get-tuple-element.37), channel_id=1, source_target_pairs={{0,3},{1,0},{2,1},{3,2},{4,7},{5,4},{6,5},{7,6},{8,11},{9,8},{10,9... | collective-permute-start | bytes 1572872 | tf_op jit(solution)/shard_map/ppermute | solution.py:26
  125.7 3.1 %copy-start.12 = (bf16[1536,128]{1,0:T(8,128)(2,1)}, bf16[1536,128]{1,0:T(8,128)(2,1)S(1)}, u32[]{:S(2)}) copy-start(bf16[1536,128]{1,0:T(8,128)(2,1)S(1)} %collective-permute-done.16.refs_1_) | copy-start | bytes 1179652
  125.7 31.7 %collective-permute-start.15 = (bf16[1536,128]{1,0:T(8,128)(2,1)S(1)}, bf16[1536,128]{1,0:T(8,128)(2,1)S(1)}, u32[]{:S(2)}, u32[]{:S(2)}) collective-permute-start(bf16[1536,128]{1,0:T(8,128)(2,1)S(1)} %bitcast.27), channel_id=1, source_target_pairs={{0,2},{1,3},{2,0},{3,1},{4,6},{5,7},{6,4},{7,5},{8,10},{9,11},{10,... | collective-permute-start | bytes 1179656 | tf_op jit(solution)/shard_map/ppermute | solution.py:26
  125.7 3.0 %copy-start.21 = (f32[4,8,128]{2,1,0:T(8,128)S(1)}, f32[4,8,128]{2,1,0:T(8,128)}, u32[]{:S(2)}) copy-start(f32[4,8,128]{2,1,0:T(8,128)} %copy.33) | copy-start | bytes 49156
  129.4 0.7 copy-start.13
  157.4 0.8 copy-start.11
  160.7 7.6 %collective-permute-start.18 = (bf16[192,256]{1,0:T(8,128)(2,1)}, bf16[192,256]{1,0:T(8,128)(2,1)S(1)}, u32[]{:S(2)}, u32[]{:S(2)}) collective-permute-start(bf16[192,256]{1,0:T(8,128)(2,1)} %expert_last.1.refs_0_), channel_id=1, source_target_pairs={{0,1},{1,2},{2,3},{3,0},{4,5},{5,6},{6,7},{7,4},{8,9},{9,10},{10,1... | collective-permute-start | bytes 294920 | tf_op jit(solution)/shard_map/ppermute | solution.py:26
  165.0 5.8 %collective-permute-start.19 = (bf16[192,256]{1,0:T(8,128)(2,1)}, bf16[192,256]{1,0:T(8,128)(2,1)S(1)}, u32[]{:S(2)}, u32[]{:S(2)}) collective-permute-start(bf16[192,256]{1,0:T(8,128)(2,1)} %expert_last.1.refs_0_), channel_id=1, source_target_pairs={{0,2},{1,3},{2,0},{3,1},{4,6},{5,7},{6,4},{7,5},{8,10},{9,11},{10,... | collective-permute-start | bytes 294920 | tf_op jit(solution)/shard_map/ppermute | solution.py:26
  167.3 4.8 %copy-start.8 = (bf16[256,1024]{1,0:T(8,128)(2,1)}, bf16[256,1024]{1,0:T(8,128)(2,1)S(1)}, u32[]{:S(2)}) copy-start(bf16[256,1024]{1,0:T(8,128)(2,1)S(1)} %collective-permute-done.21.refs_5_) | copy-start | bytes 1572868
  167.3 4.8 %collective-permute-start.20 = (bf16[192,256]{1,0:T(8,128)(2,1)}, bf16[192,256]{1,0:T(8,128)(2,1)S(1)}, u32[]{:S(2)}, u32[]{:S(2)}) collective-permute-start(bf16[192,256]{1,0:T(8,128)(2,1)} %expert_last.1.refs_0_), channel_id=1, source_target_pairs={{0,3},{1,0},{2,1},{3,2},{4,7},{5,4},{6,5},{7,6},{8,11},{9,8},{10,9... | collective-permute-start | bytes 294920 | tf_op jit(solution)/shard_map/ppermute | solution.py:26
  167.4 4.7 %copy-start.9 = (bf16[256,1024]{1,0:T(8,128)(2,1)}, bf16[256,1024]{1,0:T(8,128)(2,1)S(1)}, u32[]{:S(2)}) copy-start(bf16[256,1024]{1,0:T(8,128)(2,1)S(1)} %collective-permute-done.22.refs_6_) | copy-start | bytes 1572868
  167.4 4.7 %copy-start.10 = (bf16[256,1024]{1,0:T(8,128)(2,1)}, bf16[256,1024]{1,0:T(8,128)(2,1)S(1)}, u32[]{:S(2)}) copy-start(bf16[256,1024]{1,0:T(8,128)(2,1)S(1)} %collective-permute-done.23.refs_7_) | copy-start | bytes 1572868
  168.3 3.8 %copy-start.22 = (bf16[192,256]{1,0:T(8,128)(2,1)}, bf16[192,256]{1,0:T(8,128)(2,1)S(1)}, u32[]{:S(2)}) copy-start(bf16[192,256]{1,0:T(8,128)(2,1)S(1)} %collective-permute-done.18.refs_1_) | copy-start | bytes 294916
  170.8 1.3 copy-start.23
  172.1 0.6 copy-start.24
  175.8 21.9 %all-to-all-start.3 = ((bf16[64,24,128]{2,1,0:T(8,128)(2,1)}), bf16[64,24,128]{2,1,0:T(8,128)(2,1)S(1)}, u32[]{:S(2)}, u32[]{:S(2)}) async-start(bf16[64,24,128]{2,1,0:T(8,128)(2,1)} %bitcast.24), calls=%async_computation.3 | async-start | bytes 786432 | tf_op jit(solution)/shard_map/all_to_all | solution.py:555
  197.7 0.7 copy-start.3
  200.4 4.4 %collective-permute-start.24 = (bf16[24,1024]{1,0:T(8,128)(2,1)}, bf16[24,1024]{1,0:T(8,128)(2,1)S(1)}, u32[]{:S(2)}, u32[]{:S(2)}) collective-permute-start(bf16[24,1024]{1,0:T(8,128)(2,1)} %combine.1.refs_0_), channel_id=1, source_target_pairs={{0,1},{1,2},{2,3},{3,0},{4,5},{5,6},{6,7},{7,4},{8,9},{9,10},{10,1... | collective-permute-start | bytes 147464 | tf_op jit(solution)/shard_map/ppermute | solution.py:26
  200.4 5.3 %collective-permute-start.25 = (bf16[24,1024]{1,0:T(8,128)(2,1)}, bf16[24,1024]{1,0:T(8,128)(2,1)S(1)}, u32[]{:S(2)}, u32[]{:S(2)}) collective-permute-start(bf16[24,1024]{1,0:T(8,128)(2,1)} %combine.1.refs_0_), channel_id=1, source_target_pairs={{0,2},{1,3},{2,0},{3,1},{4,6},{5,7},{6,4},{7,5},{8,10},{9,11},{10,... | collective-permute-start | bytes 147464 | tf_op jit(solution)/shard_map/ppermute | solution.py:26
  203.1 3.6 %collective-permute-start.26 = (bf16[24,1024]{1,0:T(8,128)(2,1)}, bf16[24,1024]{1,0:T(8,128)(2,1)S(1)}, u32[]{:S(2)}, u32[]{:S(2)}) collective-permute-start(bf16[24,1024]{1,0:T(8,128)(2,1)} %combine.1.refs_0_), channel_id=1, source_target_pairs={{0,3},{1,0},{2,1},{3,2},{4,7},{5,4},{6,5},{7,6},{8,11},{9,8},{10,9... | collective-permute-start | bytes 147464 | tf_op jit(solution)/shard_map/ppermute | solution.py:26
  204.7 2.0 copy-start.25
  205.6 1.1 copy-start.26
  206.7 0.6 copy-start.27

commit v2 on v1

--- a/solution.py
+++ b/solution.py
@@ -26,24 +26,44 @@
     return lax.ppermute(value, axis, [(i, (i + by) % n) for i in range(n)])
 
 
+def order_of(n):
+    return sorted(range(1, n), key=lambda s: (-min(s, n - s), s))
+
+
 VMEM = pl.BlockSpec(memory_space=pltpu.VMEM)
 SMEM = pl.BlockSpec(memory_space=pltpu.SMEM)
 ANY = pl.BlockSpec(memory_space=pl.ANY)
+HBM = pl.BlockSpec(memory_space=pltpu.MemorySpace.HBM)
 
 
 def shaped(shape, dtype):
     return jax.ShapeDtypeStruct(shape, dtype)
 
 
+def room(mib):
+    return pltpu.CompilerParams(vmem_limit_bytes=mib << 20)
+
+
 def cost(flops, moved):
     return pl.CostEstimate(flops=int(flops), bytes_accessed=int(moved), transcendentals=0)
 
 
+def run(copies):
+    for copy in copies:
+        copy.start()
+    for copy in copies:
+        copy.wait()
+
+
 def pack_kernel(*refs):
-    out, at = refs[-1], 0
-    for ref in refs[:-1]:
-        out[:, at : at + ref.shape[1]] = ref[...]
-        at += ref.shape[1]
+    count = len(refs) - 2
+    out, sems = refs[count:]
+    copies, at = [], 0
+    for i, ref in enumerate(refs[:count]):
+        cols = ref.shape[1]
+        copies.append(pltpu.make_async_copy(ref, out.at[:, at : at + cols], sems.at[i]))
+        at += cols
+    run(copies)
 
 
 def pack(arrays):
@@ -52,12 +72,24 @@
     return pl.pallas_call(
         pack_kernel,
         out_shape=shaped((rows, cols), arrays[0].dtype),
+        in_specs=[HBM] * len(arrays),
+        out_specs=VMEM,
+        scratch_shapes=[pltpu.SemaphoreType.DMA((len(arrays),))],
         cost_estimate=cost(1e6, 4 * rows * cols),
+        compiler_params=room(62),
         name="pack",
     )(*arrays)
 
 
-def scale_kernel(tokens, gain, weight, out, scale):
+def scale_kernel(tokens_at, gain_at, weight_at, out, scale, tokens, gain, weight, sems):
+    run(
+        [
+            pltpu.make_async_copy(ref, to, sems.at[i])
+            for i, (ref, to) in enumerate(
+                ((tokens_at, tokens), (gain_at, gain), (weight_at, weight))
+            )
+        ]
+    )
     values = tokens[...].astype(f32)
     seqs = values.shape[0]
     meansq = jnp.mean(values * values, axis=-1, keepdims=True)
@@ -77,19 +109,37 @@
             shaped((nz, seqs + weight.shape[0], width // nz), bf16),
             shaped((seqs, 128), f32),
         ],
+        in_specs=[HBM] * 3,
+        out_specs=[VMEM] * 2,
+        scratch_shapes=[
+            pltpu.VMEM(tokens.shape, bf16),
+            pltpu.VMEM(gain.shape, bf16),
+            pltpu.VMEM(weight.shape, bf16),
+            pltpu.SemaphoreType.DMA((3,)),
+        ],
         cost_estimate=cost(1e6, 4 * seqs * width),
+        compiler_params=room(62),
         name="scale",
     )(tokens, gain, weight)
 
 
-def split_kernel(nz, where, down, *outs):
+def split_kernel(nz, where, down, *refs):
+    outs, sems = refs[:-1], refs[-1]
     nt = len(outs)
     chunk = outs[0].shape[1] // nz
+    copies = []
     for s in range(nt):
         other = lax.rem(where[3] + s, nt)
         for i in range(nz):
             at = pl.multiple_of((i * nt + other) * chunk, chunk)
-            outs[s][:, i * chunk : (i + 1) * chunk] = down[:, pl.ds(at, chunk)]
+            copies.append(
+                pltpu.make_async_copy(
+                    down.at[:, pl.ds(at, chunk)],
+                    outs[s].at[:, pl.ds(i * chunk, chunk)],
+                    sems.at[s, i],
+                )
+            )
+    run(copies)
 
 
 def split(where, down, nz, nt):
@@ -97,9 +147,11 @@
     return pl.pallas_call(
         functools.partial(split_kernel, nz),
         out_shape=[shaped((rows, cols // nt), bf16)] * nt,
-        in_specs=[SMEM, VMEM],
+        in_specs=[SMEM, HBM],
         out_specs=[VMEM] * nt,
+        scratch_shapes=[pltpu.SemaphoreType.DMA((nt, nz))],
         cost_estimate=cost(1e6, 4 * rows * cols),
+        compiler_params=room(6),
         name="split",
     )(where, down)
 
@@ -129,13 +181,23 @@
         out_specs=VMEM,
         scratch_shapes=[pltpu.VMEM((depth, cols), bf16)],
         cost_estimate=cost(2 * nz * seqs * depth * cols, 2 * depth * cols),
+        compiler_params=room(10),
         name="project",
     )(where, tok, *own, *other)
 
 
-def attend_kernel(heads, arrived, scale, shift_of, state, gain, out):
+def attend_kernel(step, arrived, scale, shift_of, state_at, gain, out, state, sems):
+    seqs, heads = state.shape[:2]
+    copies = [
+        pltpu.make_async_copy(
+            state_at.at[pl.ds(i * step, step)], state.at[pl.ds(i * step, step)], sems.at[i]
+        )
+        for i in range(seqs // step)
+    ]
+    for copy in copies:
+        copy.start()
     total = jnp.sum(arrived[...].astype(f32), axis=0) * scale[:, :1]
-    rows = total.shape[0]
+    rows = step
     keys = shift_of.shape[1]
     vals = out.shape[1]
     dim, width = keys // heads, vals // heads
@@ -148,15 +210,19 @@
     faded = query * jnp.exp(log_sig / tau + shift_of[...])
     product = query * key
     silu = rgate * jax.nn.sigmoid(rgate)
+    turned = [jnp.transpose(faded[:, h * dim : (h + 1) * dim]) for h in range(heads)]
+    reads = [[] for _ in range(heads)]
+    for i in range(seqs // rows):
+        copies[i].wait()
+        for s in range(i * rows, (i + 1) * rows):
+            for h in range(heads):
+                reads[h].append(
+                    jnp.sum(turned[h][:, s : s + 1] * state[s, h], axis=0, keepdims=True)
+                )
     for h in range(heads):
         at = slice(h * dim, (h + 1) * dim)
-        turned = jnp.transpose(faded[:, at])
-        reads = [
-            jnp.sum(turned[:, s : s + 1] * state[s, h], axis=0, keepdims=True)
-            for s in range(rows)
-        ]
         cols = slice(h * width, (h + 1) * width)
-        read = jnp.concatenate(reads, axis=0)
+        read = jnp.concatenate(reads[h], axis=0)
         read = read + jnp.sum(product[:, at], axis=-1, keepdims=True) * value[:, cols]
         meansq = jnp.mean(read * read, axis=-1, keepdims=True)
         out[:, cols] = (
@@ -168,22 +234,20 @@
 
 
 def attend(arrived, scale, decay_shift, state, head_gain):
-    seqs, heads, dim, width = state.shape
+    seqs, heads, _, width = state.shape
     step = 8
     vals = heads * width
     return pl.pallas_call(
-        functools.partial(attend_kernel, heads),
-        grid=(seqs // step,),
+        functools.partial(attend_kernel, step),
         out_shape=shaped((seqs, vals), bf16),
-        in_specs=[
-            pl.BlockSpec((arrived.shape[0], step, arrived.shape[2]), lambda i: (0, i, 0)),
-            pl.BlockSpec((step, scale.shape[1]), lambda i: (i, 0)),
-            pl.BlockSpec((step, heads * dim), lambda i: (i, 0)),
-            pl.BlockSpec((step, heads, dim, width), lambda i: (i, 0, 0, 0)),
-            pl.BlockSpec((vals,), lambda i: (0,)),
+        in_specs=[VMEM, VMEM, VMEM, HBM, VMEM],
+        out_specs=VMEM,
+        scratch_shapes=[
+            pltpu.VMEM(state.shape, f32),
+            pltpu.SemaphoreType.DMA((seqs // step,)),
         ],
-        out_specs=pl.BlockSpec((step, vals), lambda i: (i, 0)),
         cost_estimate=cost(4 * state.size, 4 * state.size),
+        compiler_params=room(52),
         name="attend",
     )(arrived, scale, decay_shift, state, head_gain)
 
@@ -226,6 +290,7 @@
             pltpu.SemaphoreType.DMA((nx,)),
         ],
         cost_estimate=cost(2 * seqs * cols * nx * depth, 2 * cols * nx * depth),
+        compiler_params=room(8),
         name="mix",
     )(where, gated, partner, *blocks)
 
@@ -265,6 +330,7 @@
         out_specs=[VMEM] * 2,
         scratch_shapes=[pltpu.VMEM((wide, 128), f32)],
         cost_estimate=cost(2 * slots * seqs * part, 6 * slots * part),
+        compiler_params=room(6),
         name="dispatch",
     )(where, tokens, gain, sender, mine, other)
 
@@ -277,117 +343,83 @@
     )
 
 
-def pick_kernel(step, nt, where, w_gate, w_lin, gate, lin, sems):
-    at = lax.rem(where[3] - step + nt, nt)
-    copies = (
-        pltpu.make_async_copy(w_gate.at[:, at], gate, sems.at[0]),
-        pltpu.make_async_copy(w_lin.at[:, at], lin, sems.at[1]),
-    )
-    for copy in copies:
-        copy.start()
+def pick_kernel(nt, where, w_gate, w_lin, *refs):
+    outs, sems = refs[:nt], refs[nt]
+    units = w_gate.shape[-1]
+    copies = []
+    for s in range(nt):
+        at = lax.rem(where[3] - s + nt, nt)
+        for k, ref in enumerate((w_gate, w_lin)):
+            copy = pltpu.make_async_copy(
+                ref.at[:, at], outs[s].at[:, :, pl.ds(k * units, units)], sems.at[s, k]
+            )
+            copy.start()
+            copies.append(copy)
     for copy in copies:
         copy.wait()
 
 
-def pick(where, w_gate, w_lin, step):
+def pick(where, w_gate, w_lin):
     nz, nt, chunk, units = w_gate.shape
     return pl.pallas_call(
-        functools.partial(pick_kernel, step, nt),
-        out_shape=[shaped((nz, chunk, units), bf16)] * 2,
-        in_specs=[SMEM, ANY, ANY],
-        out_specs=[VMEM, VMEM],
-        scratch_shapes=[pltpu.SemaphoreType.DMA((2,))],
-        cost_estimate=cost(1e6, 8 * nz * chunk * units),
+        functools.partial(pick_kernel, nt),
+        out_shape=[shaped((nz, chunk, 2 * units), bf16)] * nt,
+        in_specs=[SMEM, HBM, HBM],
+        out_specs=[VMEM] * nt,
+        scratch_shapes=[pltpu.SemaphoreType.DMA((nt, 2))],
+        cost_estimate=cost(1e6, 4 * w_gate.size),
+        compiler_params=room(8),
         name="pick",
     )(where, w_gate, w_lin)
 
 
-def expert_first_kernel(steps, nt, slots, where, inverse, w_gate, w_lin, *refs):
-    count = len(steps)
-    pieces, refs = refs[:count], refs[count:]
-    outs, (gates, lins, wide, sems) = refs[:3], refs[3:]
-    t = where[3]
-    copies = []
-    for i, s in enumerate(steps):
-        at = lax.rem(t - s + nt, nt)
-        pair = (
-            pltpu.make_async_copy(w_gate.at[:, at], gates.at[i], sems.at[i, 0]),
-            pltpu.make_async_copy(w_lin.at[:, at], lins.at[i], sems.at[i, 1]),
-        )
-        for copy in pair:
-            copy.start()
-        copies.append(pair)
-    gate, lin, sumsq = 0.0, 0.0, 0.0
-    units = w_gate.shape[-1]
-    for i, s in enumerate(steps):
-        at = lax.rem(t - s + nt, nt)
-        rows = take_rows(pieces[i], wide, slots)
-        plain = rows * inverse[at]
-        sumsq = sumsq + jnp.sum(plain * plain, axis=-1, keepdims=True)
-        rows = rows.astype(bf16)
-        copies[i][0].wait()
-        gate = gate + jnp.dot(
-            rows, gates[i].reshape(-1, units), preferred_element_type=f32
-        )
-        copies[i][1].wait()
-        lin = lin + jnp.dot(rows, lins[i].reshape(-1, units), preferred_element_type=f32)
-    outs[0][...] = gate
-    outs[1][...] = lin
-    outs[2][...] = jnp.broadcast_to(sumsq, outs[2].shape)
-
-
-def expert_first(where, inverse, w_gate, w_lin, steps, pieces, slots):
-    nz, nt, chunk, units = w_gate.shape
-    count = len(steps)
-    part = nz * chunk
-    return pl.pallas_call(
-        functools.partial(expert_first_kernel, steps, nt, slots),
-        out_shape=[shaped((slots, units), f32)] * 2 + [shaped((slots, 128), f32)],
-        in_specs=[SMEM, VMEM, ANY, ANY] + [VMEM] * count,
-        out_specs=[VMEM] * 3,
-        scratch_shapes=[
-            pltpu.VMEM((count, nz, chunk, units), bf16),
-            pltpu.VMEM((count, nz, chunk, units), bf16),
-            pltpu.VMEM(pieces[0].shape, f32),
-            pltpu.SemaphoreType.DMA((count, 2)),
-        ],
-        cost_estimate=cost(4 * count * slots * part * units, 4 * count * part * units),
-        name="expert_first",
-    )(where, inverse, w_gate, w_lin, *pieces)
-
-
-def expert_last_kernel(step, nt, where, inverse, w_gate, w_lin, piece, *refs):
-    gate, lin, sumsq, out, wide = refs
-    slots, units = out.shape
+def expert_kernel(step, nt, first, last, where, inverse, weight, piece, *refs):
+    if not first:
+        before, refs = refs[:2], refs[2:]
+    outs, wide = refs[:-1], refs[-1]
+    slots = outs[0].shape[0]
     rows = take_rows(piece, wide, slots)
     plain = rows * inverse[lax.rem(where[3] - step + nt, nt)]
-    meansq = (sumsq[:, :1] + jnp.sum(plain * plain, axis=-1, keepdims=True)) / (
-        nt * rows.shape[1]
-    )
-    rows = rows.astype(bf16)
-    scale = lax.rsqrt(meansq + eps)
-    gated = gate[...] + jnp.dot(
-        rows, w_gate[...].reshape(-1, units), preferred_element_type=f32
-    )
-    linear = lin[...] + jnp.dot(
-        rows, w_lin[...].reshape(-1, units), preferred_element_type=f32
-    )
-    gated = jnp.minimum(gated * scale, limit)
-    linear = jnp.clip(linear * scale, -limit, limit)
-    out[...] = (gated * jax.nn.sigmoid(glu_alpha * gated) * (linear + 1.0)).astype(bf16)
-
-
-def expert_last(where, inverse, w_gate, w_lin, step, nt, piece, before):
-    slots, units = before[0].shape
-    return pl.pallas_call(
-        functools.partial(expert_last_kernel, step, nt),
-        out_shape=shaped((slots, units), bf16),
-        in_specs=[SMEM] + [VMEM] * 7,
-        out_specs=VMEM,
+    plain = plain * plain
+    part = rows.shape[1]
+    sumsq = plain[:, :128]
+    for j in range(1, part // 128):
+        sumsq = sumsq + plain[:, j * 128 : (j + 1) * 128]
+    total = jnp.dot(
+        rows.astype(bf16), weight[...].reshape(part, -1), preferred_element_type=f32
+    )
+    if not first:
+        total = total + before[0][...]
+        sumsq = sumsq + before[1][...]
+    if not last:
+        outs[0][...] = total
+        outs[1][...] = sumsq
+        return
+    units = outs[0].shape[1]
+    meansq = jnp.sum(sumsq, axis=-1, keepdims=True) / (nt * part)
+    total = total * lax.rsqrt(meansq + eps)
+    gate = jnp.minimum(total[:, :units], limit)
+    lin = jnp.clip(total[:, units:], -limit, limit)
+    outs[0][...] = (gate * jax.nn.sigmoid(glu_alpha * gate) * (lin + 1.0)).astype(bf16)
+
+
+def expert(where, inverse, weight, step, nt, piece, slots, before=(), last=False):
+    units = weight.shape[-1]
+    out_shape = (
+        shaped((slots, units // 2), bf16)
+        if last
+        else [shaped((slots, units), f32), shaped((slots, 128), f32)]
+    )
+    return pl.pallas_call(
+        functools.partial(expert_kernel, step, nt, not before, last),
+        out_shape=out_shape,
+        in_specs=[SMEM] + [VMEM] * (3 + len(before)),
+        out_specs=VMEM if last else [VMEM] * 2,
         scratch_shapes=[pltpu.VMEM(piece.shape, f32)],
-        cost_estimate=cost(4 * slots * w_gate.size, 4 * w_gate.size),
-        name="expert_last",
-    )(where, inverse, w_gate, w_lin, piece, *before)
+        cost_estimate=cost(2 * slots * weight.size, 2 * weight.size),
+        compiler_params=room(8),
+        name="expert",
+    )(where, inverse, weight, piece, *before)
 
 
 def down_kernel(nt, *refs):
@@ -409,6 +441,7 @@
         out_shape=shaped((wide, 128), bf16),
         scratch_shapes=[pltpu.VMEM((wide, 128), f32)],
         cost_estimate=cost(2 * nt * slots * units * part, 2 * nt * units * part),
+        compiler_params=room(10),
         name="down",
     )(*acts, *downs)
 
@@ -432,6 +465,7 @@
         out_shape=shaped(stream.shape, bf16),
         scratch_shapes=[pltpu.VMEM(rows.shape, f32)],
         cost_estimate=cost(2 * weights.size * stream.shape[1], 2 * rows.size),
+        compiler_params=room(4),
         name="combine",
     )(rows, weights, stream)
 
@@ -455,6 +489,7 @@
         in_specs=[SMEM] + [VMEM] * len(pieces),
         out_specs=VMEM,
         cost_estimate=cost(1e6, 4 * seqs * part * len(pieces)),
+        compiler_params=room(2),
         name="finish",
     )(where, *pieces)
 
@@ -543,13 +578,14 @@
     pieces = [rows] + [shift(rows, T, s) for s in range(1, nt)]
     gates = w_gate.reshape(nz, nt, chunk, -1)
     lins = w_lin.reshape(nz, nt, chunk, -1)
-    far = nt // 2
-    picked = pick(where, gates, lins, far)
-    steps = [s for s in range(nt) if s != far]
-    before = expert_first(
-        where, inverse, gates, lins, steps, [pieces[s] for s in steps], slots
-    )
-    act = expert_last(where, inverse, *picked, far, nt, pieces[far], before)
+    picked = pick(where, gates, lins)
+    before = ()
+    steps = [0] + order_of(nt)[1:] + [nt // 2]
+    for s in steps:
+        before = expert(
+            where, inverse, picked[s], s, nt, pieces[s], slots, before, s == steps[-1]
+        )
+    act = before
     acts = [act] + [shift(act, T, s) for s in range(1, nt)]
     done = down_sum(acts, downs)
     returned = lax.all_to_all(

time: 210 us -> 191 us (0.910)
  Pallas kernels: 39.4 us -> 21.8 us
  waiting for transfers between devices: 75 us -> 83.7 us
  local copies, waits for them, and re-layouts: 9.78 us -> 3.09 us
  other arithmetic: 3.71 us -> 0.63 us
    pallas_call x4 -> x6, Pallas kernels: 16.5 us -> 8.21 us  [the longest x4 3.88 us: expert(): pl.pallas_call(functools.partial(expert_kernel, step, nt, not before, las...]
    ppermute x27, waiting for transfers between devices: 41.1 us -> 48.3 us  [shift(): return lax.ppermute(value, axis, [(i, (i + by) % n) for i in range(n)])]
    unnamed x67 -> x23, local copies, waits for them, and re-layouts: 7.09 us -> 2.66 us
    pallas_call x1, Pallas kernels: 3.66 us -> 1.51 us  [split(): pl.pallas_call(functools.partial(split_kernel, nz), out_shape=[shaped((ro...]
  transfers between devices with their start and end apart: 30 -> 30, of which waited for: 18 -> 19; matrix products, arithmetic and copies ran while one was open for 2% -> 1% of each run, Pallas kernels for 10% -> 6%
where the time goes in v2:
time: 191 us; the launch traced here: 190 us
  waiting for transfers between devices  83.7 us (44%)
  starting transfers between devices  58.1 us (30%)
  blocking collectives  22.7 us (12%)
  Pallas kernels  21.8 us (11%)
  local copies, waits for them, and re-layouts  3.09 us (2%)
    ppermute x27, waiting for transfers between devices, shift(): return lax.ppermute(value, axis, [(i, (i + by) % n) for i in range(n)])  48.3 us
    ppermute x27, starting transfers between devices, shift(): return lax.ppermute(value, axis, [(i, (i + by) % n) for i in range(n)])  38.8 us
    all_to_all x1, blocking collectives, on_device(): lax.all_to_all(outbound.reshape(n_ep, -1, 128), EP, 0, 0, tiled=True)  22.7 us
    all_to_all x1, waiting for transfers between devices, on_device(): arrived = lax.all_to_all(parts, Z, 0, 0, tiled=True)  16.6 us
    all_to_all x1, waiting for transfers between devices, on_device(): lax.all_to_all(done.reshape(n_ep, -1, 128), EP, 0, 0, tiled=True)  15.1 us
    all_to_all x1, starting transfers between devices, on_device(): moved = lax.all_to_all(payload, Z, 0, 0, tiled=True)  9.02 us
    all_to_all x1, starting transfers between devices, on_device(): lax.all_to_all(done.reshape(n_ep, -1, 128), EP, 0, 0, tiled=True)  6.61 us
    pallas_call x4, Pallas kernels, expert(): pl.pallas_call(functools.partial(expert_kernel, step, nt, not before, las...  3.88 us
  transfers between devices with their start and end apart: 30, of which 19 were waited for; matrix products, arithmetic and copies ran while one was open for 1% of the time, Pallas kernels for 6%

profile of v2, /device:TPU:1, one launch (start us, length us, event | category | flops | bytes accessed | tf_op | source)
XLA Modules:
  0.0 190.3 jit_solution(11572423074955712494)
XLA Ops:
  0.0 2.0 %scale.1 = (bf16[8,88,512]{2,1,0:T(8,128)(2,1)}, f32[24,128]{1,0:T(8,128)}) custom-call(bf16[24,4096]{1,0:T(8,128)(2,1)} %tokens.1, bf16[4096]{0:T(1024)(128)(2,1)} %gain_at.1, bf16[64,512]{1,0:T(8,128)(2,1)} %bitcast.30), custom_call_target="tpu_custom_call" | custom-call | flops 1000000 | bytes 393216 | tf_op jit(solution)/shard_map/scale/pallas_call | solution.py:106
  2.0 9.0 %all-to-all-start = ((bf16[8,88,512]{2,1,0:T(8,128)(2,1)}), bf16[8,88,512]{2,1,0:T(8,128)(2,1)S(1)}, u32[]{:S(2)}, u32[]{:S(2)}) async-start(bf16[8,88,512]{2,1,0:T(8,128)(2,1)} %get-tuple-element.28), calls=%async_computation | async-start | bytes 1441792 | tf_op jit(solution)/shard_map/all_to_all | solution.py:551
  11.0 1.7 pack.1.refs_0_
  12.6 1.3 collective-permute-start
  13.9 2.5 %collective-permute-start.1 = (bf16[64,1792]{1,0:T(8,128)(2,1)}, bf16[64,1792]{1,0:T(8,128)(2,1)S(1)}, u32[]{:S(2)}, u32[]{:S(2)}) collective-permute-start(bf16[64,1792]{1,0:T(8,128)(2,1)} %pack.1.refs_0_), channel_id=1, source_target_pairs={{0,16},{8,24},{16,0},{24,8},{1,17},{9,25},{17,1},{25,9},{2,18},{10... | collective-permute-start | bytes 688136 | tf_op jit(solution)/shard_map/ppermute | solution.py:26
  16.4 1.2 collective-permute-start.2
  17.5 1.8 collective-permute-start.3
  19.3 1.0 collective-permute-done.refs_1_
  20.4 2.2 %collective-permute-start.4 = (bf16[64,1792]{1,0:T(8,128)(2,1)S(1)}, bf16[64,1792]{1,0:T(8,128)(2,1)S(1)}, u32[]{:S(2)}, u32[]{:S(2)}) collective-permute-start(bf16[64,1792]{1,0:T(8,128)(2,1)S(1)} %collective-permute-done.refs_1_), channel_id=1, source_target_pairs={{0,4},{4,0},{1,5},{5,1},{2,6},{6,2},{3,7},{7,3},{8,12},{12,8},{9,1... | collective-permute-start | bytes 688136 | tf_op jit(solution)/shard_map/ppermute | solution.py:26
  22.6 3.7 %collective-permute-done.1.refs_2_ = bf16[64,1792]{1,0:T(8,128)(2,1)S(1)} collective-permute-done((bf16[64,1792]{1,0:T(8,128)(2,1)}, bf16[64,1792]{1,0:T(8,128)(2,1)S(1)}, u32[]{:S(2)}, u32[]{:S(2)}) %collective-permute-start.1) | collective-permute-done | bytes 229408 | tf_op jit(solution)/shard_map/ppermute | solution.py:26
  26.3 1.8 collective-permute-start.5
  28.2 1.0 collective-permute-done.5.refs_6_
  29.2 0.4 collective-permute-done.6.refs_7_
  29.6 3.6 %all-to-all-done.tok = bf16[8,88,512]{2,1,0:T(8,128)(2,1)S(1)} async-done(((bf16[8,88,512]{2,1,0:T(8,128)(2,1)}), bf16[8,88,512]{2,1,0:T(8,128)(2,1)S(1)}, u32[]{:S(2)}, u32[]{:S(2)}) %all-to-all-start) | async-done | bytes 720928 | tf_op jit(solution)/shard_map/all_to_all | solution.py:551
  33.2 0.9 copy-done.3
  34.1 2.0 %project.1 = bf16[8,24,1792]{2,1,0:T(8,128)(2,1)} custom-call(s32[4]{0:T(128)S(1)} %pad_add_fusion.where, bf16[8,88,512]{2,1,0:T(8,128)(2,1)S(1)} %all-to-all-done.tok, bf16[64,1792]{1,0:T(8,128)(2,1)S(1)} %copy-done.3, bf16[64,1792]{1,0:T(8,128)(2,1)S(1)} %collective-permute-done.refs_1_, bf16[64,1792]{1,0:T(8,128)(2,1)S(1)} %collective-permute-done.1.refs_2_, ...), custom_call_target="tpu_custom_call" | custom-call | flops 352321536 | bytes 1835008 | tf_op jit(solution)/shard_map/project/pallas_call | solution.py:177
  36.1 3.7 %all-to-all-start.1 = ((bf16[8,24,1792]{2,1,0:T(8,128)(2,1)}), bf16[8,24,1792]{2,1,0:T(8,128)(2,1)S(1)}, u32[]{:S(2)}, u32[]{:S(2)}) async-start(bf16[8,24,1792]{2,1,0:T(8,128)(2,1)} %project.1), calls=%async_computation.1 | async-start | bytes 1376256 | tf_op jit(solution)/shard_map/all_to_all | solution.py:564
  40.1 2.6 %collective-permute-start.10 = (bf16[8,64,512]{2,1,0:T(8,128)(2,1)S(1)}, bf16[8,64,512]{2,1,0:T(8,128)(2,1)S(1)}, u32[]{:S(2)}, u32[]{:S(2)}) collective-permute-start(bf16[8,64,512]{2,1,0:T(8,128)(2,1)S(1)} %slice.36.refs_0_), channel_id=1, source_target_pairs={{0,24},{8,0},{16,8},{24,16},{1,25},{9,1},{17,9},{25,17},{2,26},{10... | collective-permute-start | bytes 1572872 | tf_op jit(solution)/shard_map/ppermute | solution.py:26
  42.6 1.7 collective-permute-start.9
  44.6 16.6 %all-to-all-done.1.arrived = bf16[8,24,1792]{2,1,0:T(8,128)(2,1)S(1)} async-done(((bf16[8,24,1792]{2,1,0:T(8,128)(2,1)}), bf16[8,24,1792]{2,1,0:T(8,128)(2,1)S(1)}, u32[]{:S(2)}, u32[]{:S(2)}) %all-to-all-start.1) | async-done | bytes 688160 | tf_op jit(solution)/shard_map/all_to_all | solution.py:564
  61.2 3.4 %attend.1.gated = bf16[24,512]{1,0:T(8,128)(2,1)S(1)} custom-call(bf16[8,24,1792]{2,1,0:T(8,128)(2,1)S(1)} %all-to-all-done.1.arrived, f32[24,128]{1,0:T(8,128)S(1)} %copy-done.6, f32[24,256]{1,0:T(8,128)S(1)} %copy-done.5, f32[24,2,128,256]{3,2,1,0:T(8,128)} %state_at.1, bf16[512]{0:T(512)(128)(2,1)S(1)} %copy-done.7), custom_call_target="tpu_custom_call" | custom-call | flops 6291456 | bytes 6291456 | tf_op jit(solution)/shard_map/attend/pallas_call | solution.py:240
  64.7 0.6 collective-permute-start.7
  65.2 0.2 select_reduce_fusion.1
  65.6 1.4 collective-permute-done.9.refs_2_
  67.0 2.6 %mix.1 = (bf16[48,512]{1,0:T(8,128)(2,1)S(1)}, bf16[48,512]{1,0:T(8,128)(2,1)S(1)}, bf16[48,512]{1,0:T(8,128)(2,1)S(1)}, bf16[48,512]{1,0:T(8,128)(2,1)S(1)}) custom-call(s32[4]{0:T(128)S(1)} %pad_add_fusion.where, bf16[24,512]{1,0:T(8,128)(2,1)S(1)} %attend.1.gated, bf16[24,512]{1,0:T(8,128)(2,1)S(1)} %collective-permute-done.7.partner, ...), custom_call_target="tpu_custom_call" | custom-call | flops 100663296 | bytes 2097152 | tf_op jit(solution)/shard_map/mix/pallas_call | solution.py:283
  69.6 1.4 collective-permute-start.11
  70.9 2.6 %collective-permute-start.12 = (bf16[48,512]{1,0:T(8,128)(2,1)S(1)}, bf16[48,512]{1,0:T(8,128)(2,1)S(1)}, u32[]{:S(2)}, u32[]{:S(2)}) collective-permute-start(bf16[48,512]{1,0:T(8,128)(2,1)S(1)} %get-tuple-element.32), channel_id=1, source_target_pairs={{0,2},{1,3},{2,0},{3,1},{4,6},{5,7},{6,4},{7,5},{8,10},{9,11},{10,... | collective-permute-start | bytes 147464 | tf_op jit(solution)/shard_map/ppermute | solution.py:26
  73.6 1.1 collective-permute-start.13
  74.6 0.9 collective-permute-done.12
  75.6 1.2 collective-permute-done.13
  76.8 4.2 %collective-permute-start.14 = (bf16[24,512]{1,0:T(8,128)(2,1)S(1)}, bf16[24,512]{1,0:T(8,128)(2,1)S(1)}, u32[]{:S(2)}, u32[]{:S(2)}) collective-permute-start(bf16[24,512]{1,0:T(8,128)(2,1)S(1)} %get-tuple-element.51), channel_id=1, source_target_pairs={{0,4},{4,0},{1,5},{5,1},{2,6},{6,2},{3,7},{7,3},{8,12},{12,8},{9,1... | collective-permute-start | bytes 73736 | tf_op jit(solution)/shard_map/ppermute | solution.py:26
  81.3 0.6 collective-permute-done.14.other
  81.9 0.9 dispatch.1
  82.8 22.7 %all_to_all.20 = bf16[64,24,128]{2,1,0:T(8,128)(2,1)S(1)} all-to-all(bf16[64,24,128]{2,1,0:T(8,128)(2,1)S(1)} %bitcast.26), channel_id=1, replica_groups=mesh['ep_0'=8,'ep_1'=4,'ep_2'=2,'tp'=4] {'ep_0','ep_1','ep_2'}, dimensions={0} | all-to-all | bytes 786432 | tf_op jit(solution)/shard_map/all_to_all | solution.py:575
  105.5 1.5 split.1
  107.1 1.0 collective-permute-start.21
  108.0 1.9 collective-permute-start.16
  109.9 2.2 %collective-permute-start.22 = (bf16[256,1024]{1,0:T(8,128)(2,1)S(1)}, bf16[256,1024]{1,0:T(8,128)(2,1)S(1)}, u32[]{:S(2)}, u32[]{:S(2)}) collective-permute-start(bf16[256,1024]{1,0:T(8,128)(2,1)S(1)} %get-tuple-element.46), channel_id=1, source_target_pairs={{0,2},{1,3},{2,0},{3,1},{4,6},{5,7},{6,4},{7,5},{8,10},{9,11},{10,... | collective-permute-start | bytes 1572872 | tf_op jit(solution)/shard_map/ppermute | solution.py:26
  112.1 0.6 collective-permute-start.23
  112.7 4.5 %collective-permute-done.17.piece = bf16[1536,128]{1,0:T(8,128)(2,1)S(1)} collective-permute-done((bf16[1536,128]{1,0:T(8,128)(2,1)S(1)}, bf16[1536,128]{1,0:T(8,128)(2,1)S(1)}, u32[]{:S(2)}, u32[]{:S(2)}) %collective-permute-start.17) | collective-permute-done | bytes 393248 | tf_op jit(solution)/shard_map/ppermute | solution.py:26
  117.2 1.6 copy-done.2
  118.8 1.0 pick.1
  119.8 1.0 expert.4
  120.8 1.0 expert.5
  121.8 1.0 expert.6
  122.7 26.1 %collective-permute-done.15.piece = bf16[1536,128]{1,0:T(8,128)(2,1)S(1)} collective-permute-done((bf16[1536,128]{1,0:T(8,128)(2,1)S(1)}, bf16[1536,128]{1,0:T(8,128)(2,1)S(1)}, u32[]{:S(2)}, u32[]{:S(2)}) %collective-permute-start.15) | collective-permute-done | bytes 393248 | tf_op jit(solution)/shard_map/ppermute | solution.py:26
  148.8 1.0 expert.7.refs_0_
  149.8 2.4 %collective-permute-start.18 = (bf16[192,256]{1,0:T(8,128)(2,1)S(1)}, bf16[192,256]{1,0:T(8,128)(2,1)S(1)}, u32[]{:S(2)}, u32[]{:S(2)}) collective-permute-start(bf16[192,256]{1,0:T(8,128)(2,1)S(1)} %expert.7.refs_0_), channel_id=1, source_target_pairs={{0,1},{1,2},{2,3},{3,0},{4,5},{5,6},{6,7},{7,4},{8,9},{9,10},{10,1... | collective-permute-start | bytes 294920 | tf_op jit(solution)/shard_map/ppermute | solution.py:26
  152.3 2.3 %collective-permute-start.19 = (bf16[192,256]{1,0:T(8,128)(2,1)S(1)}, bf16[192,256]{1,0:T(8,128)(2,1)S(1)}, u32[]{:S(2)}, u32[]{:S(2)}) collective-permute-start(bf16[192,256]{1,0:T(8,128)(2,1)S(1)} %expert.7.refs_0_), channel_id=1, source_target_pairs={{0,2},{1,3},{2,0},{3,1},{4,6},{5,7},{6,4},{7,5},{8,10},{9,11},{10,... | collective-permute-start | bytes 294920 | tf_op jit(solution)/shard_map/ppermute | solution.py:26
  154.5 0.2 collective-permute-start.20
  154.8 0.6 collective-permute-done.18.refs_1_
  155.4 2.5 %collective-permute-done.19.refs_2_ = bf16[192,256]{1,0:T(8,128)(2,1)S(1)} collective-permute-done((bf16[192,256]{1,0:T(8,128)(2,1)S(1)}, bf16[192,256]{1,0:T(8,128)(2,1)S(1)}, u32[]{:S(2)}, u32[]{:S(2)}) %collective-permute-start.19) | collective-permute-done | bytes 98336 | tf_op jit(solution)/shard_map/ppermute | solution.py:26
  157.8 1.4 collective-permute-done.20.refs_3_
  159.2 1.4 down.1
  160.6 6.6 %all-to-all-start.3 = ((bf16[64,24,128]{2,1,0:T(8,128)(2,1)}), bf16[64,24,128]{2,1,0:T(8,128)(2,1)S(1)}, u32[]{:S(2)}, u32[]{:S(2)}) async-start(bf16[64,24,128]{2,1,0:T(8,128)(2,1)} %bitcast.14), calls=%async_computation.3 | async-start | bytes 786432 | tf_op jit(solution)/shard_map/all_to_all | solution.py:591
  167.3 15.1 %all-to-all-done.3 = bf16[64,24,128]{2,1,0:T(8,128)(2,1)S(1)} async-done(((bf16[64,24,128]{2,1,0:T(8,128)(2,1)}), bf16[64,24,128]{2,1,0:T(8,128)(2,1)S(1)}, u32[]{:S(2)}, u32[]{:S(2)}) %all-to-all-start.3) | async-done | bytes 393248 | tf_op jit(solution)/shard_map/all_to_all | solution.py:591
  182.4 0.3 combine.1.refs_0_
  182.7 0.2 collective-permute-start.24
  182.9 2.8 %collective-permute-start.25 = (bf16[24,1024]{1,0:T(8,128)(2,1)S(1)}, bf16[24,1024]{1,0:T(8,128)(2,1)S(1)}, u32[]{:S(2)}, u32[]{:S(2)}) collective-permute-start(bf16[24,1024]{1,0:T(8,128)(2,1)S(1)} %combine.1.refs_0_), channel_id=1, source_target_pairs={{0,2},{1,3},{2,0},{3,1},{4,6},{5,7},{6,4},{7,5},{8,10},{9,11},{10,... | collective-permute-start | bytes 147464 | tf_op jit(solution)/shard_map/ppermute | solution.py:26
  185.7 0.4 collective-permute-start.26
  186.1 0.9 collective-permute-done.24.refs_1_
  187.0 1.0 collective-permute-done.25.refs_2_
  188.0 1.1 collective-permute-done.26.refs_3_
  189.1 1.3 finish.1
  (52 shorter events, 1.1 us)
Async XLA Ops:
  2.0 31.2 %all-to-all-start = ((bf16[8,88,512]{2,1,0:T(8,128)(2,1)}), bf16[8,88,512]{2,1,0:T(8,128)(2,1)S(1)}, u32[]{:S(2)}, u32[]{:S(2)}) async-start(bf16[8,88,512]{2,1,0:T(8,128)(2,1)} %get-tuple-element.28), calls=%async_computation | async-start | bytes 1441792 | tf_op jit(solution)/shard_map/all_to_all | solution.py:551
  12.6 7.7 %collective-permute-start = (bf16[64,1792]{1,0:T(8,128)(2,1)}, bf16[64,1792]{1,0:T(8,128)(2,1)S(1)}, u32[]{:S(2)}, u32[]{:S(2)}) collective-permute-start(bf16[64,1792]{1,0:T(8,128)(2,1)} %pack.1.refs_0_), channel_id=1, source_target_pairs={{0,8},{8,16},{16,24},{24,0},{1,9},{9,17},{17,25},{25,1},{2,10},{10... | collective-permute-start | bytes 688136 | tf_op jit(solution)/shard_map/ppermute | solution.py:26
  13.9 12.3 %collective-permute-start.1 = (bf16[64,1792]{1,0:T(8,128)(2,1)}, bf16[64,1792]{1,0:T(8,128)(2,1)S(1)}, u32[]{:S(2)}, u32[]{:S(2)}) collective-permute-start(bf16[64,1792]{1,0:T(8,128)(2,1)} %pack.1.refs_0_), channel_id=1, source_target_pairs={{0,16},{8,24},{16,0},{24,8},{1,17},{9,25},{17,1},{25,9},{2,18},{10... | collective-permute-start | bytes 688136 | tf_op jit(solution)/shard_map/ppermute | solution.py:26
  16.4 11.7 %collective-permute-start.2 = (bf16[64,1792]{1,0:T(8,128)(2,1)}, bf16[64,1792]{1,0:T(8,128)(2,1)S(1)}, u32[]{:S(2)}, u32[]{:S(2)}) collective-permute-start(bf16[64,1792]{1,0:T(8,128)(2,1)} %pack.1.refs_0_), channel_id=1, source_target_pairs={{0,24},{8,0},{16,8},{24,16},{1,25},{9,1},{17,9},{25,17},{2,26},{10... | collective-permute-start | bytes 688136 | tf_op jit(solution)/shard_map/ppermute | solution.py:26
  17.5 10.6 %collective-permute-start.3 = (bf16[64,1792]{1,0:T(8,128)(2,1)}, bf16[64,1792]{1,0:T(8,128)(2,1)S(1)}, u32[]{:S(2)}, u32[]{:S(2)}) collective-permute-start(bf16[64,1792]{1,0:T(8,128)(2,1)} %pack.1.refs_0_), channel_id=1, source_target_pairs={{0,4},{4,0},{1,5},{5,1},{2,6},{6,2},{3,7},{7,3},{8,12},{12,8},{9,1... | collective-permute-start | bytes 688136 | tf_op jit(solution)/shard_map/ppermute | solution.py:26
  20.4 7.8 %collective-permute-start.4 = (bf16[64,1792]{1,0:T(8,128)(2,1)S(1)}, bf16[64,1792]{1,0:T(8,128)(2,1)S(1)}, u32[]{:S(2)}, u32[]{:S(2)}) collective-permute-start(bf16[64,1792]{1,0:T(8,128)(2,1)S(1)} %collective-permute-done.refs_1_), channel_id=1, source_target_pairs={{0,4},{4,0},{1,5},{5,1},{2,6},{6,2},{3,7},{7,3},{8,12},{12,8},{9,1... | collective-permute-start | bytes 688136 | tf_op jit(solution)/shard_map/ppermute | solution.py:26
  26.3 2.9 %collective-permute-start.5 = (bf16[64,1792]{1,0:T(8,128)(2,1)S(1)}, bf16[64,1792]{1,0:T(8,128)(2,1)S(1)}, u32[]{:S(2)}, u32[]{:S(2)}) collective-permute-start(bf16[64,1792]{1,0:T(8,128)(2,1)S(1)} %collective-permute-done.1.refs_2_), channel_id=1, source_target_pairs={{0,4},{4,0},{1,5},{5,1},{2,6},{6,2},{3,7},{7,3},{8,12},{12,8},{9,1... | collective-permute-start | bytes 688136 | tf_op jit(solution)/shard_map/ppermute | solution.py:26
  28.1 1.5 collective-permute-start.6
  28.1 11.8 %copy-start.9 = (s32[24,4]{0,1:T(4,128)S(1)}, s32[24,4]{0,1:T(4,128)}, u32[]{:S(2)}) copy-start(s32[24,4]{0,1:T(4,128)} %param.32) | copy-start | bytes 1156
  33.1 0.9 copy-start.3
  36.1 8.5 %copy-start.8 = (bf16[4096]{0:T(1024)(128)(2,1)S(1)}, bf16[4096]{0:T(1024)(128)(2,1)}, u32[]{:S(2)}) copy-start(bf16[4096]{0:T(1024)(128)(2,1)} %param.28) | copy-start | bytes 24580
  36.1 25.1 %copy-start.5 = (f32[24,256]{1,0:T(8,128)S(1)}, f32[24,256]{1,0:T(8,128)}, u32[]{:S(2)}) copy-start(f32[24,256]{1,0:T(8,128)} %shift_of.1) | copy-start | bytes 73732
  36.1 25.1 %copy-start.6 = (f32[24,128]{1,0:T(8,128)S(1)}, f32[24,128]{1,0:T(8,128)}, u32[]{:S(2)}) copy-start(f32[24,128]{1,0:T(8,128)} %get-tuple-element.29.scale) | copy-start | bytes 36868
  36.1 25.1 %copy-start.7 = (bf16[512]{0:T(512)(128)(2,1)S(1)}, bf16[512]{0:T(512)(128)(2,1)}, u32[]{:S(2)}) copy-start(bf16[512]{0:T(512)(128)(2,1)} %gain.1) | copy-start | bytes 3076
  36.1 25.1 %all-to-all-start.1 = ((bf16[8,24,1792]{2,1,0:T(8,128)(2,1)}), bf16[8,24,1792]{2,1,0:T(8,128)(2,1)S(1)}, u32[]{:S(2)}, u32[]{:S(2)}) async-start(bf16[8,24,1792]{2,1,0:T(8,128)(2,1)} %project.1), calls=%async_computation.1 | async-start | bytes 1376256 | tf_op jit(solution)/shard_map/all_to_all | solution.py:564
  40.1 25.5 %collective-permute-start.10 = (bf16[8,64,512]{2,1,0:T(8,128)(2,1)S(1)}, bf16[8,64,512]{2,1,0:T(8,128)(2,1)S(1)}, u32[]{:S(2)}, u32[]{:S(2)}) collective-permute-start(bf16[8,64,512]{2,1,0:T(8,128)(2,1)S(1)} %slice.36.refs_0_), channel_id=1, source_target_pairs={{0,24},{8,0},{16,8},{24,16},{1,25},{9,1},{17,9},{25,17},{2,26},{10... | collective-permute-start | bytes 1572872 | tf_op jit(solution)/shard_map/ppermute | solution.py:26
  42.6 22.9 %collective-permute-start.8 = (bf16[8,64,512]{2,1,0:T(8,128)(2,1)S(1)}, bf16[8,64,512]{2,1,0:T(8,128)(2,1)}, u32[]{:S(2)}, u32[]{:S(2)}) collective-permute-start(bf16[8,64,512]{2,1,0:T(8,128)(2,1)S(1)} %slice.36.refs_0_), channel_id=1, source_target_pairs={{0,8},{8,16},{16,24},{24,0},{1,9},{9,17},{17,25},{25,1},{2,10},{10... | collective-permute-start | bytes 1572872 | tf_op jit(solution)/shard_map/ppermute | solution.py:26
  42.6 24.4 %collective-permute-start.9 = (bf16[8,64,512]{2,1,0:T(8,128)(2,1)S(1)}, bf16[8,64,512]{2,1,0:T(8,128)(2,1)}, u32[]{:S(2)}, u32[]{:S(2)}) collective-permute-start(bf16[8,64,512]{2,1,0:T(8,128)(2,1)S(1)} %slice.36.refs_0_), channel_id=1, source_target_pairs={{0,16},{8,24},{16,0},{24,8},{1,17},{9,25},{17,1},{25,9},{2,18},{10... | collective-permute-start | bytes 1572872 | tf_op jit(solution)/shard_map/ppermute | solution.py:26
  64.6 16.4 %copy-start.10 = (f32[24,4]{0,1:T(4,128)S(1)}, f32[24,4]{0,1:T(4,128)}, u32[]{:S(2)}) copy-start(f32[24,4]{0,1:T(4,128)} %param.33) | copy-start | bytes 1156
  64.6 17.3 %copy-start.4 = (bf16[24,4096]{1,0:T(8,128)(2,1)S(1)}, bf16[24,4096]{1,0:T(8,128)(2,1)}, u32[]{:S(2)}) copy-start(bf16[24,4096]{1,0:T(8,128)(2,1)} %tokens.1) | copy-start | bytes 589828
  64.6 40.9 %copy-start = (bf16[1,256,4096]{2,1,0:T(8,128)(2,1)S(1)}, bf16[1,256,4096]{2,1,0:T(8,128)(2,1)}, u32[]{:S(2)}) copy-start(bf16[1,256,4096]{2,1,0:T(8,128)(2,1)} %param.31) | copy-start | bytes 6291460
  64.7 2.4 %collective-permute-start.7 = (bf16[24,512]{1,0:T(8,128)(2,1)S(1)}, bf16[24,512]{1,0:T(8,128)(2,1)S(1)}, u32[]{:S(2)}, u32[]{:S(2)}) collective-permute-start(bf16[24,512]{1,0:T(8,128)(2,1)S(1)} %attend.1.gated), channel_id=1, source_target_pairs={{0,4},{4,0},{1,5},{5,1},{2,6},{6,2},{3,7},{7,3},{8,12},{12,8},{9,1... | collective-permute-start | bytes 73736 | tf_op jit(solution)/shard_map/ppermute | solution.py:26
  69.6 5.1 %collective-permute-start.11 = (bf16[48,512]{1,0:T(8,128)(2,1)S(1)}, bf16[48,512]{1,0:T(8,128)(2,1)S(1)}, u32[]{:S(2)}, u32[]{:S(2)}) collective-permute-start(bf16[48,512]{1,0:T(8,128)(2,1)S(1)} %get-tuple-element.31), channel_id=1, source_target_pairs={{0,1},{1,2},{2,3},{3,0},{4,5},{5,6},{6,7},{7,4},{8,9},{9,10},{10,1... | collective-permute-start | bytes 147464 | tf_op jit(solution)/shard_map/ppermute | solution.py:26
  70.9 4.6 %collective-permute-start.12 = (bf16[48,512]{1,0:T(8,128)(2,1)S(1)}, bf16[48,512]{1,0:T(8,128)(2,1)S(1)}, u32[]{:S(2)}, u32[]{:S(2)}) collective-permute-start(bf16[48,512]{1,0:T(8,128)(2,1)S(1)} %get-tuple-element.32), channel_id=1, source_target_pairs={{0,2},{1,3},{2,0},{3,1},{4,6},{5,7},{6,4},{7,5},{8,10},{9,11},{10,... | collective-permute-start | bytes 147464 | tf_op jit(solution)/shard_map/ppermute | solution.py:26
  73.6 3.2 %collective-permute-start.13 = (bf16[48,512]{1,0:T(8,128)(2,1)S(1)}, bf16[48,512]{1,0:T(8,128)(2,1)S(1)}, u32[]{:S(2)}, u32[]{:S(2)}) collective-permute-start(bf16[48,512]{1,0:T(8,128)(2,1)S(1)} %get-tuple-element.33), channel_id=1, source_target_pairs={{0,3},{1,0},{2,1},{3,2},{4,7},{5,4},{6,5},{7,6},{8,11},{9,8},{10,9... | collective-permute-start | bytes 147464 | tf_op jit(solution)/shard_map/ppermute | solution.py:26
  76.8 5.1 %collective-permute-start.14 = (bf16[24,512]{1,0:T(8,128)(2,1)S(1)}, bf16[24,512]{1,0:T(8,128)(2,1)S(1)}, u32[]{:S(2)}, u32[]{:S(2)}) collective-permute-start(bf16[24,512]{1,0:T(8,128)(2,1)S(1)} %get-tuple-element.51), channel_id=1, source_target_pairs={{0,4},{4,0},{1,5},{5,1},{2,6},{6,2},{3,7},{7,3},{8,12},{12,8},{9,1... | collective-permute-start | bytes 73736 | tf_op jit(solution)/shard_map/ppermute | solution.py:26
  81.3 35.9 %copy-start.1 = (bf16[1,4096,256]{2,1,0:T(8,128)(2,1)S(1)}, bf16[1,4096,256]{2,1,0:T(8,128)(2,1)}, u32[]{:S(2)}) copy-start(bf16[1,4096,256]{2,1,0:T(8,128)(2,1)} %param.29) | copy-start | bytes 6291460
  105.5 11.6 %collective-permute-start.17 = (bf16[1536,128]{1,0:T(8,128)(2,1)S(1)}, bf16[1536,128]{1,0:T(8,128)(2,1)S(1)}, u32[]{:S(2)}, u32[]{:S(2)}) collective-permute-start(bf16[1536,128]{1,0:T(8,128)(2,1)S(1)} %bitcast.22), channel_id=1, source_target_pairs={{0,1},{1,2},{2,3},{3,0},{4,5},{5,6},{6,7},{7,4},{8,9},{9,10},{10,1... | collective-permute-start | bytes 1179656 | tf_op jit(solution)/shard_map/ppermute | solution.py:26
  107.1 47.5 %collective-permute-start.21 = (bf16[256,1024]{1,0:T(8,128)(2,1)S(1)}, bf16[256,1024]{1,0:T(8,128)(2,1)S(1)}, u32[]{:S(2)}, u32[]{:S(2)}) collective-permute-start(bf16[256,1024]{1,0:T(8,128)(2,1)S(1)} %get-tuple-element.45), channel_id=1, source_target_pairs={{0,1},{1,2},{2,3},{3,0},{4,5},{5,6},{6,7},{7,4},{8,9},{9,10},{10,1... | collective-permute-start | bytes 1572872 | tf_op jit(solution)/shard_map/ppermute | solution.py:26
  108.0 13.7 %collective-permute-start.16 = (bf16[1536,128]{1,0:T(8,128)(2,1)S(1)}, bf16[1536,128]{1,0:T(8,128)(2,1)S(1)}, u32[]{:S(2)}, u32[]{:S(2)}) collective-permute-start(bf16[1536,128]{1,0:T(8,128)(2,1)S(1)} %bitcast.23), channel_id=1, source_target_pairs={{0,3},{1,0},{2,1},{3,2},{4,7},{5,4},{6,5},{7,6},{8,11},{9,8},{10,9... | collective-permute-start | bytes 1179656 | tf_op jit(solution)/shard_map/ppermute | solution.py:26
  109.9 44.9 %collective-permute-start.22 = (bf16[256,1024]{1,0:T(8,128)(2,1)S(1)}, bf16[256,1024]{1,0:T(8,128)(2,1)S(1)}, u32[]{:S(2)}, u32[]{:S(2)}) collective-permute-start(bf16[256,1024]{1,0:T(8,128)(2,1)S(1)} %get-tuple-element.46), channel_id=1, source_target_pairs={{0,2},{1,3},{2,0},{3,1},{4,6},{5,7},{6,4},{7,5},{8,10},{9,11},{10,... | collective-permute-start | bytes 1572872 | tf_op jit(solution)/shard_map/ppermute | solution.py:26
  112.1 42.7 %collective-permute-start.23 = (bf16[256,1024]{1,0:T(8,128)(2,1)S(1)}, bf16[256,1024]{1,0:T(8,128)(2,1)S(1)}, u32[]{:S(2)}, u32[]{:S(2)}) collective-permute-start(bf16[256,1024]{1,0:T(8,128)(2,1)S(1)} %get-tuple-element.47), channel_id=1, source_target_pairs={{0,3},{1,0},{2,1},{3,2},{4,7},{5,4},{6,5},{7,6},{8,11},{9,8},{10,9... | collective-permute-start | bytes 1572872 | tf_op jit(solution)/shard_map/ppermute | solution.py:26
  117.2 31.7 %collective-permute-start.15 = (bf16[1536,128]{1,0:T(8,128)(2,1)S(1)}, bf16[1536,128]{1,0:T(8,128)(2,1)S(1)}, u32[]{:S(2)}, u32[]{:S(2)}) collective-permute-start(bf16[1536,128]{1,0:T(8,128)(2,1)S(1)} %bitcast.24), channel_id=1, source_target_pairs={{0,2},{1,3},{2,0},{3,1},{4,6},{5,7},{6,4},{7,5},{8,10},{9,11},{10,... | collective-permute-start | bytes 1179656 | tf_op jit(solution)/shard_map/ppermute | solution.py:26
  117.2 1.6 copy-start.2
  149.8 5.5 %collective-permute-start.18 = (bf16[192,256]{1,0:T(8,128)(2,1)S(1)}, bf16[192,256]{1,0:T(8,128)(2,1)S(1)}, u32[]{:S(2)}, u32[]{:S(2)}) collective-permute-start(bf16[192,256]{1,0:T(8,128)(2,1)S(1)} %expert.7.refs_0_), channel_id=1, source_target_pairs={{0,1},{1,2},{2,3},{3,0},{4,5},{5,6},{6,7},{7,4},{8,9},{9,10},{10,1... | collective-permute-start | bytes 294920 | tf_op jit(solution)/shard_map/ppermute | solution.py:26
  152.3 5.6 %collective-permute-start.19 = (bf16[192,256]{1,0:T(8,128)(2,1)S(1)}, bf16[192,256]{1,0:T(8,128)(2,1)S(1)}, u32[]{:S(2)}, u32[]{:S(2)}) collective-permute-start(bf16[192,256]{1,0:T(8,128)(2,1)S(1)} %expert.7.refs_0_), channel_id=1, source_target_pairs={{0,2},{1,3},{2,0},{3,1},{4,6},{5,7},{6,4},{7,5},{8,10},{9,11},{10,... | collective-permute-start | bytes 294920 | tf_op jit(solution)/shard_map/ppermute | solution.py:26
  154.5 4.7 %collective-permute-start.20 = (bf16[192,256]{1,0:T(8,128)(2,1)S(1)}, bf16[192,256]{1,0:T(8,128)(2,1)S(1)}, u32[]{:S(2)}, u32[]{:S(2)}) collective-permute-start(bf16[192,256]{1,0:T(8,128)(2,1)S(1)} %expert.7.refs_0_), channel_id=1, source_target_pairs={{0,3},{1,0},{2,1},{3,2},{4,7},{5,4},{6,5},{7,6},{8,11},{9,8},{10,9... | collective-permute-start | bytes 294920 | tf_op jit(solution)/shard_map/ppermute | solution.py:26
  160.6 21.8 %all-to-all-start.3 = ((bf16[64,24,128]{2,1,0:T(8,128)(2,1)}), bf16[64,24,128]{2,1,0:T(8,128)(2,1)S(1)}, u32[]{:S(2)}, u32[]{:S(2)}) async-start(bf16[64,24,128]{2,1,0:T(8,128)(2,1)} %bitcast.14), calls=%async_computation.3 | async-start | bytes 786432 | tf_op jit(solution)/shard_map/all_to_all | solution.py:591
  182.7 4.2 %collective-permute-start.24 = (bf16[24,1024]{1,0:T(8,128)(2,1)S(1)}, bf16[24,1024]{1,0:T(8,128)(2,1)S(1)}, u32[]{:S(2)}, u32[]{:S(2)}) collective-permute-start(bf16[24,1024]{1,0:T(8,128)(2,1)S(1)} %combine.1.refs_0_), channel_id=1, source_target_pairs={{0,1},{1,2},{2,3},{3,0},{4,5},{5,6},{6,7},{7,4},{8,9},{9,10},{10,1... | collective-permute-start | bytes 147464 | tf_op jit(solution)/shard_map/ppermute | solution.py:26
  182.9 5.1 %collective-permute-start.25 = (bf16[24,1024]{1,0:T(8,128)(2,1)S(1)}, bf16[24,1024]{1,0:T(8,128)(2,1)S(1)}, u32[]{:S(2)}, u32[]{:S(2)}) collective-permute-start(bf16[24,1024]{1,0:T(8,128)(2,1)S(1)} %combine.1.refs_0_), channel_id=1, source_target_pairs={{0,2},{1,3},{2,0},{3,1},{4,6},{5,7},{6,4},{7,5},{8,10},{9,11},{10,... | collective-permute-start | bytes 147464 | tf_op jit(solution)/shard_map/ppermute | solution.py:26
  185.7 3.4 %collective-permute-start.26 = (bf16[24,1024]{1,0:T(8,128)(2,1)S(1)}, bf16[24,1024]{1,0:T(8,128)(2,1)S(1)}, u32[]{:S(2)}, u32[]{:S(2)}) collective-permute-start(bf16[24,1024]{1,0:T(8,128)(2,1)S(1)} %combine.1.refs_0_), channel_id=1, source_target_pairs={{0,3},{1,0},{2,1},{3,2},{4,7},{5,4},{6,5},{7,6},{8,11},{9,8},{10,9... | collective-permute-start | bytes 147464 | tf_op jit(solution)/shard_map/ppermute | solution.py:26

commit v3 on v2

--- a/solution.py
+++ b/solution.py
@@ -151,34 +151,38 @@
         out_specs=[VMEM] * nt,
         scratch_shapes=[pltpu.SemaphoreType.DMA((nt, nz))],
         cost_estimate=cost(1e6, 4 * rows * cols),
-        compiler_params=room(6),
+        compiler_params=room(62),
         name="split",
     )(where, down)
 
 
-def project_kernel(nx, where, tok, *refs):
+def project_kernel(nx, nz, where, tok, *refs):
     own, other = refs[:nx], refs[nx : 2 * nx]
-    out, weight = refs[2 * nx :]
-    x, c = where[1], where[2]
+    outs = refs[2 * nx : 2 * nx + nz]
+    weight = refs[-1]
+    z, x, c = where[0], where[1], where[2]
     rows = own[0].shape[0]
-    nz, seqs, cols = out.shape
+    seqs = outs[0].shape[0]
     for i in range(nx):
         base = lax.rem(x - i + nx, nx) * (2 * rows)
         weight[pl.ds(pl.multiple_of(base + c * rows, rows), rows), :] = own[i][...]
         weight[pl.ds(pl.multiple_of(base + (1 - c) * rows, rows), rows), :] = other[i][...]
-    left = tok[:, :seqs].astype(f32).reshape(nz * seqs, tok.shape[2]).astype(bf16)
+    left = jnp.concatenate(
+        [tok[lax.rem(z + s, nz), :seqs].astype(f32) for s in range(nz)], axis=0
+    ).astype(bf16)
     total = jnp.dot(left, weight[...], preferred_element_type=f32)
-    out[...] = total.reshape(nz, seqs, cols).astype(bf16)
+    for s in range(nz):
+        outs[s][...] = total[s * seqs : (s + 1) * seqs].astype(bf16)
 
 
 def project(where, tok, seqs, own, other):
     nz, _, depth = tok.shape
     nx, cols = len(own), own[0].shape[1]
     return pl.pallas_call(
-        functools.partial(project_kernel, nx),
-        out_shape=shaped((nz, seqs, cols), bf16),
+        functools.partial(project_kernel, nx, nz),
+        out_shape=[shaped((seqs, cols), bf16)] * nz,
         in_specs=[SMEM] + [VMEM] * (1 + 2 * nx),
-        out_specs=VMEM,
+        out_specs=[VMEM] * nz,
         scratch_shapes=[pltpu.VMEM((depth, cols), bf16)],
         cost_estimate=cost(2 * nz * seqs * depth * cols, 2 * depth * cols),
         compiler_params=room(10),
@@ -186,7 +190,9 @@
     )(where, tok, *own, *other)
 
 
-def attend_kernel(step, arrived, scale, shift_of, state_at, gain, out, state, sems):
+def attend_kernel(step, count, *refs):
+    arrived, refs = refs[:count], refs[count:]
+    scale, shift_of, state_at, gain, out, state, sems = refs
     seqs, heads = state.shape[:2]
     copies = [
         pltpu.make_async_copy(
@@ -196,7 +202,10 @@
     ]
     for copy in copies:
         copy.start()
-    total = jnp.sum(arrived[...].astype(f32), axis=0) * scale[:, :1]
+    total = arrived[0][...].astype(f32)
+    for ref in arrived[1:]:
+        total = total + ref[...].astype(f32)
+    total = total * scale[:, :1]
     rows = step
     keys = shift_of.shape[1]
     vals = out.shape[1]
@@ -238,9 +247,9 @@
     step = 8
     vals = heads * width
     return pl.pallas_call(
-        functools.partial(attend_kernel, step),
+        functools.partial(attend_kernel, step, len(arrived)),
         out_shape=shaped((seqs, vals), bf16),
-        in_specs=[VMEM, VMEM, VMEM, HBM, VMEM],
+        in_specs=[VMEM] * (len(arrived) + 2) + [HBM, VMEM],
         out_specs=VMEM,
         scratch_shapes=[
             pltpu.VMEM(state.shape, f32),
@@ -249,7 +258,7 @@
         cost_estimate=cost(4 * state.size, 4 * state.size),
         compiler_params=room(52),
         name="attend",
-    )(arrived, scale, decay_shift, state, head_gain)
+    )(*arrived, scale, decay_shift, state, head_gain)
 
 
 def mix_kernel(nx, where, gated, partner, *refs):
@@ -561,7 +570,7 @@
     inverse = 1.0 / gain_of
 
     parts = project(where, moved, seqs, own, other)
-    arrived = lax.all_to_all(parts, Z, 0, 0, tiled=True)
+    arrived = [parts[0]] + [shift(parts[i], Z, i) for i in order_of(nz)]
     gated = attend(arrived, first_scale, decay_shift, state, head_gain)
     partner = shift(gated, C, 1)
     mixed = mix(where, gated, partner, blocks)

time: 191 us -> 192 us (level)
  starting transfers between devices: 58.1 us -> 71.8 us
  waiting for transfers between devices: 83.7 us -> 71.6 us
  blocking collectives: 22.7 us -> 19.8 us
    ppermute x27 -> x34, starting transfers between devices: 38.8 us -> 56.2 us  [shift(): return lax.ppermute(value, axis, [(i, (i + by) % n) for i in range(n)])]
    all_to_all x1 -> x0, waiting for transfers between devices: 16.6 us -> none  [on_device(): arrived = lax.all_to_all(parts, Z, 0, 0, tiled=True)]
    ppermute x27 -> x34, waiting for transfers between devices: 48.3 us -> 52.9 us  [shift(): return lax.ppermute(value, axis, [(i, (i + by) % n) for i in range(n)])]
    all_to_all x1 -> x0, starting transfers between devices: 3.69 us -> none  [on_device(): arrived = lax.all_to_all(parts, Z, 0, 0, tiled=True)]
    all_to_all x1, blocking collectives: 22.7 us -> 19.8 us  [on_device(): lax.all_to_all(outbound.reshape(n_ep, -1, 128), EP, 0, 0, tiled=True)]
    pallas_call x1, Pallas kernels: 1.51 us -> 3.92 us  [split(): pl.pallas_call(functools.partial(split_kernel, nz), out_shape=[shaped((ro...]
    unnamed x23 -> x27, local copies, waits for them, and re-layouts: 2.66 us -> 4.26 us
  transfers between devices with their start and end apart: 30 -> 36, of which waited for: 19 -> 22; matrix products, arithmetic and copies ran while one was open for 1% -> 1% of each run, Pallas kernels for 6% -> 7%
where the time goes in v3:
time: 192 us; the launch traced here: 191 us
  starting transfers between devices  71.8 us (37%)
  waiting for transfers between devices  71.6 us (37%)
  Pallas kernels  22.4 us (12%)
  blocking collectives  19.8 us (10%)
  local copies, waits for them, and re-layouts  4.69 us (2%)
    ppermute x34, starting transfers between devices, shift(): return lax.ppermute(value, axis, [(i, (i + by) % n) for i in range(n)])  56.2 us
    ppermute x34, waiting for transfers between devices, shift(): return lax.ppermute(value, axis, [(i, (i + by) % n) for i in range(n)])  52.9 us
    all_to_all x1, blocking collectives, on_device(): lax.all_to_all(outbound.reshape(n_ep, -1, 128), EP, 0, 0, tiled=True)  19.8 us
    all_to_all x1, waiting for transfers between devices, on_device(): lax.all_to_all(done.reshape(n_ep, -1, 128), EP, 0, 0, tiled=True)  15.1 us
    all_to_all x1, starting transfers between devices, on_device(): moved = lax.all_to_all(payload, Z, 0, 0, tiled=True)  9.02 us
    all_to_all x1, starting transfers between devices, on_device(): lax.all_to_all(done.reshape(n_ep, -1, 128), EP, 0, 0, tiled=True)  6.61 us
    unnamed x27, local copies, waits for them, and re-layouts  4.26 us
    pallas_call x1, Pallas kernels, split(): pl.pallas_call(functools.partial(split_kernel, nz), out_shape=[shaped((ro...  3.92 us
  transfers between devices with their start and end apart: 36, of which 22 were waited for; matrix products, arithmetic and copies ran while one was open for 1% of the time, Pallas kernels for 7%

profile of v3, /device:TPU:1, one launch (start us, length us, event | category | flops | bytes accessed | tf_op | source)
XLA Modules:
  0.0 191.3 jit_solution(11594922963798585292)
XLA Ops:
  0.0 2.0 %scale.1 = (bf16[8,88,512]{2,1,0:T(8,128)(2,1)}, f32[24,128]{1,0:T(8,128)}) custom-call(bf16[24,4096]{1,0:T(8,128)(2,1)} %tokens.1, bf16[4096]{0:T(1024)(128)(2,1)} %gain_at.1, bf16[64,512]{1,0:T(8,128)(2,1)} %bitcast.30), custom_call_target="tpu_custom_call" | custom-call | flops 1000000 | bytes 393216 | tf_op jit(solution)/shard_map/scale/pallas_call | solution.py:106
  2.0 9.0 %all-to-all-start = ((bf16[8,88,512]{2,1,0:T(8,128)(2,1)}), bf16[8,88,512]{2,1,0:T(8,128)(2,1)S(1)}, u32[]{:S(2)}, u32[]{:S(2)}) async-start(bf16[8,88,512]{2,1,0:T(8,128)(2,1)} %get-tuple-element.36), calls=%async_computation | async-start | bytes 1441792 | tf_op jit(solution)/shard_map/all_to_all | solution.py:560
  11.1 1.7 pack.1.refs_0_
  12.7 1.3 collective-permute-start
  14.0 2.5 %collective-permute-start.1 = (bf16[64,1792]{1,0:T(8,128)(2,1)}, bf16[64,1792]{1,0:T(8,128)(2,1)S(1)}, u32[]{:S(2)}, u32[]{:S(2)}) collective-permute-start(bf16[64,1792]{1,0:T(8,128)(2,1)} %pack.1.refs_0_), channel_id=1, source_target_pairs={{0,16},{8,24},{16,0},{24,8},{1,17},{9,25},{17,1},{25,9},{2,18},{10... | collective-permute-start | bytes 688136 | tf_op jit(solution)/shard_map/ppermute | solution.py:26
  16.5 1.2 collective-permute-start.2
  17.6 1.8 collective-permute-start.3
  19.4 1.0 collective-permute-done.refs_1_
  20.4 2.2 %collective-permute-start.4 = (bf16[64,1792]{1,0:T(8,128)(2,1)S(1)}, bf16[64,1792]{1,0:T(8,128)(2,1)S(1)}, u32[]{:S(2)}, u32[]{:S(2)}) collective-permute-start(bf16[64,1792]{1,0:T(8,128)(2,1)S(1)} %collective-permute-done.refs_1_), channel_id=1, source_target_pairs={{0,4},{4,0},{1,5},{5,1},{2,6},{6,2},{3,7},{7,3},{8,12},{12,8},{9,1... | collective-permute-start | bytes 688136 | tf_op jit(solution)/shard_map/ppermute | solution.py:26
  22.7 3.7 %collective-permute-done.1.refs_2_ = bf16[64,1792]{1,0:T(8,128)(2,1)S(1)} collective-permute-done((bf16[64,1792]{1,0:T(8,128)(2,1)}, bf16[64,1792]{1,0:T(8,128)(2,1)S(1)}, u32[]{:S(2)}, u32[]{:S(2)}) %collective-permute-start.1) | collective-permute-done | bytes 229408 | tf_op jit(solution)/shard_map/ppermute | solution.py:26
  26.3 1.8 collective-permute-start.5
  28.3 1.0 collective-permute-done.5.refs_6_
  29.7 3.5 %all-to-all-done.tok = bf16[8,88,512]{2,1,0:T(8,128)(2,1)S(1)} async-done(((bf16[8,88,512]{2,1,0:T(8,128)(2,1)}), bf16[8,88,512]{2,1,0:T(8,128)(2,1)S(1)}, u32[]{:S(2)}, u32[]{:S(2)}) %all-to-all-start) | async-done | bytes 720928 | tf_op jit(solution)/shard_map/all_to_all | solution.py:560
  33.2 0.9 copy-done.2
  34.1 1.2 project.1
  35.4 3.6 %collective-permute-start.11 = (bf16[24,1792]{1,0:T(8,128)(2,1)S(1)}, bf16[24,1792]{1,0:T(8,128)(2,1)S(1)}, u32[]{:S(2)}, u32[]{:S(2)}) collective-permute-start(bf16[24,1792]{1,0:T(8,128)(2,1)S(1)} %get-tuple-element.42), channel_id=1, source_target_pairs={{0,192},{32,224},{64,0},{96,32},{128,64},{160,96},{192,128},{224,1... | collective-permute-start | bytes 258056 | tf_op jit(solution)/shard_map/ppermute | solution.py:26
  39.2 1.3 collective-permute-start.15
  40.5 2.5 %collective-permute-start.16 = (bf16[8,64,512]{2,1,0:T(8,128)(2,1)S(1)}, bf16[8,64,512]{2,1,0:T(8,128)(2,1)S(1)}, u32[]{:S(2)}, u32[]{:S(2)}) collective-permute-start(bf16[8,64,512]{2,1,0:T(8,128)(2,1)S(1)} %slice.36.refs_0_), channel_id=1, source_target_pairs={{0,16},{8,24},{16,0},{24,8},{1,17},{9,25},{17,1},{25,9},{2,18},{10... | collective-permute-start | bytes 1572872 | tf_op jit(solution)/shard_map/ppermute | solution.py:26
  43.0 1.2 collective-permute-start.17
  44.1 2.7 %collective-permute-start.13 = (bf16[24,1792]{1,0:T(8,128)(2,1)S(1)}, bf16[24,1792]{1,0:T(8,128)(2,1)S(1)}, u32[]{:S(2)}, u32[]{:S(2)}) collective-permute-start(bf16[24,1792]{1,0:T(8,128)(2,1)S(1)} %get-tuple-element.44), channel_id=1, source_target_pairs={{0,224},{32,0},{64,32},{96,64},{128,96},{160,128},{192,160},{224,1... | collective-permute-start | bytes 258056 | tf_op jit(solution)/shard_map/ppermute | solution.py:26
  46.8 1.4 collective-permute-start.7
  48.3 0.7 collective-permute-done.13.refs_7_
  49.0 1.6 collective-permute-start.8
  50.7 3.5 %collective-permute-done.7.refs_1_ = bf16[24,1792]{1,0:T(8,128)(2,1)S(1)} collective-permute-done((bf16[24,1792]{1,0:T(8,128)(2,1)S(1)}, bf16[24,1792]{1,0:T(8,128)(2,1)S(1)}, u32[]{:S(2)}, u32[]{:S(2)}) %collective-permute-start.7) | collective-permute-done | bytes 86048 | tf_op jit(solution)/shard_map/ppermute | solution.py:26
  54.3 1.3 collective-permute-done.8.refs_2_
  55.6 4.0 %collective-permute-done.9.refs_3_ = bf16[24,1792]{1,0:T(8,128)(2,1)S(1)} collective-permute-done((bf16[24,1792]{1,0:T(8,128)(2,1)S(1)}, bf16[24,1792]{1,0:T(8,128)(2,1)S(1)}, u32[]{:S(2)}, u32[]{:S(2)}) %collective-permute-start.9) | collective-permute-done | bytes 86048 | tf_op jit(solution)/shard_map/ppermute | solution.py:26
  59.6 3.4 %attend.1.gated = bf16[24,512]{1,0:T(8,128)(2,1)S(1)} custom-call(bf16[24,1792]{1,0:T(8,128)(2,1)S(1)} %get-tuple-element.37.refs_0_, bf16[24,1792]{1,0:T(8,128)(2,1)S(1)} %collective-permute-done.7.refs_1_, bf16[24,1792]{1,0:T(8,128)(2,1)S(1)} %collective-permute-done.8.refs_2_, bf16[24,1792]{1,0:T(8,128)(2,1)S(1)} %collective-permute-done.9.refs_3_, ...), custom_call_target="tpu_custom_call" | custom-call | flops 6291456 | bytes 6291456 | tf_op jit(solution)/shard_map/attend/pallas_call | solution.py:249
  63.0 8.0 %collective-permute-start.14 = (bf16[24,512]{1,0:T(8,128)(2,1)S(1)}, bf16[24,512]{1,0:T(8,128)(2,1)S(1)}, u32[]{:S(2)}, u32[]{:S(2)}) collective-permute-start(bf16[24,512]{1,0:T(8,128)(2,1)S(1)} %attend.1.gated), channel_id=1, source_target_pairs={{0,4},{4,0},{1,5},{5,1},{2,6},{6,2},{3,7},{7,3},{8,12},{12,8},{9,1... | collective-permute-start | bytes 73736 | tf_op jit(solution)/shard_map/ppermute | solution.py:26
  71.8 1.5 mix.1
  73.3 1.5 collective-permute-start.18
  74.8 2.5 %collective-permute-start.19 = (bf16[48,512]{1,0:T(8,128)(2,1)S(1)}, bf16[48,512]{1,0:T(8,128)(2,1)S(1)}, u32[]{:S(2)}, u32[]{:S(2)}) collective-permute-start(bf16[48,512]{1,0:T(8,128)(2,1)S(1)} %get-tuple-element.48), channel_id=1, source_target_pairs={{0,2},{1,3},{2,0},{3,1},{4,6},{5,7},{6,4},{7,5},{8,10},{9,11},{10,... | collective-permute-start | bytes 147464 | tf_op jit(solution)/shard_map/ppermute | solution.py:26
  77.3 1.1 collective-permute-start.20
  78.4 1.2 collective-permute-done.19
  79.6 1.0 collective-permute-done.20
  80.6 1.8 collective-permute-start.21
  82.7 0.6 collective-permute-done.21.other
  83.3 0.9 dispatch.1
  84.3 19.8 %all_to_all.15 = bf16[64,24,128]{2,1,0:T(8,128)(2,1)S(1)} all-to-all(bf16[64,24,128]{2,1,0:T(8,128)(2,1)S(1)} %bitcast.25), channel_id=1, replica_groups=mesh['ep_0'=8,'ep_1'=4,'ep_2'=2,'tp'=4] {'ep_0','ep_1','ep_2'}, dimensions={0} | all-to-all | bytes 786432 | tf_op jit(solution)/shard_map/all_to_all | solution.py:584
  104.1 3.9 %split.1 = (bf16[256,1024]{1,0:T(8,128)(2,1)}, bf16[256,1024]{1,0:T(8,128)(2,1)}, bf16[256,1024]{1,0:T(8,128)(2,1)}, bf16[256,1024]{1,0:T(8,128)(2,1)}) custom-call(s32[4]{0:T(128)} %copy-done.5, bf16[256,4096]{1,0:T(8,128)(2,1)} %bitcast.29), custom_call_target="tpu_custom_call" | custom-call | flops 1000000 | bytes 4194304 | tf_op jit(solution)/shard_map/split/pallas_call | solution.py:147
  108.0 1.0 collective-permute-start.28
  109.0 1.9 collective-permute-start.23
  110.8 2.2 %collective-permute-start.29 = (bf16[256,1024]{1,0:T(8,128)(2,1)}, bf16[256,1024]{1,0:T(8,128)(2,1)S(1)}, u32[]{:S(2)}, u32[]{:S(2)}) collective-permute-start(bf16[256,1024]{1,0:T(8,128)(2,1)} %get-tuple-element.62), channel_id=1, source_target_pairs={{0,2},{1,3},{2,0},{3,1},{4,6},{5,7},{6,4},{7,5},{8,10},{9,11},{10,... | collective-permute-start | bytes 1572872 | tf_op jit(solution)/shard_map/ppermute | solution.py:26
  113.0 0.6 collective-permute-start.30
  113.6 2.1 %collective-permute-done.24.piece = bf16[1536,128]{1,0:T(8,128)(2,1)S(1)} collective-permute-done((bf16[1536,128]{1,0:T(8,128)(2,1)S(1)}, bf16[1536,128]{1,0:T(8,128)(2,1)S(1)}, u32[]{:S(2)}, u32[]{:S(2)}) %collective-permute-start.24) | collective-permute-done | bytes 393248 | tf_op jit(solution)/shard_map/ppermute | solution.py:26
  115.7 1.6 copy-done
  117.3 1.6 copy-done.1
  118.9 1.0 pick.1
  119.9 1.0 expert.4
  120.9 1.0 expert.5
  121.9 1.0 expert.6
  122.9 24.5 %collective-permute-done.22.piece = bf16[1536,128]{1,0:T(8,128)(2,1)S(1)} collective-permute-done((bf16[1536,128]{1,0:T(8,128)(2,1)S(1)}, bf16[1536,128]{1,0:T(8,128)(2,1)S(1)}, u32[]{:S(2)}, u32[]{:S(2)}) %collective-permute-start.22) | collective-permute-done | bytes 393248 | tf_op jit(solution)/shard_map/ppermute | solution.py:26
  147.4 1.0 expert.7.refs_0_
  148.4 4.8 %collective-permute-start.25 = (bf16[192,256]{1,0:T(8,128)(2,1)S(1)}, bf16[192,256]{1,0:T(8,128)(2,1)S(1)}, u32[]{:S(2)}, u32[]{:S(2)}) collective-permute-start(bf16[192,256]{1,0:T(8,128)(2,1)S(1)} %expert.7.refs_0_), channel_id=1, source_target_pairs={{0,1},{1,2},{2,3},{3,0},{4,5},{5,6},{6,7},{7,4},{8,9},{9,10},{10,1... | collective-permute-start | bytes 294920 | tf_op jit(solution)/shard_map/ppermute | solution.py:26
  153.2 2.3 %collective-permute-start.26 = (bf16[192,256]{1,0:T(8,128)(2,1)S(1)}, bf16[192,256]{1,0:T(8,128)(2,1)S(1)}, u32[]{:S(2)}, u32[]{:S(2)}) collective-permute-start(bf16[192,256]{1,0:T(8,128)(2,1)S(1)} %expert.7.refs_0_), channel_id=1, source_target_pairs={{0,2},{1,3},{2,0},{3,1},{4,6},{5,7},{6,4},{7,5},{8,10},{9,11},{10,... | collective-permute-start | bytes 294920 | tf_op jit(solution)/shard_map/ppermute | solution.py:26
  156.3 2.5 %collective-permute-done.26.refs_2_ = bf16[192,256]{1,0:T(8,128)(2,1)S(1)} collective-permute-done((bf16[192,256]{1,0:T(8,128)(2,1)S(1)}, bf16[192,256]{1,0:T(8,128)(2,1)S(1)}, u32[]{:S(2)}, u32[]{:S(2)}) %collective-permute-start.26) | collective-permute-done | bytes 98336 | tf_op jit(solution)/shard_map/ppermute | solution.py:26
  158.8 1.4 collective-permute-done.27.refs_3_
  160.2 1.4 down.1
  161.6 6.6 %all-to-all-start.2 = ((bf16[64,24,128]{2,1,0:T(8,128)(2,1)}), bf16[64,24,128]{2,1,0:T(8,128)(2,1)S(1)}, u32[]{:S(2)}, u32[]{:S(2)}) async-start(bf16[64,24,128]{2,1,0:T(8,128)(2,1)} %bitcast.14), calls=%async_computation.2 | async-start | bytes 786432 | tf_op jit(solution)/shard_map/all_to_all | solution.py:600
  168.2 15.1 %all-to-all-done.2 = bf16[64,24,128]{2,1,0:T(8,128)(2,1)S(1)} async-done(((bf16[64,24,128]{2,1,0:T(8,128)(2,1)}), bf16[64,24,128]{2,1,0:T(8,128)(2,1)S(1)}, u32[]{:S(2)}, u32[]{:S(2)}) %all-to-all-start.2) | async-done | bytes 393248 | tf_op jit(solution)/shard_map/all_to_all | solution.py:600
  183.8 2.8 %collective-permute-start.32 = (bf16[24,1024]{1,0:T(8,128)(2,1)S(1)}, bf16[24,1024]{1,0:T(8,128)(2,1)S(1)}, u32[]{:S(2)}, u32[]{:S(2)}) collective-permute-start(bf16[24,1024]{1,0:T(8,128)(2,1)S(1)} %combine.1.refs_0_), channel_id=1, source_target_pairs={{0,2},{1,3},{2,0},{3,1},{4,6},{5,7},{6,4},{7,5},{8,10},{9,11},{10,... | collective-permute-start | bytes 147464 | tf_op jit(solution)/shard_map/ppermute | solution.py:26
  187.0 0.9 collective-permute-done.31.refs_1_
  187.9 1.0 collective-permute-done.32.refs_2_
  188.9 1.1 collective-permute-done.33.refs_3_
  190.0 1.3 finish.1
  (68 shorter events, 4.0 us)
Async XLA Ops:
  2.0 37.0 %copy-start.11 = (s32[24,4]{0,1:T(4,128)S(1)}, s32[24,4]{0,1:T(4,128)}, u32[]{:S(2)}) copy-start(s32[24,4]{0,1:T(4,128)} %param.32) | copy-start | bytes 1156
  2.0 31.2 %all-to-all-start = ((bf16[8,88,512]{2,1,0:T(8,128)(2,1)}), bf16[8,88,512]{2,1,0:T(8,128)(2,1)S(1)}, u32[]{:S(2)}, u32[]{:S(2)}) async-start(bf16[8,88,512]{2,1,0:T(8,128)(2,1)} %get-tuple-element.36), calls=%async_computation | async-start | bytes 1441792 | tf_op jit(solution)/shard_map/all_to_all | solution.py:560
  11.0 43.2 %copy-start.10 = (bf16[4096]{0:T(1024)(128)(2,1)S(1)}, bf16[4096]{0:T(1024)(128)(2,1)}, u32[]{:S(2)}) copy-start(bf16[4096]{0:T(1024)(128)(2,1)} %param.28) | copy-start | bytes 24580
  11.0 48.6 %copy-start.7 = (f32[24,256]{1,0:T(8,128)S(1)}, f32[24,256]{1,0:T(8,128)}, u32[]{:S(2)}) copy-start(f32[24,256]{1,0:T(8,128)} %refs_9_.1) | copy-start | bytes 73732
  11.0 48.6 %copy-start.8 = (f32[24,128]{1,0:T(8,128)S(1)}, f32[24,128]{1,0:T(8,128)}, u32[]{:S(2)}) copy-start(f32[24,128]{1,0:T(8,128)} %get-tuple-element.45.refs_8_) | copy-start | bytes 36868
  11.0 48.6 %copy-start.9 = (bf16[512]{0:T(512)(128)(2,1)S(1)}, bf16[512]{0:T(512)(128)(2,1)}, u32[]{:S(2)}) copy-start(bf16[512]{0:T(512)(128)(2,1)} %refs_11_.1) | copy-start | bytes 3076
  12.7 7.7 %collective-permute-start = (bf16[64,1792]{1,0:T(8,128)(2,1)}, bf16[64,1792]{1,0:T(8,128)(2,1)S(1)}, u32[]{:S(2)}, u32[]{:S(2)}) collective-permute-start(bf16[64,1792]{1,0:T(8,128)(2,1)} %pack.1.refs_0_), channel_id=1, source_target_pairs={{0,8},{8,16},{16,24},{24,0},{1,9},{9,17},{17,25},{25,1},{2,10},{10... | collective-permute-start | bytes 688136 | tf_op jit(solution)/shard_map/ppermute | solution.py:26
  14.0 12.3 %collective-permute-start.1 = (bf16[64,1792]{1,0:T(8,128)(2,1)}, bf16[64,1792]{1,0:T(8,128)(2,1)S(1)}, u32[]{:S(2)}, u32[]{:S(2)}) collective-permute-start(bf16[64,1792]{1,0:T(8,128)(2,1)} %pack.1.refs_0_), channel_id=1, source_target_pairs={{0,16},{8,24},{16,0},{24,8},{1,17},{9,25},{17,1},{25,9},{2,18},{10... | collective-permute-start | bytes 688136 | tf_op jit(solution)/shard_map/ppermute | solution.py:26
  16.5 11.7 %collective-permute-start.2 = (bf16[64,1792]{1,0:T(8,128)(2,1)}, bf16[64,1792]{1,0:T(8,128)(2,1)S(1)}, u32[]{:S(2)}, u32[]{:S(2)}) collective-permute-start(bf16[64,1792]{1,0:T(8,128)(2,1)} %pack.1.refs_0_), channel_id=1, source_target_pairs={{0,24},{8,0},{16,8},{24,16},{1,25},{9,1},{17,9},{25,17},{2,26},{10... | collective-permute-start | bytes 688136 | tf_op jit(solution)/shard_map/ppermute | solution.py:26
  17.6 10.6 %collective-permute-start.3 = (bf16[64,1792]{1,0:T(8,128)(2,1)}, bf16[64,1792]{1,0:T(8,128)(2,1)S(1)}, u32[]{:S(2)}, u32[]{:S(2)}) collective-permute-start(bf16[64,1792]{1,0:T(8,128)(2,1)} %pack.1.refs_0_), channel_id=1, source_target_pairs={{0,4},{4,0},{1,5},{5,1},{2,6},{6,2},{3,7},{7,3},{8,12},{12,8},{9,1... | collective-permute-start | bytes 688136 | tf_op jit(solution)/shard_map/ppermute | solution.py:26
  20.4 7.8 %collective-permute-start.4 = (bf16[64,1792]{1,0:T(8,128)(2,1)S(1)}, bf16[64,1792]{1,0:T(8,128)(2,1)S(1)}, u32[]{:S(2)}, u32[]{:S(2)}) collective-permute-start(bf16[64,1792]{1,0:T(8,128)(2,1)S(1)} %collective-permute-done.refs_1_), channel_id=1, source_target_pairs={{0,4},{4,0},{1,5},{5,1},{2,6},{6,2},{3,7},{7,3},{8,12},{12,8},{9,1... | collective-permute-start | bytes 688136 | tf_op jit(solution)/shard_map/ppermute | solution.py:26
  26.3 2.9 %collective-permute-start.5 = (bf16[64,1792]{1,0:T(8,128)(2,1)S(1)}, bf16[64,1792]{1,0:T(8,128)(2,1)S(1)}, u32[]{:S(2)}, u32[]{:S(2)}) collective-permute-start(bf16[64,1792]{1,0:T(8,128)(2,1)S(1)} %collective-permute-done.1.refs_2_), channel_id=1, source_target_pairs={{0,4},{4,0},{1,5},{5,1},{2,6},{6,2},{3,7},{7,3},{8,12},{12,8},{9,1... | collective-permute-start | bytes 688136 | tf_op jit(solution)/shard_map/ppermute | solution.py:26
  28.2 1.5 collective-permute-start.6
  28.2 55.1 %copy-start.5 = (s32[4]{0:T(128)}, s32[4]{0:T(128)S(1)}, u32[]{:S(2)}) copy-start(s32[4]{0:T(128)S(1)} %pad_add_fusion.where) | copy-start | bytes 52
  33.2 0.9 copy-start.2
  35.3 7.6 %collective-permute-start.10 = (bf16[24,1792]{1,0:T(8,128)(2,1)S(1)}, bf16[24,1792]{1,0:T(8,128)(2,1)S(1)}, u32[]{:S(2)}, u32[]{:S(2)}) collective-permute-start(bf16[24,1792]{1,0:T(8,128)(2,1)S(1)} %get-tuple-element.41), channel_id=1, source_target_pairs={{0,64},{32,96},{64,128},{96,160},{128,192},{160,224},{192,0},{224,... | collective-permute-start | bytes 258056 | tf_op jit(solution)/shard_map/ppermute | solution.py:26
  35.4 8.7 %collective-permute-start.11 = (bf16[24,1792]{1,0:T(8,128)(2,1)S(1)}, bf16[24,1792]{1,0:T(8,128)(2,1)S(1)}, u32[]{:S(2)}, u32[]{:S(2)}) collective-permute-start(bf16[24,1792]{1,0:T(8,128)(2,1)S(1)} %get-tuple-element.42), channel_id=1, source_target_pairs={{0,192},{32,224},{64,0},{96,32},{128,64},{160,96},{192,128},{224,1... | collective-permute-start | bytes 258056 | tf_op jit(solution)/shard_map/ppermute | solution.py:26
  39.0 7.8 %collective-permute-start.12 = (bf16[24,1792]{1,0:T(8,128)(2,1)S(1)}, bf16[24,1792]{1,0:T(8,128)(2,1)S(1)}, u32[]{:S(2)}, u32[]{:S(2)}) collective-permute-start(bf16[24,1792]{1,0:T(8,128)(2,1)S(1)} %get-tuple-element.43), channel_id=1, source_target_pairs={{0,32},{32,64},{64,96},{96,128},{128,160},{160,192},{192,224},{224... | collective-permute-start | bytes 258056 | tf_op jit(solution)/shard_map/ppermute | solution.py:26
  39.2 32.6 %collective-permute-start.15 = (bf16[8,64,512]{2,1,0:T(8,128)(2,1)S(1)}, bf16[8,64,512]{2,1,0:T(8,128)(2,1)S(1)}, u32[]{:S(2)}, u32[]{:S(2)}) collective-permute-start(bf16[8,64,512]{2,1,0:T(8,128)(2,1)S(1)} %slice.36.refs_0_), channel_id=1, source_target_pairs={{0,8},{8,16},{16,24},{24,0},{1,9},{9,17},{17,25},{25,1},{2,10},{10... | collective-permute-start | bytes 1572872 | tf_op jit(solution)/shard_map/ppermute | solution.py:26
  40.5 31.3 %collective-permute-start.16 = (bf16[8,64,512]{2,1,0:T(8,128)(2,1)S(1)}, bf16[8,64,512]{2,1,0:T(8,128)(2,1)S(1)}, u32[]{:S(2)}, u32[]{:S(2)}) collective-permute-start(bf16[8,64,512]{2,1,0:T(8,128)(2,1)S(1)} %slice.36.refs_0_), channel_id=1, source_target_pairs={{0,16},{8,24},{16,0},{24,8},{1,17},{9,25},{17,1},{25,9},{2,18},{10... | collective-permute-start | bytes 1572872 | tf_op jit(solution)/shard_map/ppermute | solution.py:26
  43.0 28.9 %collective-permute-start.17 = (bf16[8,64,512]{2,1,0:T(8,128)(2,1)S(1)}, bf16[8,64,512]{2,1,0:T(8,128)(2,1)S(1)}, u32[]{:S(2)}, u32[]{:S(2)}) collective-permute-start(bf16[8,64,512]{2,1,0:T(8,128)(2,1)S(1)} %slice.36.refs_0_), channel_id=1, source_target_pairs={{0,24},{8,0},{16,8},{24,16},{1,25},{9,1},{17,9},{25,17},{2,26},{10... | collective-permute-start | bytes 1572872 | tf_op jit(solution)/shard_map/ppermute | solution.py:26
  44.1 4.9 %collective-permute-start.13 = (bf16[24,1792]{1,0:T(8,128)(2,1)S(1)}, bf16[24,1792]{1,0:T(8,128)(2,1)S(1)}, u32[]{:S(2)}, u32[]{:S(2)}) collective-permute-start(bf16[24,1792]{1,0:T(8,128)(2,1)S(1)} %get-tuple-element.44), channel_id=1, source_target_pairs={{0,224},{32,0},{64,32},{96,64},{128,96},{160,128},{192,160},{224,1... | collective-permute-start | bytes 258056 | tf_op jit(solution)/shard_map/ppermute | solution.py:26
  46.8 7.4 %collective-permute-start.7 = (bf16[24,1792]{1,0:T(8,128)(2,1)S(1)}, bf16[24,1792]{1,0:T(8,128)(2,1)S(1)}, u32[]{:S(2)}, u32[]{:S(2)}) collective-permute-start(bf16[24,1792]{1,0:T(8,128)(2,1)S(1)} %get-tuple-element.38), channel_id=1, source_target_pairs={{0,128},{32,160},{64,192},{96,224},{128,0},{160,32},{192,64},{224,... | collective-permute-start | bytes 258056 | tf_op jit(solution)/shard_map/ppermute | solution.py:26
  49.0 6.5 %collective-permute-start.8 = (bf16[24,1792]{1,0:T(8,128)(2,1)S(1)}, bf16[24,1792]{1,0:T(8,128)(2,1)S(1)}, u32[]{:S(2)}, u32[]{:S(2)}) collective-permute-start(bf16[24,1792]{1,0:T(8,128)(2,1)S(1)} %get-tuple-element.39), channel_id=1, source_target_pairs={{0,96},{32,128},{64,160},{96,192},{128,224},{160,0},{192,32},{224,... | collective-permute-start | bytes 258056 | tf_op jit(solution)/shard_map/ppermute | solution.py:26
  54.2 5.4 %collective-permute-start.9 = (bf16[24,1792]{1,0:T(8,128)(2,1)S(1)}, bf16[24,1792]{1,0:T(8,128)(2,1)S(1)}, u32[]{:S(2)}, u32[]{:S(2)}) collective-permute-start(bf16[24,1792]{1,0:T(8,128)(2,1)S(1)} %get-tuple-element.40), channel_id=1, source_target_pairs={{0,160},{32,192},{64,224},{96,0},{128,32},{160,64},{192,96},{224,1... | collective-permute-start | bytes 258056 | tf_op jit(solution)/shard_map/ppermute | solution.py:26
  63.0 19.5 %copy-start.12 = (f32[24,4]{0,1:T(4,128)S(1)}, f32[24,4]{0,1:T(4,128)}, u32[]{:S(2)}) copy-start(f32[24,4]{0,1:T(4,128)} %param.33) | copy-start | bytes 1156
  63.0 20.3 %copy-start.3 = (bf16[24,4096]{1,0:T(8,128)(2,1)S(1)}, bf16[24,4096]{1,0:T(8,128)(2,1)}, u32[]{:S(2)}) copy-start(bf16[24,4096]{1,0:T(8,128)(2,1)} %tokens.1) | copy-start | bytes 589828
  63.0 8.8 %collective-permute-start.14 = (bf16[24,512]{1,0:T(8,128)(2,1)S(1)}, bf16[24,512]{1,0:T(8,128)(2,1)S(1)}, u32[]{:S(2)}, u32[]{:S(2)}) collective-permute-start(bf16[24,512]{1,0:T(8,128)(2,1)S(1)} %attend.1.gated), channel_id=1, source_target_pairs={{0,4},{4,0},{1,5},{5,1},{2,6},{6,2},{3,7},{7,3},{8,12},{12,8},{9,1... | collective-permute-start | bytes 73736 | tf_op jit(solution)/shard_map/ppermute | solution.py:26
  73.3 5.1 %collective-permute-start.18 = (bf16[48,512]{1,0:T(8,128)(2,1)S(1)}, bf16[48,512]{1,0:T(8,128)(2,1)S(1)}, u32[]{:S(2)}, u32[]{:S(2)}) collective-permute-start(bf16[48,512]{1,0:T(8,128)(2,1)S(1)} %get-tuple-element.47), channel_id=1, source_target_pairs={{0,1},{1,2},{2,3},{3,0},{4,5},{5,6},{6,7},{7,4},{8,9},{9,10},{10,1... | collective-permute-start | bytes 147464 | tf_op jit(solution)/shard_map/ppermute | solution.py:26
  74.8 4.8 %collective-permute-start.19 = (bf16[48,512]{1,0:T(8,128)(2,1)S(1)}, bf16[48,512]{1,0:T(8,128)(2,1)S(1)}, u32[]{:S(2)}, u32[]{:S(2)}) collective-permute-start(bf16[48,512]{1,0:T(8,128)(2,1)S(1)} %get-tuple-element.48), channel_id=1, source_target_pairs={{0,2},{1,3},{2,0},{3,1},{4,6},{5,7},{6,4},{7,5},{8,10},{9,11},{10,... | collective-permute-start | bytes 147464 | tf_op jit(solution)/shard_map/ppermute | solution.py:26
  77.3 3.2 %collective-permute-start.20 = (bf16[48,512]{1,0:T(8,128)(2,1)S(1)}, bf16[48,512]{1,0:T(8,128)(2,1)S(1)}, u32[]{:S(2)}, u32[]{:S(2)}) collective-permute-start(bf16[48,512]{1,0:T(8,128)(2,1)S(1)} %get-tuple-element.49), channel_id=1, source_target_pairs={{0,3},{1,0},{2,1},{3,2},{4,7},{5,4},{6,5},{7,6},{8,11},{9,8},{10,9... | collective-permute-start | bytes 147464 | tf_op jit(solution)/shard_map/ppermute | solution.py:26
  80.6 2.7 %collective-permute-start.21 = (bf16[24,512]{1,0:T(8,128)(2,1)S(1)}, bf16[24,512]{1,0:T(8,128)(2,1)S(1)}, u32[]{:S(2)}, u32[]{:S(2)}) collective-permute-start(bf16[24,512]{1,0:T(8,128)(2,1)S(1)} %get-tuple-element.67), channel_id=1, source_target_pairs={{0,4},{4,0},{1,5},{5,1},{2,6},{6,2},{3,7},{7,3},{8,12},{12,8},{9,1... | collective-permute-start | bytes 73736 | tf_op jit(solution)/shard_map/ppermute | solution.py:26
  84.2 31.5 %copy-start.6 = (s32[4]{0:T(128)S(1)}, s32[4]{0:T(128)}, u32[]{:S(2)}) copy-start(s32[4]{0:T(128)} %copy-done.5) | copy-start | bytes 52
  104.1 11.6 %collective-permute-start.24 = (bf16[1536,128]{1,0:T(8,128)(2,1)S(1)}, bf16[1536,128]{1,0:T(8,128)(2,1)S(1)}, u32[]{:S(2)}, u32[]{:S(2)}) collective-permute-start(bf16[1536,128]{1,0:T(8,128)(2,1)S(1)} %bitcast.21), channel_id=1, source_target_pairs={{0,1},{1,2},{2,3},{3,0},{4,5},{5,6},{6,7},{7,4},{8,9},{9,10},{10,1... | collective-permute-start | bytes 1179656 | tf_op jit(solution)/shard_map/ppermute | solution.py:26
  108.0 47.5 %collective-permute-start.28 = (bf16[256,1024]{1,0:T(8,128)(2,1)}, bf16[256,1024]{1,0:T(8,128)(2,1)S(1)}, u32[]{:S(2)}, u32[]{:S(2)}) collective-permute-start(bf16[256,1024]{1,0:T(8,128)(2,1)} %get-tuple-element.61), channel_id=1, source_target_pairs={{0,1},{1,2},{2,3},{3,0},{4,5},{5,6},{6,7},{7,4},{8,9},{9,10},{10,1... | collective-permute-start | bytes 1572872 | tf_op jit(solution)/shard_map/ppermute | solution.py:26
  109.0 12.9 %collective-permute-start.23 = (bf16[1536,128]{1,0:T(8,128)(2,1)S(1)}, bf16[1536,128]{1,0:T(8,128)(2,1)S(1)}, u32[]{:S(2)}, u32[]{:S(2)}) collective-permute-start(bf16[1536,128]{1,0:T(8,128)(2,1)S(1)} %bitcast.22), channel_id=1, source_target_pairs={{0,3},{1,0},{2,1},{3,2},{4,7},{5,4},{6,5},{7,6},{8,11},{9,8},{10,9... | collective-permute-start | bytes 1179656 | tf_op jit(solution)/shard_map/ppermute | solution.py:26
  110.8 44.9 %collective-permute-start.29 = (bf16[256,1024]{1,0:T(8,128)(2,1)}, bf16[256,1024]{1,0:T(8,128)(2,1)S(1)}, u32[]{:S(2)}, u32[]{:S(2)}) collective-permute-start(bf16[256,1024]{1,0:T(8,128)(2,1)} %get-tuple-element.62), channel_id=1, source_target_pairs={{0,2},{1,3},{2,0},{3,1},{4,6},{5,7},{6,4},{7,5},{8,10},{9,11},{10,... | collective-permute-start | bytes 1572872 | tf_op jit(solution)/shard_map/ppermute | solution.py:26
  113.0 42.7 %collective-permute-start.30 = (bf16[256,1024]{1,0:T(8,128)(2,1)}, bf16[256,1024]{1,0:T(8,128)(2,1)S(1)}, u32[]{:S(2)}, u32[]{:S(2)}) collective-permute-start(bf16[256,1024]{1,0:T(8,128)(2,1)} %get-tuple-element.63), channel_id=1, source_target_pairs={{0,3},{1,0},{2,1},{3,2},{4,7},{5,4},{6,5},{7,6},{8,11},{9,8},{10,9... | collective-permute-start | bytes 1572872 | tf_op jit(solution)/shard_map/ppermute | solution.py:26
  115.7 31.7 %collective-permute-start.22 = (bf16[1536,128]{1,0:T(8,128)(2,1)S(1)}, bf16[1536,128]{1,0:T(8,128)(2,1)S(1)}, u32[]{:S(2)}, u32[]{:S(2)}) collective-permute-start(bf16[1536,128]{1,0:T(8,128)(2,1)S(1)} %bitcast.23), channel_id=1, source_target_pairs={{0,2},{1,3},{2,0},{3,1},{4,6},{5,7},{6,4},{7,5},{8,10},{9,11},{10,... | collective-permute-start | bytes 1179656 | tf_op jit(solution)/shard_map/ppermute | solution.py:26
  115.7 1.6 copy-start
  117.3 1.6 copy-start.1
  121.9 38.3 %copy-start.4 = (bf16[256,1024]{1,0:T(8,128)(2,1)S(1)}, bf16[256,1024]{1,0:T(8,128)(2,1)}, u32[]{:S(2)}) copy-start(bf16[256,1024]{1,0:T(8,128)(2,1)} %get-tuple-element.60.refs_4_) | copy-start | bytes 1572868
  148.4 7.9 %collective-permute-start.25 = (bf16[192,256]{1,0:T(8,128)(2,1)S(1)}, bf16[192,256]{1,0:T(8,128)(2,1)S(1)}, u32[]{:S(2)}, u32[]{:S(2)}) collective-permute-start(bf16[192,256]{1,0:T(8,128)(2,1)S(1)} %expert.7.refs_0_), channel_id=1, source_target_pairs={{0,1},{1,2},{2,3},{3,0},{4,5},{5,6},{6,7},{7,4},{8,9},{9,10},{10,1... | collective-permute-start | bytes 294920 | tf_op jit(solution)/shard_map/ppermute | solution.py:26
  153.2 5.6 %collective-permute-start.26 = (bf16[192,256]{1,0:T(8,128)(2,1)S(1)}, bf16[192,256]{1,0:T(8,128)(2,1)S(1)}, u32[]{:S(2)}, u32[]{:S(2)}) collective-permute-start(bf16[192,256]{1,0:T(8,128)(2,1)S(1)} %expert.7.refs_0_), channel_id=1, source_target_pairs={{0,2},{1,3},{2,0},{3,1},{4,6},{5,7},{6,4},{7,5},{8,10},{9,11},{10,... | collective-permute-start | bytes 294920 | tf_op jit(solution)/shard_map/ppermute | solution.py:26
  155.5 4.7 %collective-permute-start.27 = (bf16[192,256]{1,0:T(8,128)(2,1)S(1)}, bf16[192,256]{1,0:T(8,128)(2,1)S(1)}, u32[]{:S(2)}, u32[]{:S(2)}) collective-permute-start(bf16[192,256]{1,0:T(8,128)(2,1)S(1)} %expert.7.refs_0_), channel_id=1, source_target_pairs={{0,3},{1,0},{2,1},{3,2},{4,7},{5,4},{6,5},{7,6},{8,11},{9,8},{10,9... | collective-permute-start | bytes 294920 | tf_op jit(solution)/shard_map/ppermute | solution.py:26
  161.6 21.8 %all-to-all-start.2 = ((bf16[64,24,128]{2,1,0:T(8,128)(2,1)}), bf16[64,24,128]{2,1,0:T(8,128)(2,1)S(1)}, u32[]{:S(2)}, u32[]{:S(2)}) async-start(bf16[64,24,128]{2,1,0:T(8,128)(2,1)} %bitcast.14), calls=%async_computation.2 | async-start | bytes 786432 | tf_op jit(solution)/shard_map/all_to_all | solution.py:600
  183.7 4.2 %collective-permute-start.31 = (bf16[24,1024]{1,0:T(8,128)(2,1)S(1)}, bf16[24,1024]{1,0:T(8,128)(2,1)S(1)}, u32[]{:S(2)}, u32[]{:S(2)}) collective-permute-start(bf16[24,1024]{1,0:T(8,128)(2,1)S(1)} %combine.1.refs_0_), channel_id=1, source_target_pairs={{0,1},{1,2},{2,3},{3,0},{4,5},{5,6},{6,7},{7,4},{8,9},{9,10},{10,1... | collective-permute-start | bytes 147464 | tf_op jit(solution)/shard_map/ppermute | solution.py:26
  183.8 5.1 %collective-permute-start.32 = (bf16[24,1024]{1,0:T(8,128)(2,1)S(1)}, bf16[24,1024]{1,0:T(8,128)(2,1)S(1)}, u32[]{:S(2)}, u32[]{:S(2)}) collective-permute-start(bf16[24,1024]{1,0:T(8,128)(2,1)S(1)} %combine.1.refs_0_), channel_id=1, source_target_pairs={{0,2},{1,3},{2,0},{3,1},{4,6},{5,7},{6,4},{7,5},{8,10},{9,11},{10,... | collective-permute-start | bytes 147464 | tf_op jit(solution)/shard_map/ppermute | solution.py:26
  186.6 3.4 %collective-permute-start.33 = (bf16[24,1024]{1,0:T(8,128)(2,1)S(1)}, bf16[24,1024]{1,0:T(8,128)(2,1)S(1)}, u32[]{:S(2)}, u32[]{:S(2)}) collective-permute-start(bf16[24,1024]{1,0:T(8,128)(2,1)S(1)} %combine.1.refs_0_), channel_id=1, source_target_pairs={{0,3},{1,0},{2,1},{3,2},{4,7},{5,4},{6,5},{7,6},{8,11},{9,8},{10,9... | collective-permute-start | bytes 147464 | tf_op jit(solution)/shard_map/ppermute | solution.py:26

commit v4 on v3

--- a/solution.py
+++ b/solution.py
@@ -431,28 +431,53 @@
     )(where, inverse, weight, piece, *before)
 
 
+def fetch_kernel(*refs):
+    count = len(refs) - 2
+    out, sems = refs[count:]
+    rows = refs[0].shape[0]
+    run(
+        [
+            pltpu.make_async_copy(ref, out.at[pl.ds(i * rows, rows)], sems.at[i])
+            for i, ref in enumerate(refs[:count])
+        ]
+    )
+
+
+def fetch(arrays):
+    rows, cols = arrays[0].shape
+    return pl.pallas_call(
+        fetch_kernel,
+        out_shape=shaped((rows * len(arrays), cols), bf16),
+        in_specs=[HBM] * len(arrays),
+        out_specs=VMEM,
+        scratch_shapes=[pltpu.SemaphoreType.DMA((len(arrays),))],
+        cost_estimate=cost(1e6, 4 * len(arrays) * rows * cols),
+        compiler_params=room(4),
+        name="fetch",
+    )(*arrays)
+
+
 def down_kernel(nt, *refs):
-    acts, downs = refs[:nt], refs[nt : 2 * nt]
-    out, wide = refs[2 * nt :]
-    total = jnp.dot(acts[0][...], downs[0][...], preferred_element_type=f32)
-    for s in range(1, nt):
-        total = total + jnp.dot(acts[s][...], downs[s][...], preferred_element_type=f32)
+    acts = refs[:nt]
+    weight, out, wide = refs[nt:]
+    act = jnp.concatenate([ref[...] for ref in acts], axis=1)
+    total = jnp.dot(act, weight[...], preferred_element_type=f32)
     out[...] = put_rows(total, wide)
 
 
-def down_sum(acts, downs):
+def down_sum(acts, weight):
     nt = len(acts)
     slots, units = acts[0].shape
-    part = downs[0].shape[1]
+    part = weight.shape[1]
     wide = slots * part // 128
     return pl.pallas_call(
         functools.partial(down_kernel, nt),
         out_shape=shaped((wide, 128), bf16),
         scratch_shapes=[pltpu.VMEM((wide, 128), f32)],
         cost_estimate=cost(2 * nt * slots * units * part, 2 * nt * units * part),
-        compiler_params=room(10),
+        compiler_params=room(8),
         name="down",
-    )(*acts, *downs)
+    )(*acts, weight)
 
 
 def combine_kernel(rows, weights, stream, out, wide):
@@ -517,10 +542,14 @@
     hits = jnp.arange(slots, dtype=jnp.int32)[None, None, :] == slot_of[:, :, None]
     sender = jnp.sum(hits.astype(f32), axis=1).T.astype(bf16)
     weights = jnp.sum(jnp.where(hits, route_weight[:, :, None], 0.0), axis=1)
+    return sender, weights
+
+
+def three_parts(weights):
     high = to_bf16(weights)
     middle = to_bf16(weights - high)
     low = weights - high - middle
-    return sender, jnp.concatenate([high, middle, low], axis=0).astype(bf16)
+    return jnp.concatenate([high, middle, low], axis=0).astype(bf16)
 
 
 def on_device(
@@ -568,6 +597,7 @@
     gain_of = ffn_gain.astype(f32).reshape(nz, nt, chunk)
     gain_of = jnp.moveaxis(gain_of, 1, 0).reshape(nt, 1, part)
     inverse = 1.0 / gain_of
+    weights = three_parts(weights)
 
     parts = project(where, moved, seqs, own, other)
     arrived = [parts[0]] + [shift(parts[i], Z, i) for i in order_of(nz)]
@@ -588,6 +618,7 @@
     gates = w_gate.reshape(nz, nt, chunk, -1)
     lins = w_lin.reshape(nz, nt, chunk, -1)
     picked = pick(where, gates, lins)
+    fetched = fetch(downs)
     before = ()
     steps = [0] + order_of(nt)[1:] + [nt // 2]
     for s in steps:
@@ -596,7 +627,7 @@
         )
     act = before
     acts = [act] + [shift(act, T, s) for s in range(1, nt)]
-    done = down_sum(acts, downs)
+    done = down_sum(acts, fetched)
     returned = lax.all_to_all(
         done.reshape(n_ep, -1, 128), EP, 0, 0, tiled=True
     ).reshape(-1, 128)

time: 192 us -> 192 us (level)
  no operation moved by 1% of the time
where the time goes in v4:
time: 192 us; the launch traced here: 191 us
  starting transfers between devices  71.9 us (37%)
  waiting for transfers between devices  71.4 us (37%)
  Pallas kernels  22.6 us (12%)
  blocking collectives  19.8 us (10%)
  local copies, waits for them, and re-layouts  4.69 us (2%)
    ppermute x34, starting transfers between devices, shift(): return lax.ppermute(value, axis, [(i, (i + by) % n) for i in range(n)])  56.2 us
    ppermute x34, waiting for transfers between devices, shift(): return lax.ppermute(value, axis, [(i, (i + by) % n) for i in range(n)])  52.7 us
    all_to_all x1, blocking collectives, on_device(): lax.all_to_all(outbound.reshape(n_ep, -1, 128), EP, 0, 0, tiled=True)  19.8 us
    all_to_all x1, waiting for transfers between devices, on_device(): lax.all_to_all(done.reshape(n_ep, -1, 128), EP, 0, 0, tiled=True)  15.1 us
    all_to_all x1, starting transfers between devices, on_device(): moved = lax.all_to_all(payload, Z, 0, 0, tiled=True)  9.02 us
    all_to_all x1, starting transfers between devices, on_device(): lax.all_to_all(done.reshape(n_ep, -1, 128), EP, 0, 0, tiled=True)  6.61 us
    unnamed x27, local copies, waits for them, and re-layouts  4.26 us
    pallas_call x1, Pallas kernels, split(): pl.pallas_call(functools.partial(split_kernel, nz), out_shape=[shaped((ro...  3.92 us
  transfers between devices with their start and end apart: 36, of which 22 were waited for; matrix products, arithmetic and copies ran while one was open for 1% of the time, Pallas kernels for 7%

profile of v4, /device:TPU:1, one launch (start us, length us, event | category | flops | bytes accessed | tf_op | source)
XLA Modules:
  0.0 191.3 jit_solution(17251604593805117419)
XLA Ops:
  0.0 2.0 %scale.1 = (bf16[8,88,512]{2,1,0:T(8,128)(2,1)}, f32[24,128]{1,0:T(8,128)}) custom-call(bf16[24,4096]{1,0:T(8,128)(2,1)} %tokens.1, bf16[4096]{0:T(1024)(128)(2,1)} %gain_at.1, bf16[64,512]{1,0:T(8,128)(2,1)} %bitcast.30), custom_call_target="tpu_custom_call" | custom-call | flops 1000000 | bytes 393216 | tf_op jit(solution)/shard_map/scale/pallas_call | solution.py:106
  2.0 9.0 %all-to-all-start = ((bf16[8,88,512]{2,1,0:T(8,128)(2,1)}), bf16[8,88,512]{2,1,0:T(8,128)(2,1)S(1)}, u32[]{:S(2)}, u32[]{:S(2)}) async-start(bf16[8,88,512]{2,1,0:T(8,128)(2,1)} %get-tuple-element.36), calls=%async_computation | async-start | bytes 1441792 | tf_op jit(solution)/shard_map/all_to_all | solution.py:589
  11.1 1.7 pack.1.refs_0_
  12.7 1.3 collective-permute-start
  14.0 2.5 %collective-permute-start.1 = (bf16[64,1792]{1,0:T(8,128)(2,1)}, bf16[64,1792]{1,0:T(8,128)(2,1)S(1)}, u32[]{:S(2)}, u32[]{:S(2)}) collective-permute-start(bf16[64,1792]{1,0:T(8,128)(2,1)} %pack.1.refs_0_), channel_id=1, source_target_pairs={{0,16},{8,24},{16,0},{24,8},{1,17},{9,25},{17,1},{25,9},{2,18},{10... | collective-permute-start | bytes 688136 | tf_op jit(solution)/shard_map/ppermute | solution.py:26
  16.5 1.2 collective-permute-start.2
  17.6 1.8 collective-permute-start.3
  19.4 1.0 collective-permute-done.refs_1_
  20.4 2.2 %collective-permute-start.4 = (bf16[64,1792]{1,0:T(8,128)(2,1)S(1)}, bf16[64,1792]{1,0:T(8,128)(2,1)S(1)}, u32[]{:S(2)}, u32[]{:S(2)}) collective-permute-start(bf16[64,1792]{1,0:T(8,128)(2,1)S(1)} %collective-permute-done.refs_1_), channel_id=1, source_target_pairs={{0,4},{4,0},{1,5},{5,1},{2,6},{6,2},{3,7},{7,3},{8,12},{12,8},{9,1... | collective-permute-start | bytes 688136 | tf_op jit(solution)/shard_map/ppermute | solution.py:26
  22.7 3.7 %collective-permute-done.1.refs_2_ = bf16[64,1792]{1,0:T(8,128)(2,1)S(1)} collective-permute-done((bf16[64,1792]{1,0:T(8,128)(2,1)}, bf16[64,1792]{1,0:T(8,128)(2,1)S(1)}, u32[]{:S(2)}, u32[]{:S(2)}) %collective-permute-start.1) | collective-permute-done | bytes 229408 | tf_op jit(solution)/shard_map/ppermute | solution.py:26
  26.3 1.8 collective-permute-start.5
  28.3 1.0 collective-permute-done.5.refs_6_
  29.7 3.5 %all-to-all-done.tok = bf16[8,88,512]{2,1,0:T(8,128)(2,1)S(1)} async-done(((bf16[8,88,512]{2,1,0:T(8,128)(2,1)}), bf16[8,88,512]{2,1,0:T(8,128)(2,1)S(1)}, u32[]{:S(2)}, u32[]{:S(2)}) %all-to-all-start) | async-done | bytes 720928 | tf_op jit(solution)/shard_map/all_to_all | solution.py:589
  33.2 0.9 copy-done.2
  34.1 1.2 project.1
  35.4 3.6 %collective-permute-start.11 = (bf16[24,1792]{1,0:T(8,128)(2,1)S(1)}, bf16[24,1792]{1,0:T(8,128)(2,1)S(1)}, u32[]{:S(2)}, u32[]{:S(2)}) collective-permute-start(bf16[24,1792]{1,0:T(8,128)(2,1)S(1)} %get-tuple-element.42), channel_id=1, source_target_pairs={{0,192},{32,224},{64,0},{96,32},{128,64},{160,96},{192,128},{224,1... | collective-permute-start | bytes 258056 | tf_op jit(solution)/shard_map/ppermute | solution.py:26
  39.2 1.3 collective-permute-start.15
  40.5 2.5 %collective-permute-start.16 = (bf16[8,64,512]{2,1,0:T(8,128)(2,1)S(1)}, bf16[8,64,512]{2,1,0:T(8,128)(2,1)S(1)}, u32[]{:S(2)}, u32[]{:S(2)}) collective-permute-start(bf16[8,64,512]{2,1,0:T(8,128)(2,1)S(1)} %slice.36.refs_0_), channel_id=1, source_target_pairs={{0,16},{8,24},{16,0},{24,8},{1,17},{9,25},{17,1},{25,9},{2,18},{10... | collective-permute-start | bytes 1572872 | tf_op jit(solution)/shard_map/ppermute | solution.py:26
  43.0 1.2 collective-permute-start.17
  44.1 2.7 %collective-permute-start.13 = (bf16[24,1792]{1,0:T(8,128)(2,1)S(1)}, bf16[24,1792]{1,0:T(8,128)(2,1)S(1)}, u32[]{:S(2)}, u32[]{:S(2)}) collective-permute-start(bf16[24,1792]{1,0:T(8,128)(2,1)S(1)} %get-tuple-element.44), channel_id=1, source_target_pairs={{0,224},{32,0},{64,32},{96,64},{128,96},{160,128},{192,160},{224,1... | collective-permute-start | bytes 258056 | tf_op jit(solution)/shard_map/ppermute | solution.py:26
  46.8 1.4 collective-permute-start.7
  48.3 0.7 collective-permute-done.13.refs_7_
  49.0 1.6 collective-permute-start.8
  50.7 3.5 %collective-permute-done.7.refs_1_ = bf16[24,1792]{1,0:T(8,128)(2,1)S(1)} collective-permute-done((bf16[24,1792]{1,0:T(8,128)(2,1)S(1)}, bf16[24,1792]{1,0:T(8,128)(2,1)S(1)}, u32[]{:S(2)}, u32[]{:S(2)}) %collective-permute-start.7) | collective-permute-done | bytes 86048 | tf_op jit(solution)/shard_map/ppermute | solution.py:26
  54.3 1.3 collective-permute-done.8.refs_2_
  55.6 4.0 %collective-permute-done.9.refs_3_ = bf16[24,1792]{1,0:T(8,128)(2,1)S(1)} collective-permute-done((bf16[24,1792]{1,0:T(8,128)(2,1)S(1)}, bf16[24,1792]{1,0:T(8,128)(2,1)S(1)}, u32[]{:S(2)}, u32[]{:S(2)}) %collective-permute-start.9) | collective-permute-done | bytes 86048 | tf_op jit(solution)/shard_map/ppermute | solution.py:26
  59.6 3.4 %attend.1.gated = bf16[24,512]{1,0:T(8,128)(2,1)S(1)} custom-call(bf16[24,1792]{1,0:T(8,128)(2,1)S(1)} %get-tuple-element.37.refs_0_, bf16[24,1792]{1,0:T(8,128)(2,1)S(1)} %collective-permute-done.7.refs_1_, bf16[24,1792]{1,0:T(8,128)(2,1)S(1)} %collective-permute-done.8.refs_2_, bf16[24,1792]{1,0:T(8,128)(2,1)S(1)} %collective-permute-done.9.refs_3_, ...), custom_call_target="tpu_custom_call" | custom-call | flops 6291456 | bytes 6291456 | tf_op jit(solution)/shard_map/attend/pallas_call | solution.py:249
  63.0 8.0 %collective-permute-start.14 = (bf16[24,512]{1,0:T(8,128)(2,1)S(1)}, bf16[24,512]{1,0:T(8,128)(2,1)S(1)}, u32[]{:S(2)}, u32[]{:S(2)}) collective-permute-start(bf16[24,512]{1,0:T(8,128)(2,1)S(1)} %attend.1.gated), channel_id=1, source_target_pairs={{0,4},{4,0},{1,5},{5,1},{2,6},{6,2},{3,7},{7,3},{8,12},{12,8},{9,1... | collective-permute-start | bytes 73736 | tf_op jit(solution)/shard_map/ppermute | solution.py:26
  71.8 1.5 mix.1
  73.3 1.5 collective-permute-start.18
  74.8 2.5 %collective-permute-start.19 = (bf16[48,512]{1,0:T(8,128)(2,1)S(1)}, bf16[48,512]{1,0:T(8,128)(2,1)S(1)}, u32[]{:S(2)}, u32[]{:S(2)}) collective-permute-start(bf16[48,512]{1,0:T(8,128)(2,1)S(1)} %get-tuple-element.48), channel_id=1, source_target_pairs={{0,2},{1,3},{2,0},{3,1},{4,6},{5,7},{6,4},{7,5},{8,10},{9,11},{10,... | collective-permute-start | bytes 147464 | tf_op jit(solution)/shard_map/ppermute | solution.py:26
  77.3 1.1 collective-permute-start.20
  78.4 1.2 collective-permute-done.19
  79.6 1.0 collective-permute-done.20
  80.6 1.8 collective-permute-start.21
  82.7 0.6 collective-permute-done.21.other
  83.3 0.9 dispatch.1
  84.3 19.8 %all_to_all.15 = bf16[64,24,128]{2,1,0:T(8,128)(2,1)S(1)} all-to-all(bf16[64,24,128]{2,1,0:T(8,128)(2,1)S(1)} %bitcast.25), channel_id=1, replica_groups=mesh['ep_0'=8,'ep_1'=4,'ep_2'=2,'tp'=4] {'ep_0','ep_1','ep_2'}, dimensions={0} | all-to-all | bytes 786432 | tf_op jit(solution)/shard_map/all_to_all | solution.py:614
  104.1 3.9 %split.1 = (bf16[256,1024]{1,0:T(8,128)(2,1)}, bf16[256,1024]{1,0:T(8,128)(2,1)}, bf16[256,1024]{1,0:T(8,128)(2,1)}, bf16[256,1024]{1,0:T(8,128)(2,1)}) custom-call(s32[4]{0:T(128)} %copy-done.5, bf16[256,4096]{1,0:T(8,128)(2,1)} %bitcast.29), custom_call_target="tpu_custom_call" | custom-call | flops 1000000 | bytes 4194304 | tf_op jit(solution)/shard_map/split/pallas_call | solution.py:147
  108.0 1.0 collective-permute-start.28
  109.0 1.9 collective-permute-start.23
  110.8 2.2 %collective-permute-start.29 = (bf16[256,1024]{1,0:T(8,128)(2,1)}, bf16[256,1024]{1,0:T(8,128)(2,1)S(1)}, u32[]{:S(2)}, u32[]{:S(2)}) collective-permute-start(bf16[256,1024]{1,0:T(8,128)(2,1)} %get-tuple-element.62), channel_id=1, source_target_pairs={{0,2},{1,3},{2,0},{3,1},{4,6},{5,7},{6,4},{7,5},{8,10},{9,11},{10,... | collective-permute-start | bytes 1572872 | tf_op jit(solution)/shard_map/ppermute | solution.py:26
  113.0 0.6 collective-permute-start.30
  113.6 2.1 %collective-permute-done.24.piece = bf16[1536,128]{1,0:T(8,128)(2,1)S(1)} collective-permute-done((bf16[1536,128]{1,0:T(8,128)(2,1)S(1)}, bf16[1536,128]{1,0:T(8,128)(2,1)S(1)}, u32[]{:S(2)}, u32[]{:S(2)}) %collective-permute-start.24) | collective-permute-done | bytes 393248 | tf_op jit(solution)/shard_map/ppermute | solution.py:26
  115.7 1.6 copy-done
  117.3 1.6 copy-done.1
  118.9 1.0 pick.1
  119.9 1.0 expert.4
  120.9 1.0 expert.5
  121.9 1.0 expert.6
  122.9 24.5 %collective-permute-done.22.piece = bf16[1536,128]{1,0:T(8,128)(2,1)S(1)} collective-permute-done((bf16[1536,128]{1,0:T(8,128)(2,1)S(1)}, bf16[1536,128]{1,0:T(8,128)(2,1)S(1)}, u32[]{:S(2)}, u32[]{:S(2)}) %collective-permute-start.22) | collective-permute-done | bytes 393248 | tf_op jit(solution)/shard_map/ppermute | solution.py:26
  147.4 1.0 expert.7.refs_0_
  148.4 4.8 %collective-permute-start.25 = (bf16[192,256]{1,0:T(8,128)(2,1)S(1)}, bf16[192,256]{1,0:T(8,128)(2,1)S(1)}, u32[]{:S(2)}, u32[]{:S(2)}) collective-permute-start(bf16[192,256]{1,0:T(8,128)(2,1)S(1)} %expert.7.refs_0_), channel_id=1, source_target_pairs={{0,1},{1,2},{2,3},{3,0},{4,5},{5,6},{6,7},{7,4},{8,9},{9,10},{10,1... | collective-permute-start | bytes 294920 | tf_op jit(solution)/shard_map/ppermute | solution.py:26
  153.2 2.3 %collective-permute-start.26 = (bf16[192,256]{1,0:T(8,128)(2,1)S(1)}, bf16[192,256]{1,0:T(8,128)(2,1)S(1)}, u32[]{:S(2)}, u32[]{:S(2)}) collective-permute-start(bf16[192,256]{1,0:T(8,128)(2,1)S(1)} %expert.7.refs_0_), channel_id=1, source_target_pairs={{0,2},{1,3},{2,0},{3,1},{4,6},{5,7},{6,4},{7,5},{8,10},{9,11},{10,... | collective-permute-start | bytes 294920 | tf_op jit(solution)/shard_map/ppermute | solution.py:26
  156.3 2.5 %collective-permute-done.26.refs_2_ = bf16[192,256]{1,0:T(8,128)(2,1)S(1)} collective-permute-done((bf16[192,256]{1,0:T(8,128)(2,1)S(1)}, bf16[192,256]{1,0:T(8,128)(2,1)S(1)}, u32[]{:S(2)}, u32[]{:S(2)}) %collective-permute-start.26) | collective-permute-done | bytes 98336 | tf_op jit(solution)/shard_map/ppermute | solution.py:26
  158.8 1.4 collective-permute-done.27.refs_3_
  160.2 1.4 down.1
  161.6 6.6 %all-to-all-start.2 = ((bf16[64,24,128]{2,1,0:T(8,128)(2,1)}), bf16[64,24,128]{2,1,0:T(8,128)(2,1)S(1)}, u32[]{:S(2)}, u32[]{:S(2)}) async-start(bf16[64,24,128]{2,1,0:T(8,128)(2,1)} %bitcast.14), calls=%async_computation.2 | async-start | bytes 786432 | tf_op jit(solution)/shard_map/all_to_all | solution.py:631
  168.2 15.1 %all-to-all-done.2 = bf16[64,24,128]{2,1,0:T(8,128)(2,1)S(1)} async-done(((bf16[64,24,128]{2,1,0:T(8,128)(2,1)}), bf16[64,24,128]{2,1,0:T(8,128)(2,1)S(1)}, u32[]{:S(2)}, u32[]{:S(2)}) %all-to-all-start.2) | async-done | bytes 393248 | tf_op jit(solution)/shard_map/all_to_all | solution.py:631
  183.8 2.8 %collective-permute-start.32 = (bf16[24,1024]{1,0:T(8,128)(2,1)S(1)}, bf16[24,1024]{1,0:T(8,128)(2,1)S(1)}, u32[]{:S(2)}, u32[]{:S(2)}) collective-permute-start(bf16[24,1024]{1,0:T(8,128)(2,1)S(1)} %combine.1.refs_0_), channel_id=1, source_target_pairs={{0,2},{1,3},{2,0},{3,1},{4,6},{5,7},{6,4},{7,5},{8,10},{9,11},{10,... | collective-permute-start | bytes 147464 | tf_op jit(solution)/shard_map/ppermute | solution.py:26
  187.1 0.9 collective-permute-done.31.refs_1_
  187.9 1.0 collective-permute-done.32.refs_2_
  189.0 1.1 collective-permute-done.33.refs_3_
  190.0 1.3 finish.1
  (69 shorter events, 4.0 us)
Async XLA Ops:
  2.0 37.0 %copy-start.11 = (s32[24,4]{0,1:T(4,128)S(1)}, s32[24,4]{0,1:T(4,128)}, u32[]{:S(2)}) copy-start(s32[24,4]{0,1:T(4,128)} %param.32) | copy-start | bytes 1156
  2.0 31.2 %all-to-all-start = ((bf16[8,88,512]{2,1,0:T(8,128)(2,1)}), bf16[8,88,512]{2,1,0:T(8,128)(2,1)S(1)}, u32[]{:S(2)}, u32[]{:S(2)}) async-start(bf16[8,88,512]{2,1,0:T(8,128)(2,1)} %get-tuple-element.36), calls=%async_computation | async-start | bytes 1441792 | tf_op jit(solution)/shard_map/all_to_all | solution.py:589
  11.0 43.2 %copy-start.10 = (bf16[4096]{0:T(1024)(128)(2,1)S(1)}, bf16[4096]{0:T(1024)(128)(2,1)}, u32[]{:S(2)}) copy-start(bf16[4096]{0:T(1024)(128)(2,1)} %param.28) | copy-start | bytes 24580
  11.0 48.6 %copy-start.7 = (f32[24,256]{1,0:T(8,128)S(1)}, f32[24,256]{1,0:T(8,128)}, u32[]{:S(2)}) copy-start(f32[24,256]{1,0:T(8,128)} %refs_9_.1) | copy-start | bytes 73732
  11.0 48.6 %copy-start.8 = (f32[24,128]{1,0:T(8,128)S(1)}, f32[24,128]{1,0:T(8,128)}, u32[]{:S(2)}) copy-start(f32[24,128]{1,0:T(8,128)} %get-tuple-element.45.refs_8_) | copy-start | bytes 36868
  11.0 48.6 %copy-start.9 = (bf16[512]{0:T(512)(128)(2,1)S(1)}, bf16[512]{0:T(512)(128)(2,1)}, u32[]{:S(2)}) copy-start(bf16[512]{0:T(512)(128)(2,1)} %refs_11_.1) | copy-start | bytes 3076
  12.7 7.7 %collective-permute-start = (bf16[64,1792]{1,0:T(8,128)(2,1)}, bf16[64,1792]{1,0:T(8,128)(2,1)S(1)}, u32[]{:S(2)}, u32[]{:S(2)}) collective-permute-start(bf16[64,1792]{1,0:T(8,128)(2,1)} %pack.1.refs_0_), channel_id=1, source_target_pairs={{0,8},{8,16},{16,24},{24,0},{1,9},{9,17},{17,25},{25,1},{2,10},{10... | collective-permute-start | bytes 688136 | tf_op jit(solution)/shard_map/ppermute | solution.py:26
  14.0 12.3 %collective-permute-start.1 = (bf16[64,1792]{1,0:T(8,128)(2,1)}, bf16[64,1792]{1,0:T(8,128)(2,1)S(1)}, u32[]{:S(2)}, u32[]{:S(2)}) collective-permute-start(bf16[64,1792]{1,0:T(8,128)(2,1)} %pack.1.refs_0_), channel_id=1, source_target_pairs={{0,16},{8,24},{16,0},{24,8},{1,17},{9,25},{17,1},{25,9},{2,18},{10... | collective-permute-start | bytes 688136 | tf_op jit(solution)/shard_map/ppermute | solution.py:26
  16.5 11.7 %collective-permute-start.2 = (bf16[64,1792]{1,0:T(8,128)(2,1)}, bf16[64,1792]{1,0:T(8,128)(2,1)S(1)}, u32[]{:S(2)}, u32[]{:S(2)}) collective-permute-start(bf16[64,1792]{1,0:T(8,128)(2,1)} %pack.1.refs_0_), channel_id=1, source_target_pairs={{0,24},{8,0},{16,8},{24,16},{1,25},{9,1},{17,9},{25,17},{2,26},{10... | collective-permute-start | bytes 688136 | tf_op jit(solution)/shard_map/ppermute | solution.py:26
  17.6 10.6 %collective-permute-start.3 = (bf16[64,1792]{1,0:T(8,128)(2,1)}, bf16[64,1792]{1,0:T(8,128)(2,1)S(1)}, u32[]{:S(2)}, u32[]{:S(2)}) collective-permute-start(bf16[64,1792]{1,0:T(8,128)(2,1)} %pack.1.refs_0_), channel_id=1, source_target_pairs={{0,4},{4,0},{1,5},{5,1},{2,6},{6,2},{3,7},{7,3},{8,12},{12,8},{9,1... | collective-permute-start | bytes 688136 | tf_op jit(solution)/shard_map/ppermute | solution.py:26
  20.4 7.8 %collective-permute-start.4 = (bf16[64,1792]{1,0:T(8,128)(2,1)S(1)}, bf16[64,1792]{1,0:T(8,128)(2,1)S(1)}, u32[]{:S(2)}, u32[]{:S(2)}) collective-permute-start(bf16[64,1792]{1,0:T(8,128)(2,1)S(1)} %collective-permute-done.refs_1_), channel_id=1, source_target_pairs={{0,4},{4,0},{1,5},{5,1},{2,6},{6,2},{3,7},{7,3},{8,12},{12,8},{9,1... | collective-permute-start | bytes 688136 | tf_op jit(solution)/shard_map/ppermute | solution.py:26
  26.3 2.9 %collective-permute-start.5 = (bf16[64,1792]{1,0:T(8,128)(2,1)S(1)}, bf16[64,1792]{1,0:T(8,128)(2,1)S(1)}, u32[]{:S(2)}, u32[]{:S(2)}) collective-permute-start(bf16[64,1792]{1,0:T(8,128)(2,1)S(1)} %collective-permute-done.1.refs_2_), channel_id=1, source_target_pairs={{0,4},{4,0},{1,5},{5,1},{2,6},{6,2},{3,7},{7,3},{8,12},{12,8},{9,1... | collective-permute-start | bytes 688136 | tf_op jit(solution)/shard_map/ppermute | solution.py:26
  28.2 1.5 collective-permute-start.6
  28.2 55.1 %copy-start.5 = (s32[4]{0:T(128)}, s32[4]{0:T(128)S(1)}, u32[]{:S(2)}) copy-start(s32[4]{0:T(128)S(1)} %pad_add_fusion.where) | copy-start | bytes 52
  33.2 0.9 copy-start.2
  35.3 7.6 %collective-permute-start.10 = (bf16[24,1792]{1,0:T(8,128)(2,1)S(1)}, bf16[24,1792]{1,0:T(8,128)(2,1)S(1)}, u32[]{:S(2)}, u32[]{:S(2)}) collective-permute-start(bf16[24,1792]{1,0:T(8,128)(2,1)S(1)} %get-tuple-element.41), channel_id=1, source_target_pairs={{0,64},{32,96},{64,128},{96,160},{128,192},{160,224},{192,0},{224,... | collective-permute-start | bytes 258056 | tf_op jit(solution)/shard_map/ppermute | solution.py:26
  35.4 8.7 %collective-permute-start.11 = (bf16[24,1792]{1,0:T(8,128)(2,1)S(1)}, bf16[24,1792]{1,0:T(8,128)(2,1)S(1)}, u32[]{:S(2)}, u32[]{:S(2)}) collective-permute-start(bf16[24,1792]{1,0:T(8,128)(2,1)S(1)} %get-tuple-element.42), channel_id=1, source_target_pairs={{0,192},{32,224},{64,0},{96,32},{128,64},{160,96},{192,128},{224,1... | collective-permute-start | bytes 258056 | tf_op jit(solution)/shard_map/ppermute | solution.py:26
  39.0 7.8 %collective-permute-start.12 = (bf16[24,1792]{1,0:T(8,128)(2,1)S(1)}, bf16[24,1792]{1,0:T(8,128)(2,1)S(1)}, u32[]{:S(2)}, u32[]{:S(2)}) collective-permute-start(bf16[24,1792]{1,0:T(8,128)(2,1)S(1)} %get-tuple-element.43), channel_id=1, source_target_pairs={{0,32},{32,64},{64,96},{96,128},{128,160},{160,192},{192,224},{224... | collective-permute-start | bytes 258056 | tf_op jit(solution)/shard_map/ppermute | solution.py:26
  39.2 32.6 %collective-permute-start.15 = (bf16[8,64,512]{2,1,0:T(8,128)(2,1)S(1)}, bf16[8,64,512]{2,1,0:T(8,128)(2,1)S(1)}, u32[]{:S(2)}, u32[]{:S(2)}) collective-permute-start(bf16[8,64,512]{2,1,0:T(8,128)(2,1)S(1)} %slice.36.refs_0_), channel_id=1, source_target_pairs={{0,8},{8,16},{16,24},{24,0},{1,9},{9,17},{17,25},{25,1},{2,10},{10... | collective-permute-start | bytes 1572872 | tf_op jit(solution)/shard_map/ppermute | solution.py:26
  40.5 31.3 %collective-permute-start.16 = (bf16[8,64,512]{2,1,0:T(8,128)(2,1)S(1)}, bf16[8,64,512]{2,1,0:T(8,128)(2,1)S(1)}, u32[]{:S(2)}, u32[]{:S(2)}) collective-permute-start(bf16[8,64,512]{2,1,0:T(8,128)(2,1)S(1)} %slice.36.refs_0_), channel_id=1, source_target_pairs={{0,16},{8,24},{16,0},{24,8},{1,17},{9,25},{17,1},{25,9},{2,18},{10... | collective-permute-start | bytes 1572872 | tf_op jit(solution)/shard_map/ppermute | solution.py:26
  43.0 28.9 %collective-permute-start.17 = (bf16[8,64,512]{2,1,0:T(8,128)(2,1)S(1)}, bf16[8,64,512]{2,1,0:T(8,128)(2,1)S(1)}, u32[]{:S(2)}, u32[]{:S(2)}) collective-permute-start(bf16[8,64,512]{2,1,0:T(8,128)(2,1)S(1)} %slice.36.refs_0_), channel_id=1, source_target_pairs={{0,24},{8,0},{16,8},{24,16},{1,25},{9,1},{17,9},{25,17},{2,26},{10... | collective-permute-start | bytes 1572872 | tf_op jit(solution)/shard_map/ppermute | solution.py:26
  44.1 4.9 %collective-permute-start.13 = (bf16[24,1792]{1,0:T(8,128)(2,1)S(1)}, bf16[24,1792]{1,0:T(8,128)(2,1)S(1)}, u32[]{:S(2)}, u32[]{:S(2)}) collective-permute-start(bf16[24,1792]{1,0:T(8,128)(2,1)S(1)} %get-tuple-element.44), channel_id=1, source_target_pairs={{0,224},{32,0},{64,32},{96,64},{128,96},{160,128},{192,160},{224,1... | collective-permute-start | bytes 258056 | tf_op jit(solution)/shard_map/ppermute | solution.py:26
  46.8 7.4 %collective-permute-start.7 = (bf16[24,1792]{1,0:T(8,128)(2,1)S(1)}, bf16[24,1792]{1,0:T(8,128)(2,1)S(1)}, u32[]{:S(2)}, u32[]{:S(2)}) collective-permute-start(bf16[24,1792]{1,0:T(8,128)(2,1)S(1)} %get-tuple-element.38), channel_id=1, source_target_pairs={{0,128},{32,160},{64,192},{96,224},{128,0},{160,32},{192,64},{224,... | collective-permute-start | bytes 258056 | tf_op jit(solution)/shard_map/ppermute | solution.py:26
  49.0 6.5 %collective-permute-start.8 = (bf16[24,1792]{1,0:T(8,128)(2,1)S(1)}, bf16[24,1792]{1,0:T(8,128)(2,1)S(1)}, u32[]{:S(2)}, u32[]{:S(2)}) collective-permute-start(bf16[24,1792]{1,0:T(8,128)(2,1)S(1)} %get-tuple-element.39), channel_id=1, source_target_pairs={{0,96},{32,128},{64,160},{96,192},{128,224},{160,0},{192,32},{224,... | collective-permute-start | bytes 258056 | tf_op jit(solution)/shard_map/ppermute | solution.py:26
  54.2 5.4 %collective-permute-start.9 = (bf16[24,1792]{1,0:T(8,128)(2,1)S(1)}, bf16[24,1792]{1,0:T(8,128)(2,1)S(1)}, u32[]{:S(2)}, u32[]{:S(2)}) collective-permute-start(bf16[24,1792]{1,0:T(8,128)(2,1)S(1)} %get-tuple-element.40), channel_id=1, source_target_pairs={{0,160},{32,192},{64,224},{96,0},{128,32},{160,64},{192,96},{224,1... | collective-permute-start | bytes 258056 | tf_op jit(solution)/shard_map/ppermute | solution.py:26
  63.0 19.5 %copy-start.12 = (f32[24,4]{0,1:T(4,128)S(1)}, f32[24,4]{0,1:T(4,128)}, u32[]{:S(2)}) copy-start(f32[24,4]{0,1:T(4,128)} %param.33) | copy-start | bytes 1156
  63.0 20.3 %copy-start.3 = (bf16[24,4096]{1,0:T(8,128)(2,1)S(1)}, bf16[24,4096]{1,0:T(8,128)(2,1)}, u32[]{:S(2)}) copy-start(bf16[24,4096]{1,0:T(8,128)(2,1)} %tokens.1) | copy-start | bytes 589828
  63.0 8.8 %collective-permute-start.14 = (bf16[24,512]{1,0:T(8,128)(2,1)S(1)}, bf16[24,512]{1,0:T(8,128)(2,1)S(1)}, u32[]{:S(2)}, u32[]{:S(2)}) collective-permute-start(bf16[24,512]{1,0:T(8,128)(2,1)S(1)} %attend.1.gated), channel_id=1, source_target_pairs={{0,4},{4,0},{1,5},{5,1},{2,6},{6,2},{3,7},{7,3},{8,12},{12,8},{9,1... | collective-permute-start | bytes 73736 | tf_op jit(solution)/shard_map/ppermute | solution.py:26
  73.3 5.1 %collective-permute-start.18 = (bf16[48,512]{1,0:T(8,128)(2,1)S(1)}, bf16[48,512]{1,0:T(8,128)(2,1)S(1)}, u32[]{:S(2)}, u32[]{:S(2)}) collective-permute-start(bf16[48,512]{1,0:T(8,128)(2,1)S(1)} %get-tuple-element.47), channel_id=1, source_target_pairs={{0,1},{1,2},{2,3},{3,0},{4,5},{5,6},{6,7},{7,4},{8,9},{9,10},{10,1... | collective-permute-start | bytes 147464 | tf_op jit(solution)/shard_map/ppermute | solution.py:26
  74.8 4.8 %collective-permute-start.19 = (bf16[48,512]{1,0:T(8,128)(2,1)S(1)}, bf16[48,512]{1,0:T(8,128)(2,1)S(1)}, u32[]{:S(2)}, u32[]{:S(2)}) collective-permute-start(bf16[48,512]{1,0:T(8,128)(2,1)S(1)} %get-tuple-element.48), channel_id=1, source_target_pairs={{0,2},{1,3},{2,0},{3,1},{4,6},{5,7},{6,4},{7,5},{8,10},{9,11},{10,... | collective-permute-start | bytes 147464 | tf_op jit(solution)/shard_map/ppermute | solution.py:26
  77.3 3.2 %collective-permute-start.20 = (bf16[48,512]{1,0:T(8,128)(2,1)S(1)}, bf16[48,512]{1,0:T(8,128)(2,1)S(1)}, u32[]{:S(2)}, u32[]{:S(2)}) collective-permute-start(bf16[48,512]{1,0:T(8,128)(2,1)S(1)} %get-tuple-element.49), channel_id=1, source_target_pairs={{0,3},{1,0},{2,1},{3,2},{4,7},{5,4},{6,5},{7,6},{8,11},{9,8},{10,9... | collective-permute-start | bytes 147464 | tf_op jit(solution)/shard_map/ppermute | solution.py:26
  80.6 2.7 %collective-permute-start.21 = (bf16[24,512]{1,0:T(8,128)(2,1)S(1)}, bf16[24,512]{1,0:T(8,128)(2,1)S(1)}, u32[]{:S(2)}, u32[]{:S(2)}) collective-permute-start(bf16[24,512]{1,0:T(8,128)(2,1)S(1)} %get-tuple-element.67), channel_id=1, source_target_pairs={{0,4},{4,0},{1,5},{5,1},{2,6},{6,2},{3,7},{7,3},{8,12},{12,8},{9,1... | collective-permute-start | bytes 73736 | tf_op jit(solution)/shard_map/ppermute | solution.py:26
  84.2 31.5 %copy-start.6 = (s32[4]{0:T(128)S(1)}, s32[4]{0:T(128)}, u32[]{:S(2)}) copy-start(s32[4]{0:T(128)} %copy-done.5) | copy-start | bytes 52
  104.1 11.6 %collective-permute-start.24 = (bf16[1536,128]{1,0:T(8,128)(2,1)S(1)}, bf16[1536,128]{1,0:T(8,128)(2,1)S(1)}, u32[]{:S(2)}, u32[]{:S(2)}) collective-permute-start(bf16[1536,128]{1,0:T(8,128)(2,1)S(1)} %bitcast.21), channel_id=1, source_target_pairs={{0,1},{1,2},{2,3},{3,0},{4,5},{5,6},{6,7},{7,4},{8,9},{9,10},{10,1... | collective-permute-start | bytes 1179656 | tf_op jit(solution)/shard_map/ppermute | solution.py:26
  108.0 47.5 %collective-permute-start.28 = (bf16[256,1024]{1,0:T(8,128)(2,1)}, bf16[256,1024]{1,0:T(8,128)(2,1)S(1)}, u32[]{:S(2)}, u32[]{:S(2)}) collective-permute-start(bf16[256,1024]{1,0:T(8,128)(2,1)} %get-tuple-element.61), channel_id=1, source_target_pairs={{0,1},{1,2},{2,3},{3,0},{4,5},{5,6},{6,7},{7,4},{8,9},{9,10},{10,1... | collective-permute-start | bytes 1572872 | tf_op jit(solution)/shard_map/ppermute | solution.py:26
  109.0 12.9 %collective-permute-start.23 = (bf16[1536,128]{1,0:T(8,128)(2,1)S(1)}, bf16[1536,128]{1,0:T(8,128)(2,1)S(1)}, u32[]{:S(2)}, u32[]{:S(2)}) collective-permute-start(bf16[1536,128]{1,0:T(8,128)(2,1)S(1)} %bitcast.22), channel_id=1, source_target_pairs={{0,3},{1,0},{2,1},{3,2},{4,7},{5,4},{6,5},{7,6},{8,11},{9,8},{10,9... | collective-permute-start | bytes 1179656 | tf_op jit(solution)/shard_map/ppermute | solution.py:26
  110.8 44.9 %collective-permute-start.29 = (bf16[256,1024]{1,0:T(8,128)(2,1)}, bf16[256,1024]{1,0:T(8,128)(2,1)S(1)}, u32[]{:S(2)}, u32[]{:S(2)}) collective-permute-start(bf16[256,1024]{1,0:T(8,128)(2,1)} %get-tuple-element.62), channel_id=1, source_target_pairs={{0,2},{1,3},{2,0},{3,1},{4,6},{5,7},{6,4},{7,5},{8,10},{9,11},{10,... | collective-permute-start | bytes 1572872 | tf_op jit(solution)/shard_map/ppermute | solution.py:26
  113.0 42.7 %collective-permute-start.30 = (bf16[256,1024]{1,0:T(8,128)(2,1)}, bf16[256,1024]{1,0:T(8,128)(2,1)S(1)}, u32[]{:S(2)}, u32[]{:S(2)}) collective-permute-start(bf16[256,1024]{1,0:T(8,128)(2,1)} %get-tuple-element.63), channel_id=1, source_target_pairs={{0,3},{1,0},{2,1},{3,2},{4,7},{5,4},{6,5},{7,6},{8,11},{9,8},{10,9... | collective-permute-start | bytes 1572872 | tf_op jit(solution)/shard_map/ppermute | solution.py:26
  115.7 31.7 %collective-permute-start.22 = (bf16[1536,128]{1,0:T(8,128)(2,1)S(1)}, bf16[1536,128]{1,0:T(8,128)(2,1)S(1)}, u32[]{:S(2)}, u32[]{:S(2)}) collective-permute-start(bf16[1536,128]{1,0:T(8,128)(2,1)S(1)} %bitcast.23), channel_id=1, source_target_pairs={{0,2},{1,3},{2,0},{3,1},{4,6},{5,7},{6,4},{7,5},{8,10},{9,11},{10,... | collective-permute-start | bytes 1179656 | tf_op jit(solution)/shard_map/ppermute | solution.py:26
  115.7 1.6 copy-start
  117.3 1.6 copy-start.1
  121.9 33.8 %copy-start.4 = (bf16[256,1024]{1,0:T(8,128)(2,1)S(1)}, bf16[256,1024]{1,0:T(8,128)(2,1)}, u32[]{:S(2)}) copy-start(bf16[256,1024]{1,0:T(8,128)(2,1)} %get-tuple-element.60.refs_0_) | copy-start | bytes 1572868
  148.4 7.9 %collective-permute-start.25 = (bf16[192,256]{1,0:T(8,128)(2,1)S(1)}, bf16[192,256]{1,0:T(8,128)(2,1)S(1)}, u32[]{:S(2)}, u32[]{:S(2)}) collective-permute-start(bf16[192,256]{1,0:T(8,128)(2,1)S(1)} %expert.7.refs_0_), channel_id=1, source_target_pairs={{0,1},{1,2},{2,3},{3,0},{4,5},{5,6},{6,7},{7,4},{8,9},{9,10},{10,1... | collective-permute-start | bytes 294920 | tf_op jit(solution)/shard_map/ppermute | solution.py:26
  153.2 5.6 %collective-permute-start.26 = (bf16[192,256]{1,0:T(8,128)(2,1)S(1)}, bf16[192,256]{1,0:T(8,128)(2,1)S(1)}, u32[]{:S(2)}, u32[]{:S(2)}) collective-permute-start(bf16[192,256]{1,0:T(8,128)(2,1)S(1)} %expert.7.refs_0_), channel_id=1, source_target_pairs={{0,2},{1,3},{2,0},{3,1},{4,6},{5,7},{6,4},{7,5},{8,10},{9,11},{10,... | collective-permute-start | bytes 294920 | tf_op jit(solution)/shard_map/ppermute | solution.py:26
  155.5 4.7 %collective-permute-start.27 = (bf16[192,256]{1,0:T(8,128)(2,1)S(1)}, bf16[192,256]{1,0:T(8,128)(2,1)S(1)}, u32[]{:S(2)}, u32[]{:S(2)}) collective-permute-start(bf16[192,256]{1,0:T(8,128)(2,1)S(1)} %expert.7.refs_0_), channel_id=1, source_target_pairs={{0,3},{1,0},{2,1},{3,2},{4,7},{5,4},{6,5},{7,6},{8,11},{9,8},{10,9... | collective-permute-start | bytes 294920 | tf_op jit(solution)/shard_map/ppermute | solution.py:26
  161.6 21.8 %all-to-all-start.2 = ((bf16[64,24,128]{2,1,0:T(8,128)(2,1)}), bf16[64,24,128]{2,1,0:T(8,128)(2,1)S(1)}, u32[]{:S(2)}, u32[]{:S(2)}) async-start(bf16[64,24,128]{2,1,0:T(8,128)(2,1)} %bitcast.14), calls=%async_computation.2 | async-start | bytes 786432 | tf_op jit(solution)/shard_map/all_to_all | solution.py:631
  183.7 4.2 %collective-permute-start.31 = (bf16[24,1024]{1,0:T(8,128)(2,1)S(1)}, bf16[24,1024]{1,0:T(8,128)(2,1)S(1)}, u32[]{:S(2)}, u32[]{:S(2)}) collective-permute-start(bf16[24,1024]{1,0:T(8,128)(2,1)S(1)} %combine.1.refs_0_), channel_id=1, source_target_pairs={{0,1},{1,2},{2,3},{3,0},{4,5},{5,6},{6,7},{7,4},{8,9},{9,10},{10,1... | collective-permute-start | bytes 147464 | tf_op jit(solution)/shard_map/ppermute | solution.py:26
  183.8 5.1 %collective-permute-start.32 = (bf16[24,1024]{1,0:T(8,128)(2,1)S(1)}, bf16[24,1024]{1,0:T(8,128)(2,1)S(1)}, u32[]{:S(2)}, u32[]{:S(2)}) collective-permute-start(bf16[24,1024]{1,0:T(8,128)(2,1)S(1)} %combine.1.refs_0_), channel_id=1, source_target_pairs={{0,2},{1,3},{2,0},{3,1},{4,6},{5,7},{6,4},{7,5},{8,10},{9,11},{10,... | collective-permute-start | bytes 147464 | tf_op jit(solution)/shard_map/ppermute | solution.py:26
  186.6 3.4 %collective-permute-start.33 = (bf16[24,1024]{1,0:T(8,128)(2,1)S(1)}, bf16[24,1024]{1,0:T(8,128)(2,1)S(1)}, u32[]{:S(2)}, u32[]{:S(2)}) collective-permute-start(bf16[24,1024]{1,0:T(8,128)(2,1)S(1)} %combine.1.refs_0_), channel_id=1, source_target_pairs={{0,3},{1,0},{2,1},{3,2},{4,7},{5,4},{6,5},{7,6},{8,11},{9,8},{10,9... | collective-permute-start | bytes 147464 | tf_op jit(solution)/shard_map/ppermute | solution.py:26

commit v5 on v4

--- a/solution.py
+++ b/solution.py
@@ -588,7 +588,9 @@
     payload, first_scale = scale(tokens, norm_gain, w_out.T, nz)
     moved = lax.all_to_all(payload, Z, 0, 0, tiled=True)
     out_z = moved[:, seqs:]
-    blocks = [out_z] + [shift(out_z, X, i) for i in range(1, nx)]
+    blocks = [out_z] + [None] * (nx - 1)
+    for i in range(1, nx):
+        blocks[i] = shift(out_z, X, i)
 
     downs = split(where, w_down[0], nz, nt)
     downs = [downs[0]] + [shift(downs[s], T, s) for s in range(1, nt)]
@@ -600,7 +602,9 @@
     weights = three_parts(weights)
 
     parts = project(where, moved, seqs, own, other)
-    arrived = [parts[0]] + [shift(parts[i], Z, i) for i in order_of(nz)]
+    arrived = [parts[0]]
+    for i in order_of(nz):
+        arrived.append(shift(parts[i], Z, i))
     gated = attend(arrived, first_scale, decay_shift, state, head_gain)
     partner = shift(gated, C, 1)
     mixed = mix(where, gated, partner, blocks)

time: 192 us -> 192 us (level)
  no operation moved by 1% of the time
where the time goes in v5:
time: 192 us; the launch traced here: 191 us
  starting transfers between devices  71.9 us (37%)
  waiting for transfers between devices  71.4 us (37%)
  Pallas kernels  22.6 us (12%)
  blocking collectives  19.8 us (10%)
  local copies, waits for them, and re-layouts  4.69 us (2%)
    ppermute x34, starting transfers between devices, shift(): return lax.ppermute(value, axis, [(i, (i + by) % n) for i in range(n)])  56.2 us
    ppermute x34, waiting for transfers between devices, shift(): return lax.ppermute(value, axis, [(i, (i + by) % n) for i in range(n)])  52.7 us
    all_to_all x1, blocking collectives, on_device(): lax.all_to_all(outbound.reshape(n_ep, -1, 128), EP, 0, 0, tiled=True)  19.8 us
    all_to_all x1, waiting for transfers between devices, on_device(): lax.all_to_all(done.reshape(n_ep, -1, 128), EP, 0, 0, tiled=True)  15.1 us
    all_to_all x1, starting transfers between devices, on_device(): moved = lax.all_to_all(payload, Z, 0, 0, tiled=True)  9.02 us
    all_to_all x1, starting transfers between devices, on_device(): lax.all_to_all(done.reshape(n_ep, -1, 128), EP, 0, 0, tiled=True)  6.61 us
    unnamed x27, local copies, waits for them, and re-layouts  4.26 us
    pallas_call x1, Pallas kernels, split(): pl.pallas_call(functools.partial(split_kernel, nz), out_shape=[shaped((ro...  3.92 us
  transfers between devices with their start and end apart: 36, of which 22 were waited for; matrix products, arithmetic and copies ran while one was open for 1% of the time, Pallas kernels for 7%

profile of v5, /device:TPU:1, one launch (start us, length us, event | category | flops | bytes accessed | tf_op | source)
XLA Modules:
  0.0 191.3 jit_solution(17251604593805117419)
XLA Ops:
  0.0 2.0 %scale.1 = (bf16[8,88,512]{2,1,0:T(8,128)(2,1)}, f32[24,128]{1,0:T(8,128)}) custom-call(bf16[24,4096]{1,0:T(8,128)(2,1)} %tokens.1, bf16[4096]{0:T(1024)(128)(2,1)} %gain_at.1, bf16[64,512]{1,0:T(8,128)(2,1)} %bitcast.30), custom_call_target="tpu_custom_call" | custom-call | flops 1000000 | bytes 393216 | tf_op jit(solution)/shard_map/scale/pallas_call | solution.py:106
  2.0 9.0 %all-to-all-start = ((bf16[8,88,512]{2,1,0:T(8,128)(2,1)}), bf16[8,88,512]{2,1,0:T(8,128)(2,1)S(1)}, u32[]{:S(2)}, u32[]{:S(2)}) async-start(bf16[8,88,512]{2,1,0:T(8,128)(2,1)} %get-tuple-element.36), calls=%async_computation | async-start | bytes 1441792 | tf_op jit(solution)/shard_map/all_to_all | solution.py:589
  11.1 1.7 pack.1.refs_0_
  12.7 1.3 collective-permute-start
  14.0 2.5 %collective-permute-start.1 = (bf16[64,1792]{1,0:T(8,128)(2,1)}, bf16[64,1792]{1,0:T(8,128)(2,1)S(1)}, u32[]{:S(2)}, u32[]{:S(2)}) collective-permute-start(bf16[64,1792]{1,0:T(8,128)(2,1)} %pack.1.refs_0_), channel_id=1, source_target_pairs={{0,16},{8,24},{16,0},{24,8},{1,17},{9,25},{17,1},{25,9},{2,18},{10... | collective-permute-start | bytes 688136 | tf_op jit(solution)/shard_map/ppermute | solution.py:26
  16.5 1.2 collective-permute-start.2
  17.6 1.8 collective-permute-start.3
  19.4 1.0 collective-permute-done.refs_1_
  20.4 2.2 %collective-permute-start.4 = (bf16[64,1792]{1,0:T(8,128)(2,1)S(1)}, bf16[64,1792]{1,0:T(8,128)(2,1)S(1)}, u32[]{:S(2)}, u32[]{:S(2)}) collective-permute-start(bf16[64,1792]{1,0:T(8,128)(2,1)S(1)} %collective-permute-done.refs_1_), channel_id=1, source_target_pairs={{0,4},{4,0},{1,5},{5,1},{2,6},{6,2},{3,7},{7,3},{8,12},{12,8},{9,1... | collective-permute-start | bytes 688136 | tf_op jit(solution)/shard_map/ppermute | solution.py:26
  22.7 3.7 %collective-permute-done.1.refs_2_ = bf16[64,1792]{1,0:T(8,128)(2,1)S(1)} collective-permute-done((bf16[64,1792]{1,0:T(8,128)(2,1)}, bf16[64,1792]{1,0:T(8,128)(2,1)S(1)}, u32[]{:S(2)}, u32[]{:S(2)}) %collective-permute-start.1) | collective-permute-done | bytes 229408 | tf_op jit(solution)/shard_map/ppermute | solution.py:26
  26.3 1.8 collective-permute-start.5
  28.3 1.0 collective-permute-done.5.refs_6_
  29.7 3.5 %all-to-all-done.tok = bf16[8,88,512]{2,1,0:T(8,128)(2,1)S(1)} async-done(((bf16[8,88,512]{2,1,0:T(8,128)(2,1)}), bf16[8,88,512]{2,1,0:T(8,128)(2,1)S(1)}, u32[]{:S(2)}, u32[]{:S(2)}) %all-to-all-start) | async-done | bytes 720928 | tf_op jit(solution)/shard_map/all_to_all | solution.py:589
  33.2 0.9 copy-done.2
  34.1 1.2 project.1
  35.4 3.6 %collective-permute-start.11 = (bf16[24,1792]{1,0:T(8,128)(2,1)S(1)}, bf16[24,1792]{1,0:T(8,128)(2,1)S(1)}, u32[]{:S(2)}, u32[]{:S(2)}) collective-permute-start(bf16[24,1792]{1,0:T(8,128)(2,1)S(1)} %get-tuple-element.42), channel_id=1, source_target_pairs={{0,192},{32,224},{64,0},{96,32},{128,64},{160,96},{192,128},{224,1... | collective-permute-start | bytes 258056 | tf_op jit(solution)/shard_map/ppermute | solution.py:26
  39.2 1.3 collective-permute-start.15
  40.5 2.5 %collective-permute-start.16 = (bf16[8,64,512]{2,1,0:T(8,128)(2,1)S(1)}, bf16[8,64,512]{2,1,0:T(8,128)(2,1)S(1)}, u32[]{:S(2)}, u32[]{:S(2)}) collective-permute-start(bf16[8,64,512]{2,1,0:T(8,128)(2,1)S(1)} %slice.36.refs_0_), channel_id=1, source_target_pairs={{0,16},{8,24},{16,0},{24,8},{1,17},{9,25},{17,1},{25,9},{2,18},{10... | collective-permute-start | bytes 1572872 | tf_op jit(solution)/shard_map/ppermute | solution.py:26
  43.0 1.2 collective-permute-start.17
  44.1 2.7 %collective-permute-start.13 = (bf16[24,1792]{1,0:T(8,128)(2,1)S(1)}, bf16[24,1792]{1,0:T(8,128)(2,1)S(1)}, u32[]{:S(2)}, u32[]{:S(2)}) collective-permute-start(bf16[24,1792]{1,0:T(8,128)(2,1)S(1)} %get-tuple-element.44), channel_id=1, source_target_pairs={{0,224},{32,0},{64,32},{96,64},{128,96},{160,128},{192,160},{224,1... | collective-permute-start | bytes 258056 | tf_op jit(solution)/shard_map/ppermute | solution.py:26
  46.8 1.4 collective-permute-start.7
  48.3 0.7 collective-permute-done.13.refs_7_
  49.0 1.6 collective-permute-start.8
  50.7 3.5 %collective-permute-done.7.refs_1_ = bf16[24,1792]{1,0:T(8,128)(2,1)S(1)} collective-permute-done((bf16[24,1792]{1,0:T(8,128)(2,1)S(1)}, bf16[24,1792]{1,0:T(8,128)(2,1)S(1)}, u32[]{:S(2)}, u32[]{:S(2)}) %collective-permute-start.7) | collective-permute-done | bytes 86048 | tf_op jit(solution)/shard_map/ppermute | solution.py:26
  54.3 1.3 collective-permute-done.8.refs_2_
  55.6 4.0 %collective-permute-done.9.refs_3_ = bf16[24,1792]{1,0:T(8,128)(2,1)S(1)} collective-permute-done((bf16[24,1792]{1,0:T(8,128)(2,1)S(1)}, bf16[24,1792]{1,0:T(8,128)(2,1)S(1)}, u32[]{:S(2)}, u32[]{:S(2)}) %collective-permute-start.9) | collective-permute-done | bytes 86048 | tf_op jit(solution)/shard_map/ppermute | solution.py:26
  59.6 3.4 %attend.1.gated = bf16[24,512]{1,0:T(8,128)(2,1)S(1)} custom-call(bf16[24,1792]{1,0:T(8,128)(2,1)S(1)} %get-tuple-element.37.refs_0_, bf16[24,1792]{1,0:T(8,128)(2,1)S(1)} %collective-permute-done.7.refs_1_, bf16[24,1792]{1,0:T(8,128)(2,1)S(1)} %collective-permute-done.8.refs_2_, bf16[24,1792]{1,0:T(8,128)(2,1)S(1)} %collective-permute-done.9.refs_3_, ...), custom_call_target="tpu_custom_call" | custom-call | flops 6291456 | bytes 6291456 | tf_op jit(solution)/shard_map/attend/pallas_call | solution.py:249
  63.0 8.0 %collective-permute-start.14 = (bf16[24,512]{1,0:T(8,128)(2,1)S(1)}, bf16[24,512]{1,0:T(8,128)(2,1)S(1)}, u32[]{:S(2)}, u32[]{:S(2)}) collective-permute-start(bf16[24,512]{1,0:T(8,128)(2,1)S(1)} %attend.1.gated), channel_id=1, source_target_pairs={{0,4},{4,0},{1,5},{5,1},{2,6},{6,2},{3,7},{7,3},{8,12},{12,8},{9,1... | collective-permute-start | bytes 73736 | tf_op jit(solution)/shard_map/ppermute | solution.py:26
  71.8 1.5 mix.1
  73.3 1.5 collective-permute-start.18
  74.8 2.5 %collective-permute-start.19 = (bf16[48,512]{1,0:T(8,128)(2,1)S(1)}, bf16[48,512]{1,0:T(8,128)(2,1)S(1)}, u32[]{:S(2)}, u32[]{:S(2)}) collective-permute-start(bf16[48,512]{1,0:T(8,128)(2,1)S(1)} %get-tuple-element.48), channel_id=1, source_target_pairs={{0,2},{1,3},{2,0},{3,1},{4,6},{5,7},{6,4},{7,5},{8,10},{9,11},{10,... | collective-permute-start | bytes 147464 | tf_op jit(solution)/shard_map/ppermute | solution.py:26
  77.3 1.1 collective-permute-start.20
  78.4 1.2 collective-permute-done.19
  79.6 1.0 collective-permute-done.20
  80.6 1.8 collective-permute-start.21
  82.7 0.6 collective-permute-done.21.other
  83.3 0.9 dispatch.1
  84.3 19.8 %all_to_all.15 = bf16[64,24,128]{2,1,0:T(8,128)(2,1)S(1)} all-to-all(bf16[64,24,128]{2,1,0:T(8,128)(2,1)S(1)} %bitcast.25), channel_id=1, replica_groups=mesh['ep_0'=8,'ep_1'=4,'ep_2'=2,'tp'=4] {'ep_0','ep_1','ep_2'}, dimensions={0} | all-to-all | bytes 786432 | tf_op jit(solution)/shard_map/all_to_all | solution.py:618
  104.1 3.9 %split.1 = (bf16[256,1024]{1,0:T(8,128)(2,1)}, bf16[256,1024]{1,0:T(8,128)(2,1)}, bf16[256,1024]{1,0:T(8,128)(2,1)}, bf16[256,1024]{1,0:T(8,128)(2,1)}) custom-call(s32[4]{0:T(128)} %copy-done.5, bf16[256,4096]{1,0:T(8,128)(2,1)} %bitcast.29), custom_call_target="tpu_custom_call" | custom-call | flops 1000000 | bytes 4194304 | tf_op jit(solution)/shard_map/split/pallas_call | solution.py:147
  108.0 1.0 collective-permute-start.28
  109.0 1.9 collective-permute-start.23
  110.8 2.2 %collective-permute-start.29 = (bf16[256,1024]{1,0:T(8,128)(2,1)}, bf16[256,1024]{1,0:T(8,128)(2,1)S(1)}, u32[]{:S(2)}, u32[]{:S(2)}) collective-permute-start(bf16[256,1024]{1,0:T(8,128)(2,1)} %get-tuple-element.62), channel_id=1, source_target_pairs={{0,2},{1,3},{2,0},{3,1},{4,6},{5,7},{6,4},{7,5},{8,10},{9,11},{10,... | collective-permute-start | bytes 1572872 | tf_op jit(solution)/shard_map/ppermute | solution.py:26
  113.0 0.6 collective-permute-start.30
  113.6 2.1 %collective-permute-done.24.piece = bf16[1536,128]{1,0:T(8,128)(2,1)S(1)} collective-permute-done((bf16[1536,128]{1,0:T(8,128)(2,1)S(1)}, bf16[1536,128]{1,0:T(8,128)(2,1)S(1)}, u32[]{:S(2)}, u32[]{:S(2)}) %collective-permute-start.24) | collective-permute-done | bytes 393248 | tf_op jit(solution)/shard_map/ppermute | solution.py:26
  115.7 1.6 copy-done
  117.3 1.6 copy-done.1
  118.9 1.0 pick.1
  119.9 1.0 expert.4
  120.9 1.0 expert.5
  121.9 1.0 expert.6
  122.9 24.5 %collective-permute-done.22.piece = bf16[1536,128]{1,0:T(8,128)(2,1)S(1)} collective-permute-done((bf16[1536,128]{1,0:T(8,128)(2,1)S(1)}, bf16[1536,128]{1,0:T(8,128)(2,1)S(1)}, u32[]{:S(2)}, u32[]{:S(2)}) %collective-permute-start.22) | collective-permute-done | bytes 393248 | tf_op jit(solution)/shard_map/ppermute | solution.py:26
  147.4 1.0 expert.7.refs_0_
  148.4 4.8 %collective-permute-start.25 = (bf16[192,256]{1,0:T(8,128)(2,1)S(1)}, bf16[192,256]{1,0:T(8,128)(2,1)S(1)}, u32[]{:S(2)}, u32[]{:S(2)}) collective-permute-start(bf16[192,256]{1,0:T(8,128)(2,1)S(1)} %expert.7.refs_0_), channel_id=1, source_target_pairs={{0,1},{1,2},{2,3},{3,0},{4,5},{5,6},{6,7},{7,4},{8,9},{9,10},{10,1... | collective-permute-start | bytes 294920 | tf_op jit(solution)/shard_map/ppermute | solution.py:26
  153.2 2.3 %collective-permute-start.26 = (bf16[192,256]{1,0:T(8,128)(2,1)S(1)}, bf16[192,256]{1,0:T(8,128)(2,1)S(1)}, u32[]{:S(2)}, u32[]{:S(2)}) collective-permute-start(bf16[192,256]{1,0:T(8,128)(2,1)S(1)} %expert.7.refs_0_), channel_id=1, source_target_pairs={{0,2},{1,3},{2,0},{3,1},{4,6},{5,7},{6,4},{7,5},{8,10},{9,11},{10,... | collective-permute-start | bytes 294920 | tf_op jit(solution)/shard_map/ppermute | solution.py:26
  156.3 2.5 %collective-permute-done.26.refs_2_ = bf16[192,256]{1,0:T(8,128)(2,1)S(1)} collective-permute-done((bf16[192,256]{1,0:T(8,128)(2,1)S(1)}, bf16[192,256]{1,0:T(8,128)(2,1)S(1)}, u32[]{:S(2)}, u32[]{:S(2)}) %collective-permute-start.26) | collective-permute-done | bytes 98336 | tf_op jit(solution)/shard_map/ppermute | solution.py:26
  158.8 1.4 collective-permute-done.27.refs_3_
  160.2 1.4 down.1
  161.6 6.6 %all-to-all-start.2 = ((bf16[64,24,128]{2,1,0:T(8,128)(2,1)}), bf16[64,24,128]{2,1,0:T(8,128)(2,1)S(1)}, u32[]{:S(2)}, u32[]{:S(2)}) async-start(bf16[64,24,128]{2,1,0:T(8,128)(2,1)} %bitcast.14), calls=%async_computation.2 | async-start | bytes 786432 | tf_op jit(solution)/shard_map/all_to_all | solution.py:635
  168.2 15.1 %all-to-all-done.2 = bf16[64,24,128]{2,1,0:T(8,128)(2,1)S(1)} async-done(((bf16[64,24,128]{2,1,0:T(8,128)(2,1)}), bf16[64,24,128]{2,1,0:T(8,128)(2,1)S(1)}, u32[]{:S(2)}, u32[]{:S(2)}) %all-to-all-start.2) | async-done | bytes 393248 | tf_op jit(solution)/shard_map/all_to_all | solution.py:635
  183.8 2.8 %collective-permute-start.32 = (bf16[24,1024]{1,0:T(8,128)(2,1)S(1)}, bf16[24,1024]{1,0:T(8,128)(2,1)S(1)}, u32[]{:S(2)}, u32[]{:S(2)}) collective-permute-start(bf16[24,1024]{1,0:T(8,128)(2,1)S(1)} %combine.1.refs_0_), channel_id=1, source_target_pairs={{0,2},{1,3},{2,0},{3,1},{4,6},{5,7},{6,4},{7,5},{8,10},{9,11},{10,... | collective-permute-start | bytes 147464 | tf_op jit(solution)/shard_map/ppermute | solution.py:26
  187.1 0.9 collective-permute-done.31.refs_1_
  187.9 1.0 collective-permute-done.32.refs_2_
  189.0 1.1 collective-permute-done.33.refs_3_
  190.0 1.3 finish.1
  (69 shorter events, 4.0 us)
Async XLA Ops:
  2.0 37.0 %copy-start.11 = (s32[24,4]{0,1:T(4,128)S(1)}, s32[24,4]{0,1:T(4,128)}, u32[]{:S(2)}) copy-start(s32[24,4]{0,1:T(4,128)} %param.32) | copy-start | bytes 1156
  2.0 31.2 %all-to-all-start = ((bf16[8,88,512]{2,1,0:T(8,128)(2,1)}), bf16[8,88,512]{2,1,0:T(8,128)(2,1)S(1)}, u32[]{:S(2)}, u32[]{:S(2)}) async-start(bf16[8,88,512]{2,1,0:T(8,128)(2,1)} %get-tuple-element.36), calls=%async_computation | async-start | bytes 1441792 | tf_op jit(solution)/shard_map/all_to_all | solution.py:589
  11.0 43.2 %copy-start.10 = (bf16[4096]{0:T(1024)(128)(2,1)S(1)}, bf16[4096]{0:T(1024)(128)(2,1)}, u32[]{:S(2)}) copy-start(bf16[4096]{0:T(1024)(128)(2,1)} %param.28) | copy-start | bytes 24580
  11.0 48.6 %copy-start.7 = (f32[24,256]{1,0:T(8,128)S(1)}, f32[24,256]{1,0:T(8,128)}, u32[]{:S(2)}) copy-start(f32[24,256]{1,0:T(8,128)} %refs_9_.1) | copy-start | bytes 73732
  11.0 48.6 %copy-start.8 = (f32[24,128]{1,0:T(8,128)S(1)}, f32[24,128]{1,0:T(8,128)}, u32[]{:S(2)}) copy-start(f32[24,128]{1,0:T(8,128)} %get-tuple-element.45.refs_8_) | copy-start | bytes 36868
  11.0 48.6 %copy-start.9 = (bf16[512]{0:T(512)(128)(2,1)S(1)}, bf16[512]{0:T(512)(128)(2,1)}, u32[]{:S(2)}) copy-start(bf16[512]{0:T(512)(128)(2,1)} %refs_11_.1) | copy-start | bytes 3076
  12.7 7.7 %collective-permute-start = (bf16[64,1792]{1,0:T(8,128)(2,1)}, bf16[64,1792]{1,0:T(8,128)(2,1)S(1)}, u32[]{:S(2)}, u32[]{:S(2)}) collective-permute-start(bf16[64,1792]{1,0:T(8,128)(2,1)} %pack.1.refs_0_), channel_id=1, source_target_pairs={{0,8},{8,16},{16,24},{24,0},{1,9},{9,17},{17,25},{25,1},{2,10},{10... | collective-permute-start | bytes 688136 | tf_op jit(solution)/shard_map/ppermute | solution.py:26
  14.0 12.3 %collective-permute-start.1 = (bf16[64,1792]{1,0:T(8,128)(2,1)}, bf16[64,1792]{1,0:T(8,128)(2,1)S(1)}, u32[]{:S(2)}, u32[]{:S(2)}) collective-permute-start(bf16[64,1792]{1,0:T(8,128)(2,1)} %pack.1.refs_0_), channel_id=1, source_target_pairs={{0,16},{8,24},{16,0},{24,8},{1,17},{9,25},{17,1},{25,9},{2,18},{10... | collective-permute-start | bytes 688136 | tf_op jit(solution)/shard_map/ppermute | solution.py:26
  16.5 11.7 %collective-permute-start.2 = (bf16[64,1792]{1,0:T(8,128)(2,1)}, bf16[64,1792]{1,0:T(8,128)(2,1)S(1)}, u32[]{:S(2)}, u32[]{:S(2)}) collective-permute-start(bf16[64,1792]{1,0:T(8,128)(2,1)} %pack.1.refs_0_), channel_id=1, source_target_pairs={{0,24},{8,0},{16,8},{24,16},{1,25},{9,1},{17,9},{25,17},{2,26},{10... | collective-permute-start | bytes 688136 | tf_op jit(solution)/shard_map/ppermute | solution.py:26
  17.6 10.6 %collective-permute-start.3 = (bf16[64,1792]{1,0:T(8,128)(2,1)}, bf16[64,1792]{1,0:T(8,128)(2,1)S(1)}, u32[]{:S(2)}, u32[]{:S(2)}) collective-permute-start(bf16[64,1792]{1,0:T(8,128)(2,1)} %pack.1.refs_0_), channel_id=1, source_target_pairs={{0,4},{4,0},{1,5},{5,1},{2,6},{6,2},{3,7},{7,3},{8,12},{12,8},{9,1... | collective-permute-start | bytes 688136 | tf_op jit(solution)/shard_map/ppermute | solution.py:26
  20.4 7.8 %collective-permute-start.4 = (bf16[64,1792]{1,0:T(8,128)(2,1)S(1)}, bf16[64,1792]{1,0:T(8,128)(2,1)S(1)}, u32[]{:S(2)}, u32[]{:S(2)}) collective-permute-start(bf16[64,1792]{1,0:T(8,128)(2,1)S(1)} %collective-permute-done.refs_1_), channel_id=1, source_target_pairs={{0,4},{4,0},{1,5},{5,1},{2,6},{6,2},{3,7},{7,3},{8,12},{12,8},{9,1... | collective-permute-start | bytes 688136 | tf_op jit(solution)/shard_map/ppermute | solution.py:26
  26.3 2.9 %collective-permute-start.5 = (bf16[64,1792]{1,0:T(8,128)(2,1)S(1)}, bf16[64,1792]{1,0:T(8,128)(2,1)S(1)}, u32[]{:S(2)}, u32[]{:S(2)}) collective-permute-start(bf16[64,1792]{1,0:T(8,128)(2,1)S(1)} %collective-permute-done.1.refs_2_), channel_id=1, source_target_pairs={{0,4},{4,0},{1,5},{5,1},{2,6},{6,2},{3,7},{7,3},{8,12},{12,8},{9,1... | collective-permute-start | bytes 688136 | tf_op jit(solution)/shard_map/ppermute | solution.py:26
  28.2 1.5 collective-permute-start.6
  28.2 55.1 %copy-start.5 = (s32[4]{0:T(128)}, s32[4]{0:T(128)S(1)}, u32[]{:S(2)}) copy-start(s32[4]{0:T(128)S(1)} %pad_add_fusion.where) | copy-start | bytes 52
  33.2 0.9 copy-start.2
  35.3 7.6 %collective-permute-start.10 = (bf16[24,1792]{1,0:T(8,128)(2,1)S(1)}, bf16[24,1792]{1,0:T(8,128)(2,1)S(1)}, u32[]{:S(2)}, u32[]{:S(2)}) collective-permute-start(bf16[24,1792]{1,0:T(8,128)(2,1)S(1)} %get-tuple-element.41), channel_id=1, source_target_pairs={{0,64},{32,96},{64,128},{96,160},{128,192},{160,224},{192,0},{224,... | collective-permute-start | bytes 258056 | tf_op jit(solution)/shard_map/ppermute | solution.py:26
  35.4 8.7 %collective-permute-start.11 = (bf16[24,1792]{1,0:T(8,128)(2,1)S(1)}, bf16[24,1792]{1,0:T(8,128)(2,1)S(1)}, u32[]{:S(2)}, u32[]{:S(2)}) collective-permute-start(bf16[24,1792]{1,0:T(8,128)(2,1)S(1)} %get-tuple-element.42), channel_id=1, source_target_pairs={{0,192},{32,224},{64,0},{96,32},{128,64},{160,96},{192,128},{224,1... | collective-permute-start | bytes 258056 | tf_op jit(solution)/shard_map/ppermute | solution.py:26
  39.0 7.8 %collective-permute-start.12 = (bf16[24,1792]{1,0:T(8,128)(2,1)S(1)}, bf16[24,1792]{1,0:T(8,128)(2,1)S(1)}, u32[]{:S(2)}, u32[]{:S(2)}) collective-permute-start(bf16[24,1792]{1,0:T(8,128)(2,1)S(1)} %get-tuple-element.43), channel_id=1, source_target_pairs={{0,32},{32,64},{64,96},{96,128},{128,160},{160,192},{192,224},{224... | collective-permute-start | bytes 258056 | tf_op jit(solution)/shard_map/ppermute | solution.py:26
  39.2 32.6 %collective-permute-start.15 = (bf16[8,64,512]{2,1,0:T(8,128)(2,1)S(1)}, bf16[8,64,512]{2,1,0:T(8,128)(2,1)S(1)}, u32[]{:S(2)}, u32[]{:S(2)}) collective-permute-start(bf16[8,64,512]{2,1,0:T(8,128)(2,1)S(1)} %slice.36.refs_0_), channel_id=1, source_target_pairs={{0,8},{8,16},{16,24},{24,0},{1,9},{9,17},{17,25},{25,1},{2,10},{10... | collective-permute-start | bytes 1572872 | tf_op jit(solution)/shard_map/ppermute | solution.py:26
  40.5 31.3 %collective-permute-start.16 = (bf16[8,64,512]{2,1,0:T(8,128)(2,1)S(1)}, bf16[8,64,512]{2,1,0:T(8,128)(2,1)S(1)}, u32[]{:S(2)}, u32[]{:S(2)}) collective-permute-start(bf16[8,64,512]{2,1,0:T(8,128)(2,1)S(1)} %slice.36.refs_0_), channel_id=1, source_target_pairs={{0,16},{8,24},{16,0},{24,8},{1,17},{9,25},{17,1},{25,9},{2,18},{10... | collective-permute-start | bytes 1572872 | tf_op jit(solution)/shard_map/ppermute | solution.py:26
  43.0 28.9 %collective-permute-start.17 = (bf16[8,64,512]{2,1,0:T(8,128)(2,1)S(1)}, bf16[8,64,512]{2,1,0:T(8,128)(2,1)S(1)}, u32[]{:S(2)}, u32[]{:S(2)}) collective-permute-start(bf16[8,64,512]{2,1,0:T(8,128)(2,1)S(1)} %slice.36.refs_0_), channel_id=1, source_target_pairs={{0,24},{8,0},{16,8},{24,16},{1,25},{9,1},{17,9},{25,17},{2,26},{10... | collective-permute-start | bytes 1572872 | tf_op jit(solution)/shard_map/ppermute | solution.py:26
  44.1 4.9 %collective-permute-start.13 = (bf16[24,1792]{1,0:T(8,128)(2,1)S(1)}, bf16[24,1792]{1,0:T(8,128)(2,1)S(1)}, u32[]{:S(2)}, u32[]{:S(2)}) collective-permute-start(bf16[24,1792]{1,0:T(8,128)(2,1)S(1)} %get-tuple-element.44), channel_id=1, source_target_pairs={{0,224},{32,0},{64,32},{96,64},{128,96},{160,128},{192,160},{224,1... | collective-permute-start | bytes 258056 | tf_op jit(solution)/shard_map/ppermute | solution.py:26
  46.8 7.4 %collective-permute-start.7 = (bf16[24,1792]{1,0:T(8,128)(2,1)S(1)}, bf16[24,1792]{1,0:T(8,128)(2,1)S(1)}, u32[]{:S(2)}, u32[]{:S(2)}) collective-permute-start(bf16[24,1792]{1,0:T(8,128)(2,1)S(1)} %get-tuple-element.38), channel_id=1, source_target_pairs={{0,128},{32,160},{64,192},{96,224},{128,0},{160,32},{192,64},{224,... | collective-permute-start | bytes 258056 | tf_op jit(solution)/shard_map/ppermute | solution.py:26
  49.0 6.5 %collective-permute-start.8 = (bf16[24,1792]{1,0:T(8,128)(2,1)S(1)}, bf16[24,1792]{1,0:T(8,128)(2,1)S(1)}, u32[]{:S(2)}, u32[]{:S(2)}) collective-permute-start(bf16[24,1792]{1,0:T(8,128)(2,1)S(1)} %get-tuple-element.39), channel_id=1, source_target_pairs={{0,96},{32,128},{64,160},{96,192},{128,224},{160,0},{192,32},{224,... | collective-permute-start | bytes 258056 | tf_op jit(solution)/shard_map/ppermute | solution.py:26
  54.2 5.4 %collective-permute-start.9 = (bf16[24,1792]{1,0:T(8,128)(2,1)S(1)}, bf16[24,1792]{1,0:T(8,128)(2,1)S(1)}, u32[]{:S(2)}, u32[]{:S(2)}) collective-permute-start(bf16[24,1792]{1,0:T(8,128)(2,1)S(1)} %get-tuple-element.40), channel_id=1, source_target_pairs={{0,160},{32,192},{64,224},{96,0},{128,32},{160,64},{192,96},{224,1... | collective-permute-start | bytes 258056 | tf_op jit(solution)/shard_map/ppermute | solution.py:26
  63.0 19.5 %copy-start.12 = (f32[24,4]{0,1:T(4,128)S(1)}, f32[24,4]{0,1:T(4,128)}, u32[]{:S(2)}) copy-start(f32[24,4]{0,1:T(4,128)} %param.33) | copy-start | bytes 1156
  63.0 20.3 %copy-start.3 = (bf16[24,4096]{1,0:T(8,128)(2,1)S(1)}, bf16[24,4096]{1,0:T(8,128)(2,1)}, u32[]{:S(2)}) copy-start(bf16[24,4096]{1,0:T(8,128)(2,1)} %tokens.1) | copy-start | bytes 589828
  63.0 8.8 %collective-permute-start.14 = (bf16[24,512]{1,0:T(8,128)(2,1)S(1)}, bf16[24,512]{1,0:T(8,128)(2,1)S(1)}, u32[]{:S(2)}, u32[]{:S(2)}) collective-permute-start(bf16[24,512]{1,0:T(8,128)(2,1)S(1)} %attend.1.gated), channel_id=1, source_target_pairs={{0,4},{4,0},{1,5},{5,1},{2,6},{6,2},{3,7},{7,3},{8,12},{12,8},{9,1... | collective-permute-start | bytes 73736 | tf_op jit(solution)/shard_map/ppermute | solution.py:26
  73.3 5.1 %collective-permute-start.18 = (bf16[48,512]{1,0:T(8,128)(2,1)S(1)}, bf16[48,512]{1,0:T(8,128)(2,1)S(1)}, u32[]{:S(2)}, u32[]{:S(2)}) collective-permute-start(bf16[48,512]{1,0:T(8,128)(2,1)S(1)} %get-tuple-element.47), channel_id=1, source_target_pairs={{0,1},{1,2},{2,3},{3,0},{4,5},{5,6},{6,7},{7,4},{8,9},{9,10},{10,1... | collective-permute-start | bytes 147464 | tf_op jit(solution)/shard_map/ppermute | solution.py:26
  74.8 4.8 %collective-permute-start.19 = (bf16[48,512]{1,0:T(8,128)(2,1)S(1)}, bf16[48,512]{1,0:T(8,128)(2,1)S(1)}, u32[]{:S(2)}, u32[]{:S(2)}) collective-permute-start(bf16[48,512]{1,0:T(8,128)(2,1)S(1)} %get-tuple-element.48), channel_id=1, source_target_pairs={{0,2},{1,3},{2,0},{3,1},{4,6},{5,7},{6,4},{7,5},{8,10},{9,11},{10,... | collective-permute-start | bytes 147464 | tf_op jit(solution)/shard_map/ppermute | solution.py:26
  77.3 3.2 %collective-permute-start.20 = (bf16[48,512]{1,0:T(8,128)(2,1)S(1)}, bf16[48,512]{1,0:T(8,128)(2,1)S(1)}, u32[]{:S(2)}, u32[]{:S(2)}) collective-permute-start(bf16[48,512]{1,0:T(8,128)(2,1)S(1)} %get-tuple-element.49), channel_id=1, source_target_pairs={{0,3},{1,0},{2,1},{3,2},{4,7},{5,4},{6,5},{7,6},{8,11},{9,8},{10,9... | collective-permute-start | bytes 147464 | tf_op jit(solution)/shard_map/ppermute | solution.py:26
  80.6 2.7 %collective-permute-start.21 = (bf16[24,512]{1,0:T(8,128)(2,1)S(1)}, bf16[24,512]{1,0:T(8,128)(2,1)S(1)}, u32[]{:S(2)}, u32[]{:S(2)}) collective-permute-start(bf16[24,512]{1,0:T(8,128)(2,1)S(1)} %get-tuple-element.67), channel_id=1, source_target_pairs={{0,4},{4,0},{1,5},{5,1},{2,6},{6,2},{3,7},{7,3},{8,12},{12,8},{9,1... | collective-permute-start | bytes 73736 | tf_op jit(solution)/shard_map/ppermute | solution.py:26
  84.2 31.5 %copy-start.6 = (s32[4]{0:T(128)S(1)}, s32[4]{0:T(128)}, u32[]{:S(2)}) copy-start(s32[4]{0:T(128)} %copy-done.5) | copy-start | bytes 52
  104.1 11.6 %collective-permute-start.24 = (bf16[1536,128]{1,0:T(8,128)(2,1)S(1)}, bf16[1536,128]{1,0:T(8,128)(2,1)S(1)}, u32[]{:S(2)}, u32[]{:S(2)}) collective-permute-start(bf16[1536,128]{1,0:T(8,128)(2,1)S(1)} %bitcast.21), channel_id=1, source_target_pairs={{0,1},{1,2},{2,3},{3,0},{4,5},{5,6},{6,7},{7,4},{8,9},{9,10},{10,1... | collective-permute-start | bytes 1179656 | tf_op jit(solution)/shard_map/ppermute | solution.py:26
  108.0 47.5 %collective-permute-start.28 = (bf16[256,1024]{1,0:T(8,128)(2,1)}, bf16[256,1024]{1,0:T(8,128)(2,1)S(1)}, u32[]{:S(2)}, u32[]{:S(2)}) collective-permute-start(bf16[256,1024]{1,0:T(8,128)(2,1)} %get-tuple-element.61), channel_id=1, source_target_pairs={{0,1},{1,2},{2,3},{3,0},{4,5},{5,6},{6,7},{7,4},{8,9},{9,10},{10,1... | collective-permute-start | bytes 1572872 | tf_op jit(solution)/shard_map/ppermute | solution.py:26
  109.0 12.9 %collective-permute-start.23 = (bf16[1536,128]{1,0:T(8,128)(2,1)S(1)}, bf16[1536,128]{1,0:T(8,128)(2,1)S(1)}, u32[]{:S(2)}, u32[]{:S(2)}) collective-permute-start(bf16[1536,128]{1,0:T(8,128)(2,1)S(1)} %bitcast.22), channel_id=1, source_target_pairs={{0,3},{1,0},{2,1},{3,2},{4,7},{5,4},{6,5},{7,6},{8,11},{9,8},{10,9... | collective-permute-start | bytes 1179656 | tf_op jit(solution)/shard_map/ppermute | solution.py:26
  110.8 44.9 %collective-permute-start.29 = (bf16[256,1024]{1,0:T(8,128)(2,1)}, bf16[256,1024]{1,0:T(8,128)(2,1)S(1)}, u32[]{:S(2)}, u32[]{:S(2)}) collective-permute-start(bf16[256,1024]{1,0:T(8,128)(2,1)} %get-tuple-element.62), channel_id=1, source_target_pairs={{0,2},{1,3},{2,0},{3,1},{4,6},{5,7},{6,4},{7,5},{8,10},{9,11},{10,... | collective-permute-start | bytes 1572872 | tf_op jit(solution)/shard_map/ppermute | solution.py:26
  113.0 42.7 %collective-permute-start.30 = (bf16[256,1024]{1,0:T(8,128)(2,1)}, bf16[256,1024]{1,0:T(8,128)(2,1)S(1)}, u32[]{:S(2)}, u32[]{:S(2)}) collective-permute-start(bf16[256,1024]{1,0:T(8,128)(2,1)} %get-tuple-element.63), channel_id=1, source_target_pairs={{0,3},{1,0},{2,1},{3,2},{4,7},{5,4},{6,5},{7,6},{8,11},{9,8},{10,9... | collective-permute-start | bytes 1572872 | tf_op jit(solution)/shard_map/ppermute | solution.py:26
  115.7 31.7 %collective-permute-start.22 = (bf16[1536,128]{1,0:T(8,128)(2,1)S(1)}, bf16[1536,128]{1,0:T(8,128)(2,1)S(1)}, u32[]{:S(2)}, u32[]{:S(2)}) collective-permute-start(bf16[1536,128]{1,0:T(8,128)(2,1)S(1)} %bitcast.23), channel_id=1, source_target_pairs={{0,2},{1,3},{2,0},{3,1},{4,6},{5,7},{6,4},{7,5},{8,10},{9,11},{10,... | collective-permute-start | bytes 1179656 | tf_op jit(solution)/shard_map/ppermute | solution.py:26
  115.7 1.6 copy-start
  117.3 1.6 copy-start.1
  121.9 33.8 %copy-start.4 = (bf16[256,1024]{1,0:T(8,128)(2,1)S(1)}, bf16[256,1024]{1,0:T(8,128)(2,1)}, u32[]{:S(2)}) copy-start(bf16[256,1024]{1,0:T(8,128)(2,1)} %get-tuple-element.60.refs_0_) | copy-start | bytes 1572868
  148.4 7.9 %collective-permute-start.25 = (bf16[192,256]{1,0:T(8,128)(2,1)S(1)}, bf16[192,256]{1,0:T(8,128)(2,1)S(1)}, u32[]{:S(2)}, u32[]{:S(2)}) collective-permute-start(bf16[192,256]{1,0:T(8,128)(2,1)S(1)} %expert.7.refs_0_), channel_id=1, source_target_pairs={{0,1},{1,2},{2,3},{3,0},{4,5},{5,6},{6,7},{7,4},{8,9},{9,10},{10,1... | collective-permute-start | bytes 294920 | tf_op jit(solution)/shard_map/ppermute | solution.py:26
  153.2 5.6 %collective-permute-start.26 = (bf16[192,256]{1,0:T(8,128)(2,1)S(1)}, bf16[192,256]{1,0:T(8,128)(2,1)S(1)}, u32[]{:S(2)}, u32[]{:S(2)}) collective-permute-start(bf16[192,256]{1,0:T(8,128)(2,1)S(1)} %expert.7.refs_0_), channel_id=1, source_target_pairs={{0,2},{1,3},{2,0},{3,1},{4,6},{5,7},{6,4},{7,5},{8,10},{9,11},{10,... | collective-permute-start | bytes 294920 | tf_op jit(solution)/shard_map/ppermute | solution.py:26
  155.5 4.7 %collective-permute-start.27 = (bf16[192,256]{1,0:T(8,128)(2,1)S(1)}, bf16[192,256]{1,0:T(8,128)(2,1)S(1)}, u32[]{:S(2)}, u32[]{:S(2)}) collective-permute-start(bf16[192,256]{1,0:T(8,128)(2,1)S(1)} %expert.7.refs_0_), channel_id=1, source_target_pairs={{0,3},{1,0},{2,1},{3,2},{4,7},{5,4},{6,5},{7,6},{8,11},{9,8},{10,9... | collective-permute-start | bytes 294920 | tf_op jit(solution)/shard_map/ppermute | solution.py:26
  161.6 21.8 %all-to-all-start.2 = ((bf16[64,24,128]{2,1,0:T(8,128)(2,1)}), bf16[64,24,128]{2,1,0:T(8,128)(2,1)S(1)}, u32[]{:S(2)}, u32[]{:S(2)}) async-start(bf16[64,24,128]{2,1,0:T(8,128)(2,1)} %bitcast.14), calls=%async_computation.2 | async-start | bytes 786432 | tf_op jit(solution)/shard_map/all_to_all | solution.py:635
  183.7 4.2 %collective-permute-start.31 = (bf16[24,1024]{1,0:T(8,128)(2,1)S(1)}, bf16[24,1024]{1,0:T(8,128)(2,1)S(1)}, u32[]{:S(2)}, u32[]{:S(2)}) collective-permute-start(bf16[24,1024]{1,0:T(8,128)(2,1)S(1)} %combine.1.refs_0_), channel_id=1, source_target_pairs={{0,1},{1,2},{2,3},{3,0},{4,5},{5,6},{6,7},{7,4},{8,9},{9,10},{10,1... | collective-permute-start | bytes 147464 | tf_op jit(solution)/shard_map/ppermute | solution.py:26
  183.8 5.1 %collective-permute-start.32 = (bf16[24,1024]{1,0:T(8,128)(2,1)S(1)}, bf16[24,1024]{1,0:T(8,128)(2,1)S(1)}, u32[]{:S(2)}, u32[]{:S(2)}) collective-permute-start(bf16[24,1024]{1,0:T(8,128)(2,1)S(1)} %combine.1.refs_0_), channel_id=1, source_target_pairs={{0,2},{1,3},{2,0},{3,1},{4,6},{5,7},{6,4},{7,5},{8,10},{9,11},{10,... | collective-permute-start | bytes 147464 | tf_op jit(solution)/shard_map/ppermute | solution.py:26
  186.6 3.4 %collective-permute-start.33 = (bf16[24,1024]{1,0:T(8,128)(2,1)S(1)}, bf16[24,1024]{1,0:T(8,128)(2,1)S(1)}, u32[]{:S(2)}, u32[]{:S(2)}) collective-permute-start(bf16[24,1024]{1,0:T(8,128)(2,1)S(1)} %combine.1.refs_0_), channel_id=1, source_target_pairs={{0,3},{1,0},{2,1},{3,2},{4,7},{5,4},{6,5},{7,6},{8,11},{9,8},{10,9... | collective-permute-start | bytes 147464 | tf_op jit(solution)/shard_map/ppermute | solution.py:26

commit v6 on v5

--- a/solution.py
+++ b/solution.py
@@ -24,6 +24,14 @@
 def shift(value, axis, by):
     n = lax.axis_size(axis)
     return lax.ppermute(value, axis, [(i, (i + by) % n) for i in range(n)])
+
+
+def spread(values):
+    n = len(values)
+    out = [values[0]] + [None] * (n - 1)
+    for s in sorted(range(1, n), key=lambda s: (-min(s, n - s), s)):
+        out[s] = shift(values[s], T, s)
+    return out
 
 
 def order_of(n):
@@ -608,7 +616,7 @@
     gated = attend(arrived, first_scale, decay_shift, state, head_gain)
     partner = shift(gated, C, 1)
     mixed = mix(where, gated, partner, blocks)
-    mixed = [mixed[0]] + [shift(mixed[s], T, s) for s in range(1, nt)]
+    mixed = spread(mixed)
     mine = functools.reduce(jnp.add, [m[:seqs].astype(f32) for m in mixed]).astype(bf16)
     theirs = functools.reduce(jnp.add, [m[seqs:].astype(f32) for m in mixed]).astype(bf16)
     other_half = shift(theirs, C, 1)
@@ -630,13 +638,13 @@
             where, inverse, picked[s], s, nt, pieces[s], slots, before, s == steps[-1]
         )
     act = before
-    acts = [act] + [shift(act, T, s) for s in range(1, nt)]
+    acts = spread([act] * nt)
     done = down_sum(acts, fetched)
     returned = lax.all_to_all(
         done.reshape(n_ep, -1, 128), EP, 0, 0, tiled=True
     ).reshape(-1, 128)
     result = combine(returned, weights, stream)
-    results = [result] + [shift(result, T, s) for s in range(1, nt)]
+    results = spread([result] * nt)
     return finish(where, results, nz)
 
 

time: 192 us -> 192 us (level)
  no operation moved by 1% of the time
where the time goes in v6:
time: 192 us; the launch traced here: 191 us
  starting transfers between devices  71.9 us (37%)
  waiting for transfers between devices  71.4 us (37%)
  Pallas kernels  22.6 us (12%)
  blocking collectives  19.8 us (10%)
  local copies, waits for them, and re-layouts  4.69 us (2%)
    ppermute x34, starting transfers between devices, shift(): return lax.ppermute(value, axis, [(i, (i + by) % n) for i in range(n)])  56.2 us
    ppermute x34, waiting for transfers between devices, shift(): return lax.ppermute(value, axis, [(i, (i + by) % n) for i in range(n)])  52.7 us
    all_to_all x1, blocking collectives, on_device(): lax.all_to_all(outbound.reshape(n_ep, -1, 128), EP, 0, 0, tiled=True)  19.8 us
    all_to_all x1, waiting for transfers between devices, on_device(): lax.all_to_all(done.reshape(n_ep, -1, 128), EP, 0, 0, tiled=True)  15.1 us
    all_to_all x1, starting transfers between devices, on_device(): moved = lax.all_to_all(payload, Z, 0, 0, tiled=True)  9.02 us
    all_to_all x1, starting transfers between devices, on_device(): lax.all_to_all(done.reshape(n_ep, -1, 128), EP, 0, 0, tiled=True)  6.61 us
    unnamed x27, local copies, waits for them, and re-layouts  4.26 us
    pallas_call x1, Pallas kernels, split(): pl.pallas_call(functools.partial(split_kernel, nz), out_shape=[shaped((ro...  3.92 us
  transfers between devices with their start and end apart: 36, of which 22 were waited for; matrix products, arithmetic and copies ran while one was open for 1% of the time, Pallas kernels for 7%

profile of v6, /device:TPU:1, one launch (start us, length us, event | category | flops | bytes accessed | tf_op | source)
XLA Modules:
  0.0 191.3 jit_solution(17251604593805117419)
XLA Ops:
  0.0 2.0 %scale.1 = (bf16[8,88,512]{2,1,0:T(8,128)(2,1)}, f32[24,128]{1,0:T(8,128)}) custom-call(bf16[24,4096]{1,0:T(8,128)(2,1)} %tokens.1, bf16[4096]{0:T(1024)(128)(2,1)} %gain_at.1, bf16[64,512]{1,0:T(8,128)(2,1)} %bitcast.30), custom_call_target="tpu_custom_call" | custom-call | flops 1000000 | bytes 393216 | tf_op jit(solution)/shard_map/scale/pallas_call | solution.py:114
  2.0 9.0 %all-to-all-start = ((bf16[8,88,512]{2,1,0:T(8,128)(2,1)}), bf16[8,88,512]{2,1,0:T(8,128)(2,1)S(1)}, u32[]{:S(2)}, u32[]{:S(2)}) async-start(bf16[8,88,512]{2,1,0:T(8,128)(2,1)} %get-tuple-element.36), calls=%async_computation | async-start | bytes 1441792 | tf_op jit(solution)/shard_map/all_to_all | solution.py:597
  11.1 1.7 pack.1.refs_0_
  12.7 1.3 collective-permute-start
  14.0 2.5 %collective-permute-start.1 = (bf16[64,1792]{1,0:T(8,128)(2,1)}, bf16[64,1792]{1,0:T(8,128)(2,1)S(1)}, u32[]{:S(2)}, u32[]{:S(2)}) collective-permute-start(bf16[64,1792]{1,0:T(8,128)(2,1)} %pack.1.refs_0_), channel_id=1, source_target_pairs={{0,16},{8,24},{16,0},{24,8},{1,17},{9,25},{17,1},{25,9},{2,18},{10... | collective-permute-start | bytes 688136 | tf_op jit(solution)/shard_map/ppermute | solution.py:26
  16.5 1.2 collective-permute-start.2
  17.6 1.8 collective-permute-start.3
  19.4 1.0 collective-permute-done.refs_1_
  20.4 2.2 %collective-permute-start.4 = (bf16[64,1792]{1,0:T(8,128)(2,1)S(1)}, bf16[64,1792]{1,0:T(8,128)(2,1)S(1)}, u32[]{:S(2)}, u32[]{:S(2)}) collective-permute-start(bf16[64,1792]{1,0:T(8,128)(2,1)S(1)} %collective-permute-done.refs_1_), channel_id=1, source_target_pairs={{0,4},{4,0},{1,5},{5,1},{2,6},{6,2},{3,7},{7,3},{8,12},{12,8},{9,1... | collective-permute-start | bytes 688136 | tf_op jit(solution)/shard_map/ppermute | solution.py:26
  22.7 3.7 %collective-permute-done.1.refs_2_ = bf16[64,1792]{1,0:T(8,128)(2,1)S(1)} collective-permute-done((bf16[64,1792]{1,0:T(8,128)(2,1)}, bf16[64,1792]{1,0:T(8,128)(2,1)S(1)}, u32[]{:S(2)}, u32[]{:S(2)}) %collective-permute-start.1) | collective-permute-done | bytes 229408 | tf_op jit(solution)/shard_map/ppermute | solution.py:26
  26.3 1.8 collective-permute-start.5
  28.3 1.0 collective-permute-done.5.refs_6_
  29.7 3.5 %all-to-all-done.tok = bf16[8,88,512]{2,1,0:T(8,128)(2,1)S(1)} async-done(((bf16[8,88,512]{2,1,0:T(8,128)(2,1)}), bf16[8,88,512]{2,1,0:T(8,128)(2,1)S(1)}, u32[]{:S(2)}, u32[]{:S(2)}) %all-to-all-start) | async-done | bytes 720928 | tf_op jit(solution)/shard_map/all_to_all | solution.py:597
  33.2 0.9 copy-done.2
  34.1 1.2 project.1
  35.4 3.6 %collective-permute-start.11 = (bf16[24,1792]{1,0:T(8,128)(2,1)S(1)}, bf16[24,1792]{1,0:T(8,128)(2,1)S(1)}, u32[]{:S(2)}, u32[]{:S(2)}) collective-permute-start(bf16[24,1792]{1,0:T(8,128)(2,1)S(1)} %get-tuple-element.42), channel_id=1, source_target_pairs={{0,192},{32,224},{64,0},{96,32},{128,64},{160,96},{192,128},{224,1... | collective-permute-start | bytes 258056 | tf_op jit(solution)/shard_map/ppermute | solution.py:26
  39.2 1.3 collective-permute-start.15
  40.5 2.5 %collective-permute-start.16 = (bf16[8,64,512]{2,1,0:T(8,128)(2,1)S(1)}, bf16[8,64,512]{2,1,0:T(8,128)(2,1)S(1)}, u32[]{:S(2)}, u32[]{:S(2)}) collective-permute-start(bf16[8,64,512]{2,1,0:T(8,128)(2,1)S(1)} %slice.36.refs_0_), channel_id=1, source_target_pairs={{0,16},{8,24},{16,0},{24,8},{1,17},{9,25},{17,1},{25,9},{2,18},{10... | collective-permute-start | bytes 1572872 | tf_op jit(solution)/shard_map/ppermute | solution.py:26
  43.0 1.2 collective-permute-start.17
  44.1 2.7 %collective-permute-start.13 = (bf16[24,1792]{1,0:T(8,128)(2,1)S(1)}, bf16[24,1792]{1,0:T(8,128)(2,1)S(1)}, u32[]{:S(2)}, u32[]{:S(2)}) collective-permute-start(bf16[24,1792]{1,0:T(8,128)(2,1)S(1)} %get-tuple-element.44), channel_id=1, source_target_pairs={{0,224},{32,0},{64,32},{96,64},{128,96},{160,128},{192,160},{224,1... | collective-permute-start | bytes 258056 | tf_op jit(solution)/shard_map/ppermute | solution.py:26
  46.8 1.4 collective-permute-start.7
  48.3 0.7 collective-permute-done.13.refs_7_
  49.0 1.6 collective-permute-start.8
  50.7 3.5 %collective-permute-done.7.refs_1_ = bf16[24,1792]{1,0:T(8,128)(2,1)S(1)} collective-permute-done((bf16[24,1792]{1,0:T(8,128)(2,1)S(1)}, bf16[24,1792]{1,0:T(8,128)(2,1)S(1)}, u32[]{:S(2)}, u32[]{:S(2)}) %collective-permute-start.7) | collective-permute-done | bytes 86048 | tf_op jit(solution)/shard_map/ppermute | solution.py:26
  54.3 1.3 collective-permute-done.8.refs_2_
  55.6 4.0 %collective-permute-done.9.refs_3_ = bf16[24,1792]{1,0:T(8,128)(2,1)S(1)} collective-permute-done((bf16[24,1792]{1,0:T(8,128)(2,1)S(1)}, bf16[24,1792]{1,0:T(8,128)(2,1)S(1)}, u32[]{:S(2)}, u32[]{:S(2)}) %collective-permute-start.9) | collective-permute-done | bytes 86048 | tf_op jit(solution)/shard_map/ppermute | solution.py:26
  59.6 3.4 %attend.1.gated = bf16[24,512]{1,0:T(8,128)(2,1)S(1)} custom-call(bf16[24,1792]{1,0:T(8,128)(2,1)S(1)} %get-tuple-element.37.refs_0_, bf16[24,1792]{1,0:T(8,128)(2,1)S(1)} %collective-permute-done.7.refs_1_, bf16[24,1792]{1,0:T(8,128)(2,1)S(1)} %collective-permute-done.8.refs_2_, bf16[24,1792]{1,0:T(8,128)(2,1)S(1)} %collective-permute-done.9.refs_3_, ...), custom_call_target="tpu_custom_call" | custom-call | flops 6291456 | bytes 6291456 | tf_op jit(solution)/shard_map/attend/pallas_call | solution.py:257
  63.0 8.0 %collective-permute-start.14 = (bf16[24,512]{1,0:T(8,128)(2,1)S(1)}, bf16[24,512]{1,0:T(8,128)(2,1)S(1)}, u32[]{:S(2)}, u32[]{:S(2)}) collective-permute-start(bf16[24,512]{1,0:T(8,128)(2,1)S(1)} %attend.1.gated), channel_id=1, source_target_pairs={{0,4},{4,0},{1,5},{5,1},{2,6},{6,2},{3,7},{7,3},{8,12},{12,8},{9,1... | collective-permute-start | bytes 73736 | tf_op jit(solution)/shard_map/ppermute | solution.py:26
  71.8 1.5 mix.1
  73.3 1.5 collective-permute-start.18
  74.8 2.5 %collective-permute-start.19 = (bf16[48,512]{1,0:T(8,128)(2,1)S(1)}, bf16[48,512]{1,0:T(8,128)(2,1)S(1)}, u32[]{:S(2)}, u32[]{:S(2)}) collective-permute-start(bf16[48,512]{1,0:T(8,128)(2,1)S(1)} %get-tuple-element.48), channel_id=1, source_target_pairs={{0,2},{1,3},{2,0},{3,1},{4,6},{5,7},{6,4},{7,5},{8,10},{9,11},{10,... | collective-permute-start | bytes 147464 | tf_op jit(solution)/shard_map/ppermute | solution.py:26
  77.3 1.1 collective-permute-start.20
  78.4 1.2 collective-permute-done.19
  79.6 1.0 collective-permute-done.20
  80.6 1.8 collective-permute-start.21
  82.7 0.6 collective-permute-done.21.other
  83.3 0.9 dispatch.1
  84.3 19.8 %all_to_all.15 = bf16[64,24,128]{2,1,0:T(8,128)(2,1)S(1)} all-to-all(bf16[64,24,128]{2,1,0:T(8,128)(2,1)S(1)} %bitcast.25), channel_id=1, replica_groups=mesh['ep_0'=8,'ep_1'=4,'ep_2'=2,'tp'=4] {'ep_0','ep_1','ep_2'}, dimensions={0} | all-to-all | bytes 786432 | tf_op jit(solution)/shard_map/all_to_all | solution.py:626
  104.1 3.9 %split.1 = (bf16[256,1024]{1,0:T(8,128)(2,1)}, bf16[256,1024]{1,0:T(8,128)(2,1)}, bf16[256,1024]{1,0:T(8,128)(2,1)}, bf16[256,1024]{1,0:T(8,128)(2,1)}) custom-call(s32[4]{0:T(128)} %copy-done.5, bf16[256,4096]{1,0:T(8,128)(2,1)} %bitcast.29), custom_call_target="tpu_custom_call" | custom-call | flops 1000000 | bytes 4194304 | tf_op jit(solution)/shard_map/split/pallas_call | solution.py:155
  108.0 1.0 collective-permute-start.28
  109.0 1.9 collective-permute-start.23
  110.8 2.2 %collective-permute-start.29 = (bf16[256,1024]{1,0:T(8,128)(2,1)}, bf16[256,1024]{1,0:T(8,128)(2,1)S(1)}, u32[]{:S(2)}, u32[]{:S(2)}) collective-permute-start(bf16[256,1024]{1,0:T(8,128)(2,1)} %get-tuple-element.62), channel_id=1, source_target_pairs={{0,2},{1,3},{2,0},{3,1},{4,6},{5,7},{6,4},{7,5},{8,10},{9,11},{10,... | collective-permute-start | bytes 1572872 | tf_op jit(solution)/shard_map/ppermute | solution.py:26
  113.0 0.6 collective-permute-start.30
  113.6 2.1 %collective-permute-done.24.piece = bf16[1536,128]{1,0:T(8,128)(2,1)S(1)} collective-permute-done((bf16[1536,128]{1,0:T(8,128)(2,1)S(1)}, bf16[1536,128]{1,0:T(8,128)(2,1)S(1)}, u32[]{:S(2)}, u32[]{:S(2)}) %collective-permute-start.24) | collective-permute-done | bytes 393248 | tf_op jit(solution)/shard_map/ppermute | solution.py:26
  115.7 1.6 copy-done
  117.3 1.6 copy-done.1
  118.9 1.0 pick.1
  119.9 1.0 expert.4
  120.9 1.0 expert.5
  121.9 1.0 expert.6
  122.9 24.5 %collective-permute-done.22.piece = bf16[1536,128]{1,0:T(8,128)(2,1)S(1)} collective-permute-done((bf16[1536,128]{1,0:T(8,128)(2,1)S(1)}, bf16[1536,128]{1,0:T(8,128)(2,1)S(1)}, u32[]{:S(2)}, u32[]{:S(2)}) %collective-permute-start.22) | collective-permute-done | bytes 393248 | tf_op jit(solution)/shard_map/ppermute | solution.py:26
  147.4 1.0 expert.7.refs_0_
  148.4 4.8 %collective-permute-start.25 = (bf16[192,256]{1,0:T(8,128)(2,1)S(1)}, bf16[192,256]{1,0:T(8,128)(2,1)S(1)}, u32[]{:S(2)}, u32[]{:S(2)}) collective-permute-start(bf16[192,256]{1,0:T(8,128)(2,1)S(1)} %expert.7.refs_0_), channel_id=1, source_target_pairs={{0,1},{1,2},{2,3},{3,0},{4,5},{5,6},{6,7},{7,4},{8,9},{9,10},{10,1... | collective-permute-start | bytes 294920 | tf_op jit(solution)/shard_map/ppermute | solution.py:26
  153.2 2.3 %collective-permute-start.26 = (bf16[192,256]{1,0:T(8,128)(2,1)S(1)}, bf16[192,256]{1,0:T(8,128)(2,1)S(1)}, u32[]{:S(2)}, u32[]{:S(2)}) collective-permute-start(bf16[192,256]{1,0:T(8,128)(2,1)S(1)} %expert.7.refs_0_), channel_id=1, source_target_pairs={{0,2},{1,3},{2,0},{3,1},{4,6},{5,7},{6,4},{7,5},{8,10},{9,11},{10,... | collective-permute-start | bytes 294920 | tf_op jit(solution)/shard_map/ppermute | solution.py:26
  156.3 2.5 %collective-permute-done.26.refs_2_ = bf16[192,256]{1,0:T(8,128)(2,1)S(1)} collective-permute-done((bf16[192,256]{1,0:T(8,128)(2,1)S(1)}, bf16[192,256]{1,0:T(8,128)(2,1)S(1)}, u32[]{:S(2)}, u32[]{:S(2)}) %collective-permute-start.26) | collective-permute-done | bytes 98336 | tf_op jit(solution)/shard_map/ppermute | solution.py:26
  158.8 1.4 collective-permute-done.27.refs_3_
  160.2 1.4 down.1
  161.6 6.6 %all-to-all-start.2 = ((bf16[64,24,128]{2,1,0:T(8,128)(2,1)}), bf16[64,24,128]{2,1,0:T(8,128)(2,1)S(1)}, u32[]{:S(2)}, u32[]{:S(2)}) async-start(bf16[64,24,128]{2,1,0:T(8,128)(2,1)} %bitcast.14), calls=%async_computation.2 | async-start | bytes 786432 | tf_op jit(solution)/shard_map/all_to_all | solution.py:643
  168.2 15.1 %all-to-all-done.2 = bf16[64,24,128]{2,1,0:T(8,128)(2,1)S(1)} async-done(((bf16[64,24,128]{2,1,0:T(8,128)(2,1)}), bf16[64,24,128]{2,1,0:T(8,128)(2,1)S(1)}, u32[]{:S(2)}, u32[]{:S(2)}) %all-to-all-start.2) | async-done | bytes 393248 | tf_op jit(solution)/shard_map/all_to_all | solution.py:643
  183.8 2.8 %collective-permute-start.32 = (bf16[24,1024]{1,0:T(8,128)(2,1)S(1)}, bf16[24,1024]{1,0:T(8,128)(2,1)S(1)}, u32[]{:S(2)}, u32[]{:S(2)}) collective-permute-start(bf16[24,1024]{1,0:T(8,128)(2,1)S(1)} %combine.1.refs_0_), channel_id=1, source_target_pairs={{0,2},{1,3},{2,0},{3,1},{4,6},{5,7},{6,4},{7,5},{8,10},{9,11},{10,... | collective-permute-start | bytes 147464 | tf_op jit(solution)/shard_map/ppermute | solution.py:26
  187.1 0.9 collective-permute-done.31.refs_1_
  187.9 1.0 collective-permute-done.32.refs_2_
  189.0 1.1 collective-permute-done.33.refs_3_
  190.0 1.3 finish.1
  (69 shorter events, 4.0 us)
Async XLA Ops:
  2.0 37.0 %copy-start.11 = (s32[24,4]{0,1:T(4,128)S(1)}, s32[24,4]{0,1:T(4,128)}, u32[]{:S(2)}) copy-start(s32[24,4]{0,1:T(4,128)} %param.32) | copy-start | bytes 1156
  2.0 31.2 %all-to-all-start = ((bf16[8,88,512]{2,1,0:T(8,128)(2,1)}), bf16[8,88,512]{2,1,0:T(8,128)(2,1)S(1)}, u32[]{:S(2)}, u32[]{:S(2)}) async-start(bf16[8,88,512]{2,1,0:T(8,128)(2,1)} %get-tuple-element.36), calls=%async_computation | async-start | bytes 1441792 | tf_op jit(solution)/shard_map/all_to_all | solution.py:597
  11.0 43.2 %copy-start.10 = (bf16[4096]{0:T(1024)(128)(2,1)S(1)}, bf16[4096]{0:T(1024)(128)(2,1)}, u32[]{:S(2)}) copy-start(bf16[4096]{0:T(1024)(128)(2,1)} %param.28) | copy-start | bytes 24580
  11.0 48.6 %copy-start.7 = (f32[24,256]{1,0:T(8,128)S(1)}, f32[24,256]{1,0:T(8,128)}, u32[]{:S(2)}) copy-start(f32[24,256]{1,0:T(8,128)} %refs_9_.1) | copy-start | bytes 73732
  11.0 48.6 %copy-start.8 = (f32[24,128]{1,0:T(8,128)S(1)}, f32[24,128]{1,0:T(8,128)}, u32[]{:S(2)}) copy-start(f32[24,128]{1,0:T(8,128)} %get-tuple-element.45.refs_8_) | copy-start | bytes 36868
  11.0 48.6 %copy-start.9 = (bf16[512]{0:T(512)(128)(2,1)S(1)}, bf16[512]{0:T(512)(128)(2,1)}, u32[]{:S(2)}) copy-start(bf16[512]{0:T(512)(128)(2,1)} %refs_11_.1) | copy-start | bytes 3076
  12.7 7.7 %collective-permute-start = (bf16[64,1792]{1,0:T(8,128)(2,1)}, bf16[64,1792]{1,0:T(8,128)(2,1)S(1)}, u32[]{:S(2)}, u32[]{:S(2)}) collective-permute-start(bf16[64,1792]{1,0:T(8,128)(2,1)} %pack.1.refs_0_), channel_id=1, source_target_pairs={{0,8},{8,16},{16,24},{24,0},{1,9},{9,17},{17,25},{25,1},{2,10},{10... | collective-permute-start | bytes 688136 | tf_op jit(solution)/shard_map/ppermute | solution.py:26
  14.0 12.3 %collective-permute-start.1 = (bf16[64,1792]{1,0:T(8,128)(2,1)}, bf16[64,1792]{1,0:T(8,128)(2,1)S(1)}, u32[]{:S(2)}, u32[]{:S(2)}) collective-permute-start(bf16[64,1792]{1,0:T(8,128)(2,1)} %pack.1.refs_0_), channel_id=1, source_target_pairs={{0,16},{8,24},{16,0},{24,8},{1,17},{9,25},{17,1},{25,9},{2,18},{10... | collective-permute-start | bytes 688136 | tf_op jit(solution)/shard_map/ppermute | solution.py:26
  16.5 11.7 %collective-permute-start.2 = (bf16[64,1792]{1,0:T(8,128)(2,1)}, bf16[64,1792]{1,0:T(8,128)(2,1)S(1)}, u32[]{:S(2)}, u32[]{:S(2)}) collective-permute-start(bf16[64,1792]{1,0:T(8,128)(2,1)} %pack.1.refs_0_), channel_id=1, source_target_pairs={{0,24},{8,0},{16,8},{24,16},{1,25},{9,1},{17,9},{25,17},{2,26},{10... | collective-permute-start | bytes 688136 | tf_op jit(solution)/shard_map/ppermute | solution.py:26
  17.6 10.6 %collective-permute-start.3 = (bf16[64,1792]{1,0:T(8,128)(2,1)}, bf16[64,1792]{1,0:T(8,128)(2,1)S(1)}, u32[]{:S(2)}, u32[]{:S(2)}) collective-permute-start(bf16[64,1792]{1,0:T(8,128)(2,1)} %pack.1.refs_0_), channel_id=1, source_target_pairs={{0,4},{4,0},{1,5},{5,1},{2,6},{6,2},{3,7},{7,3},{8,12},{12,8},{9,1... | collective-permute-start | bytes 688136 | tf_op jit(solution)/shard_map/ppermute | solution.py:26
  20.4 7.8 %collective-permute-start.4 = (bf16[64,1792]{1,0:T(8,128)(2,1)S(1)}, bf16[64,1792]{1,0:T(8,128)(2,1)S(1)}, u32[]{:S(2)}, u32[]{:S(2)}) collective-permute-start(bf16[64,1792]{1,0:T(8,128)(2,1)S(1)} %collective-permute-done.refs_1_), channel_id=1, source_target_pairs={{0,4},{4,0},{1,5},{5,1},{2,6},{6,2},{3,7},{7,3},{8,12},{12,8},{9,1... | collective-permute-start | bytes 688136 | tf_op jit(solution)/shard_map/ppermute | solution.py:26
  26.3 2.9 %collective-permute-start.5 = (bf16[64,1792]{1,0:T(8,128)(2,1)S(1)}, bf16[64,1792]{1,0:T(8,128)(2,1)S(1)}, u32[]{:S(2)}, u32[]{:S(2)}) collective-permute-start(bf16[64,1792]{1,0:T(8,128)(2,1)S(1)} %collective-permute-done.1.refs_2_), channel_id=1, source_target_pairs={{0,4},{4,0},{1,5},{5,1},{2,6},{6,2},{3,7},{7,3},{8,12},{12,8},{9,1... | collective-permute-start | bytes 688136 | tf_op jit(solution)/shard_map/ppermute | solution.py:26
  28.2 1.5 collective-permute-start.6
  28.2 55.1 %copy-start.5 = (s32[4]{0:T(128)}, s32[4]{0:T(128)S(1)}, u32[]{:S(2)}) copy-start(s32[4]{0:T(128)S(1)} %pad_add_fusion.where) | copy-start | bytes 52
  33.2 0.9 copy-start.2
  35.3 7.6 %collective-permute-start.10 = (bf16[24,1792]{1,0:T(8,128)(2,1)S(1)}, bf16[24,1792]{1,0:T(8,128)(2,1)S(1)}, u32[]{:S(2)}, u32[]{:S(2)}) collective-permute-start(bf16[24,1792]{1,0:T(8,128)(2,1)S(1)} %get-tuple-element.41), channel_id=1, source_target_pairs={{0,64},{32,96},{64,128},{96,160},{128,192},{160,224},{192,0},{224,... | collective-permute-start | bytes 258056 | tf_op jit(solution)/shard_map/ppermute | solution.py:26
  35.4 8.7 %collective-permute-start.11 = (bf16[24,1792]{1,0:T(8,128)(2,1)S(1)}, bf16[24,1792]{1,0:T(8,128)(2,1)S(1)}, u32[]{:S(2)}, u32[]{:S(2)}) collective-permute-start(bf16[24,1792]{1,0:T(8,128)(2,1)S(1)} %get-tuple-element.42), channel_id=1, source_target_pairs={{0,192},{32,224},{64,0},{96,32},{128,64},{160,96},{192,128},{224,1... | collective-permute-start | bytes 258056 | tf_op jit(solution)/shard_map/ppermute | solution.py:26
  39.0 7.8 %collective-permute-start.12 = (bf16[24,1792]{1,0:T(8,128)(2,1)S(1)}, bf16[24,1792]{1,0:T(8,128)(2,1)S(1)}, u32[]{:S(2)}, u32[]{:S(2)}) collective-permute-start(bf16[24,1792]{1,0:T(8,128)(2,1)S(1)} %get-tuple-element.43), channel_id=1, source_target_pairs={{0,32},{32,64},{64,96},{96,128},{128,160},{160,192},{192,224},{224... | collective-permute-start | bytes 258056 | tf_op jit(solution)/shard_map/ppermute | solution.py:26
  39.2 32.6 %collective-permute-start.15 = (bf16[8,64,512]{2,1,0:T(8,128)(2,1)S(1)}, bf16[8,64,512]{2,1,0:T(8,128)(2,1)S(1)}, u32[]{:S(2)}, u32[]{:S(2)}) collective-permute-start(bf16[8,64,512]{2,1,0:T(8,128)(2,1)S(1)} %slice.36.refs_0_), channel_id=1, source_target_pairs={{0,8},{8,16},{16,24},{24,0},{1,9},{9,17},{17,25},{25,1},{2,10},{10... | collective-permute-start | bytes 1572872 | tf_op jit(solution)/shard_map/ppermute | solution.py:26
  40.5 31.3 %collective-permute-start.16 = (bf16[8,64,512]{2,1,0:T(8,128)(2,1)S(1)}, bf16[8,64,512]{2,1,0:T(8,128)(2,1)S(1)}, u32[]{:S(2)}, u32[]{:S(2)}) collective-permute-start(bf16[8,64,512]{2,1,0:T(8,128)(2,1)S(1)} %slice.36.refs_0_), channel_id=1, source_target_pairs={{0,16},{8,24},{16,0},{24,8},{1,17},{9,25},{17,1},{25,9},{2,18},{10... | collective-permute-start | bytes 1572872 | tf_op jit(solution)/shard_map/ppermute | solution.py:26
  43.0 28.9 %collective-permute-start.17 = (bf16[8,64,512]{2,1,0:T(8,128)(2,1)S(1)}, bf16[8,64,512]{2,1,0:T(8,128)(2,1)S(1)}, u32[]{:S(2)}, u32[]{:S(2)}) collective-permute-start(bf16[8,64,512]{2,1,0:T(8,128)(2,1)S(1)} %slice.36.refs_0_), channel_id=1, source_target_pairs={{0,24},{8,0},{16,8},{24,16},{1,25},{9,1},{17,9},{25,17},{2,26},{10... | collective-permute-start | bytes 1572872 | tf_op jit(solution)/shard_map/ppermute | solution.py:26
  44.1 4.9 %collective-permute-start.13 = (bf16[24,1792]{1,0:T(8,128)(2,1)S(1)}, bf16[24,1792]{1,0:T(8,128)(2,1)S(1)}, u32[]{:S(2)}, u32[]{:S(2)}) collective-permute-start(bf16[24,1792]{1,0:T(8,128)(2,1)S(1)} %get-tuple-element.44), channel_id=1, source_target_pairs={{0,224},{32,0},{64,32},{96,64},{128,96},{160,128},{192,160},{224,1... | collective-permute-start | bytes 258056 | tf_op jit(solution)/shard_map/ppermute | solution.py:26
  46.8 7.4 %collective-permute-start.7 = (bf16[24,1792]{1,0:T(8,128)(2,1)S(1)}, bf16[24,1792]{1,0:T(8,128)(2,1)S(1)}, u32[]{:S(2)}, u32[]{:S(2)}) collective-permute-start(bf16[24,1792]{1,0:T(8,128)(2,1)S(1)} %get-tuple-element.38), channel_id=1, source_target_pairs={{0,128},{32,160},{64,192},{96,224},{128,0},{160,32},{192,64},{224,... | collective-permute-start | bytes 258056 | tf_op jit(solution)/shard_map/ppermute | solution.py:26
  49.0 6.5 %collective-permute-start.8 = (bf16[24,1792]{1,0:T(8,128)(2,1)S(1)}, bf16[24,1792]{1,0:T(8,128)(2,1)S(1)}, u32[]{:S(2)}, u32[]{:S(2)}) collective-permute-start(bf16[24,1792]{1,0:T(8,128)(2,1)S(1)} %get-tuple-element.39), channel_id=1, source_target_pairs={{0,96},{32,128},{64,160},{96,192},{128,224},{160,0},{192,32},{224,... | collective-permute-start | bytes 258056 | tf_op jit(solution)/shard_map/ppermute | solution.py:26
  54.2 5.4 %collective-permute-start.9 = (bf16[24,1792]{1,0:T(8,128)(2,1)S(1)}, bf16[24,1792]{1,0:T(8,128)(2,1)S(1)}, u32[]{:S(2)}, u32[]{:S(2)}) collective-permute-start(bf16[24,1792]{1,0:T(8,128)(2,1)S(1)} %get-tuple-element.40), channel_id=1, source_target_pairs={{0,160},{32,192},{64,224},{96,0},{128,32},{160,64},{192,96},{224,1... | collective-permute-start | bytes 258056 | tf_op jit(solution)/shard_map/ppermute | solution.py:26
  63.0 19.5 %copy-start.12 = (f32[24,4]{0,1:T(4,128)S(1)}, f32[24,4]{0,1:T(4,128)}, u32[]{:S(2)}) copy-start(f32[24,4]{0,1:T(4,128)} %param.33) | copy-start | bytes 1156
  63.0 20.3 %copy-start.3 = (bf16[24,4096]{1,0:T(8,128)(2,1)S(1)}, bf16[24,4096]{1,0:T(8,128)(2,1)}, u32[]{:S(2)}) copy-start(bf16[24,4096]{1,0:T(8,128)(2,1)} %tokens.1) | copy-start | bytes 589828
  63.0 8.8 %collective-permute-start.14 = (bf16[24,512]{1,0:T(8,128)(2,1)S(1)}, bf16[24,512]{1,0:T(8,128)(2,1)S(1)}, u32[]{:S(2)}, u32[]{:S(2)}) collective-permute-start(bf16[24,512]{1,0:T(8,128)(2,1)S(1)} %attend.1.gated), channel_id=1, source_target_pairs={{0,4},{4,0},{1,5},{5,1},{2,6},{6,2},{3,7},{7,3},{8,12},{12,8},{9,1... | collective-permute-start | bytes 73736 | tf_op jit(solution)/shard_map/ppermute | solution.py:26
  73.3 5.1 %collective-permute-start.18 = (bf16[48,512]{1,0:T(8,128)(2,1)S(1)}, bf16[48,512]{1,0:T(8,128)(2,1)S(1)}, u32[]{:S(2)}, u32[]{:S(2)}) collective-permute-start(bf16[48,512]{1,0:T(8,128)(2,1)S(1)} %get-tuple-element.47), channel_id=1, source_target_pairs={{0,1},{1,2},{2,3},{3,0},{4,5},{5,6},{6,7},{7,4},{8,9},{9,10},{10,1... | collective-permute-start | bytes 147464 | tf_op jit(solution)/shard_map/ppermute | solution.py:26
  74.8 4.8 %collective-permute-start.19 = (bf16[48,512]{1,0:T(8,128)(2,1)S(1)}, bf16[48,512]{1,0:T(8,128)(2,1)S(1)}, u32[]{:S(2)}, u32[]{:S(2)}) collective-permute-start(bf16[48,512]{1,0:T(8,128)(2,1)S(1)} %get-tuple-element.48), channel_id=1, source_target_pairs={{0,2},{1,3},{2,0},{3,1},{4,6},{5,7},{6,4},{7,5},{8,10},{9,11},{10,... | collective-permute-start | bytes 147464 | tf_op jit(solution)/shard_map/ppermute | solution.py:26
  77.3 3.2 %collective-permute-start.20 = (bf16[48,512]{1,0:T(8,128)(2,1)S(1)}, bf16[48,512]{1,0:T(8,128)(2,1)S(1)}, u32[]{:S(2)}, u32[]{:S(2)}) collective-permute-start(bf16[48,512]{1,0:T(8,128)(2,1)S(1)} %get-tuple-element.49), channel_id=1, source_target_pairs={{0,3},{1,0},{2,1},{3,2},{4,7},{5,4},{6,5},{7,6},{8,11},{9,8},{10,9... | collective-permute-start | bytes 147464 | tf_op jit(solution)/shard_map/ppermute | solution.py:26
  80.6 2.7 %collective-permute-start.21 = (bf16[24,512]{1,0:T(8,128)(2,1)S(1)}, bf16[24,512]{1,0:T(8,128)(2,1)S(1)}, u32[]{:S(2)}, u32[]{:S(2)}) collective-permute-start(bf16[24,512]{1,0:T(8,128)(2,1)S(1)} %get-tuple-element.67), channel_id=1, source_target_pairs={{0,4},{4,0},{1,5},{5,1},{2,6},{6,2},{3,7},{7,3},{8,12},{12,8},{9,1... | collective-permute-start | bytes 73736 | tf_op jit(solution)/shard_map/ppermute | solution.py:26
  84.2 31.5 %copy-start.6 = (s32[4]{0:T(128)S(1)}, s32[4]{0:T(128)}, u32[]{:S(2)}) copy-start(s32[4]{0:T(128)} %copy-done.5) | copy-start | bytes 52
  104.1 11.6 %collective-permute-start.24 = (bf16[1536,128]{1,0:T(8,128)(2,1)S(1)}, bf16[1536,128]{1,0:T(8,128)(2,1)S(1)}, u32[]{:S(2)}, u32[]{:S(2)}) collective-permute-start(bf16[1536,128]{1,0:T(8,128)(2,1)S(1)} %bitcast.21), channel_id=1, source_target_pairs={{0,1},{1,2},{2,3},{3,0},{4,5},{5,6},{6,7},{7,4},{8,9},{9,10},{10,1... | collective-permute-start | bytes 1179656 | tf_op jit(solution)/shard_map/ppermute | solution.py:26
  108.0 47.5 %collective-permute-start.28 = (bf16[256,1024]{1,0:T(8,128)(2,1)}, bf16[256,1024]{1,0:T(8,128)(2,1)S(1)}, u32[]{:S(2)}, u32[]{:S(2)}) collective-permute-start(bf16[256,1024]{1,0:T(8,128)(2,1)} %get-tuple-element.61), channel_id=1, source_target_pairs={{0,1},{1,2},{2,3},{3,0},{4,5},{5,6},{6,7},{7,4},{8,9},{9,10},{10,1... | collective-permute-start | bytes 1572872 | tf_op jit(solution)/shard_map/ppermute | solution.py:26
  109.0 12.9 %collective-permute-start.23 = (bf16[1536,128]{1,0:T(8,128)(2,1)S(1)}, bf16[1536,128]{1,0:T(8,128)(2,1)S(1)}, u32[]{:S(2)}, u32[]{:S(2)}) collective-permute-start(bf16[1536,128]{1,0:T(8,128)(2,1)S(1)} %bitcast.22), channel_id=1, source_target_pairs={{0,3},{1,0},{2,1},{3,2},{4,7},{5,4},{6,5},{7,6},{8,11},{9,8},{10,9... | collective-permute-start | bytes 1179656 | tf_op jit(solution)/shard_map/ppermute | solution.py:26
  110.8 44.9 %collective-permute-start.29 = (bf16[256,1024]{1,0:T(8,128)(2,1)}, bf16[256,1024]{1,0:T(8,128)(2,1)S(1)}, u32[]{:S(2)}, u32[]{:S(2)}) collective-permute-start(bf16[256,1024]{1,0:T(8,128)(2,1)} %get-tuple-element.62), channel_id=1, source_target_pairs={{0,2},{1,3},{2,0},{3,1},{4,6},{5,7},{6,4},{7,5},{8,10},{9,11},{10,... | collective-permute-start | bytes 1572872 | tf_op jit(solution)/shard_map/ppermute | solution.py:26
  113.0 42.7 %collective-permute-start.30 = (bf16[256,1024]{1,0:T(8,128)(2,1)}, bf16[256,1024]{1,0:T(8,128)(2,1)S(1)}, u32[]{:S(2)}, u32[]{:S(2)}) collective-permute-start(bf16[256,1024]{1,0:T(8,128)(2,1)} %get-tuple-element.63), channel_id=1, source_target_pairs={{0,3},{1,0},{2,1},{3,2},{4,7},{5,4},{6,5},{7,6},{8,11},{9,8},{10,9... | collective-permute-start | bytes 1572872 | tf_op jit(solution)/shard_map/ppermute | solution.py:26
  115.7 31.7 %collective-permute-start.22 = (bf16[1536,128]{1,0:T(8,128)(2,1)S(1)}, bf16[1536,128]{1,0:T(8,128)(2,1)S(1)}, u32[]{:S(2)}, u32[]{:S(2)}) collective-permute-start(bf16[1536,128]{1,0:T(8,128)(2,1)S(1)} %bitcast.23), channel_id=1, source_target_pairs={{0,2},{1,3},{2,0},{3,1},{4,6},{5,7},{6,4},{7,5},{8,10},{9,11},{10,... | collective-permute-start | bytes 1179656 | tf_op jit(solution)/shard_map/ppermute | solution.py:26
  115.7 1.6 copy-start
  117.3 1.6 copy-start.1
  121.9 33.8 %copy-start.4 = (bf16[256,1024]{1,0:T(8,128)(2,1)S(1)}, bf16[256,1024]{1,0:T(8,128)(2,1)}, u32[]{:S(2)}) copy-start(bf16[256,1024]{1,0:T(8,128)(2,1)} %get-tuple-element.60.refs_0_) | copy-start | bytes 1572868
  148.4 7.9 %collective-permute-start.25 = (bf16[192,256]{1,0:T(8,128)(2,1)S(1)}, bf16[192,256]{1,0:T(8,128)(2,1)S(1)}, u32[]{:S(2)}, u32[]{:S(2)}) collective-permute-start(bf16[192,256]{1,0:T(8,128)(2,1)S(1)} %expert.7.refs_0_), channel_id=1, source_target_pairs={{0,1},{1,2},{2,3},{3,0},{4,5},{5,6},{6,7},{7,4},{8,9},{9,10},{10,1... | collective-permute-start | bytes 294920 | tf_op jit(solution)/shard_map/ppermute | solution.py:26
  153.2 5.6 %collective-permute-start.26 = (bf16[192,256]{1,0:T(8,128)(2,1)S(1)}, bf16[192,256]{1,0:T(8,128)(2,1)S(1)}, u32[]{:S(2)}, u32[]{:S(2)}) collective-permute-start(bf16[192,256]{1,0:T(8,128)(2,1)S(1)} %expert.7.refs_0_), channel_id=1, source_target_pairs={{0,2},{1,3},{2,0},{3,1},{4,6},{5,7},{6,4},{7,5},{8,10},{9,11},{10,... | collective-permute-start | bytes 294920 | tf_op jit(solution)/shard_map/ppermute | solution.py:26
  155.5 4.7 %collective-permute-start.27 = (bf16[192,256]{1,0:T(8,128)(2,1)S(1)}, bf16[192,256]{1,0:T(8,128)(2,1)S(1)}, u32[]{:S(2)}, u32[]{:S(2)}) collective-permute-start(bf16[192,256]{1,0:T(8,128)(2,1)S(1)} %expert.7.refs_0_), channel_id=1, source_target_pairs={{0,3},{1,0},{2,1},{3,2},{4,7},{5,4},{6,5},{7,6},{8,11},{9,8},{10,9... | collective-permute-start | bytes 294920 | tf_op jit(solution)/shard_map/ppermute | solution.py:26
  161.6 21.8 %all-to-all-start.2 = ((bf16[64,24,128]{2,1,0:T(8,128)(2,1)}), bf16[64,24,128]{2,1,0:T(8,128)(2,1)S(1)}, u32[]{:S(2)}, u32[]{:S(2)}) async-start(bf16[64,24,128]{2,1,0:T(8,128)(2,1)} %bitcast.14), calls=%async_computation.2 | async-start | bytes 786432 | tf_op jit(solution)/shard_map/all_to_all | solution.py:643
  183.7 4.2 %collective-permute-start.31 = (bf16[24,1024]{1,0:T(8,128)(2,1)S(1)}, bf16[24,1024]{1,0:T(8,128)(2,1)S(1)}, u32[]{:S(2)}, u32[]{:S(2)}) collective-permute-start(bf16[24,1024]{1,0:T(8,128)(2,1)S(1)} %combine.1.refs_0_), channel_id=1, source_target_pairs={{0,1},{1,2},{2,3},{3,0},{4,5},{5,6},{6,7},{7,4},{8,9},{9,10},{10,1... | collective-permute-start | bytes 147464 | tf_op jit(solution)/shard_map/ppermute | solution.py:26
  183.8 5.1 %collective-permute-start.32 = (bf16[24,1024]{1,0:T(8,128)(2,1)S(1)}, bf16[24,1024]{1,0:T(8,128)(2,1)S(1)}, u32[]{:S(2)}, u32[]{:S(2)}) collective-permute-start(bf16[24,1024]{1,0:T(8,128)(2,1)S(1)} %combine.1.refs_0_), channel_id=1, source_target_pairs={{0,2},{1,3},{2,0},{3,1},{4,6},{5,7},{6,4},{7,5},{8,10},{9,11},{10,... | collective-permute-start | bytes 147464 | tf_op jit(solution)/shard_map/ppermute | solution.py:26
  186.6 3.4 %collective-permute-start.33 = (bf16[24,1024]{1,0:T(8,128)(2,1)S(1)}, bf16[24,1024]{1,0:T(8,128)(2,1)S(1)}, u32[]{:S(2)}, u32[]{:S(2)}) collective-permute-start(bf16[24,1024]{1,0:T(8,128)(2,1)S(1)} %combine.1.refs_0_), channel_id=1, source_target_pairs={{0,3},{1,0},{2,1},{3,2},{4,7},{5,4},{6,5},{7,6},{8,11},{9,8},{10,9... | collective-permute-start | bytes 147464 | tf_op jit(solution)/shard_map/ppermute | solution.py:26
